TPU v7x, 256 devices: a whole 4x4x8 slice. The times are simulated.
256 devices in a mesh: kv: 32 (over z, x), tp: 8 (over y, core).
Axes of the slice: x: 4, y: 4, z: 8, core: 2. Of those that a mesh axis runs over, the one named last changes fastest.
Arguments:
- tokens: bfloat16 [32768, 2048], P('kv'), may hold values from -72 to 72
- query_weight: bfloat16 [2048, 2048], P(None, 'tp'), may hold values from -0.125 to 0.125
- key_projection_matrix: bfloat16 [2048, 1024], P(None, 'tp'), may hold values from -0.125 to 0.125
- value_projection_matrix: bfloat16 [2048, 1024], P(None, 'tp'), may hold values from -0.125 to 0.125
- out_weight: bfloat16 [2048, 2048], P('tp'), may hold values from -1.5 to 1.5
- chosen: int32 [256, 12], P('kv'), may hold values from -1 to 1023, as said below
Outputs:
- layer_out: bfloat16 [32768, 2048], P(('kv', 'tp'))
Inputs may be any that keep to these rules, and one draw needn't show every extreme that they name: `chosen`: positions are grouped in consecutive groups of 1024. The blocks named in one row lie in distinct groups, all earlier than the group of the row's query block; a query block in group g has exactly min(12, g) entries that are not -1, first in its row, and the rest are -1. So the query blocks of one group name at most 8 blocks of any one other group, and in every draw some group's query blocks all name blocks of one same earlier group.
All inputs are finite; a program needn't handle non-finite values.
Results may differ from a plain program's by a relative error of at most 0.014.
The roundings to bfloat16 on the way count: a program that leaves them out, or rounds other values in their place, can miss the bound.
Values may be sent and summed in bfloat16 or wider, within the bound.
No kernel may reach another device: no remote copies, remote signals or barrier semaphores. Data moves between devices by JAX's collectives and lax.ppermute only.
A program may use at most 64 MiB of HBM per device.

v0:
```python
import jax
import jax.numpy as jnp
from jax import lax
from jax.sharding import PartitionSpec as P

HEAD_SIZE = 128
QUERY_BLOCK_SPAN = 128
KEY_BLOCK_SPAN = 32
NFAR = 12


def joined_along(blocks, dim):
    dims = list(blocks.shape[1:])
    dims[dim] *= blocks.shape[0]
    return jnp.moveaxis(blocks, 0, dim).reshape(dims)


def from_everyone(x, axis):
    size = lax.axis_size(axis)
    return lax.all_to_all(jnp.broadcast_to(x[None], (size, *x.shape)), axis, 0, 0, tiled=True)


def gather_directly(x, axis, dim):
    return joined_along(from_everyone(x, axis), dim)


def shards(
    tokens, query_weight, key_projection_matrix, value_projection_matrix, out_weight, chosen
):
    tok_rows = tokens.shape[0]
    kv_width = key_projection_matrix.shape[1]
    kv_heads = kv_width // HEAD_SIZE
    q_heads = query_weight.shape[1] // HEAD_SIZE
    grouped_head_index = q_heads // kv_heads
    query_blocks = tok_rows // QUERY_BLOCK_SPAN
    blocked_keys = tok_rows // KEY_BLOCK_SPAN
    queries = jnp.dot(tokens, query_weight, preferred_element_type=jnp.float32).astype(jnp.bfloat16)
    key_vectors = jnp.dot(tokens, key_projection_matrix, preferred_element_type=jnp.float32).astype(
        jnp.bfloat16
    )
    value_vectors = jnp.dot(
        tokens, value_projection_matrix, preferred_element_type=jnp.float32
    ).astype(jnp.bfloat16)
    my_index = lax.axis_index("kv")
    key_rows = key_vectors.reshape(blocked_keys, KEY_BLOCK_SPAN, kv_width)
    value_rows = value_vectors.reshape(blocked_keys, KEY_BLOCK_SPAN, kv_width)
    all_lists = gather_directly(chosen, "kv", 0)
    peer_count = all_lists.shape[0] // query_blocks
    asked_ids = all_lists.reshape(peer_count, query_blocks, NFAR)
    is_mine = (asked_ids >= 0) & (asked_ids // blocked_keys == my_index)
    wanted = jnp.sum(jnp.where(is_mine, asked_ids - my_index * blocked_keys, 0), axis=2)
    received = (
        lax.all_to_all(key_rows[wanted], "kv", split_axis=0, concat_axis=0, tiled=True),
        lax.all_to_all(value_rows[wanted], "kv", split_axis=0, concat_axis=0, tiled=True),
    )
    owners = jnp.where(chosen >= 0, chosen // blocked_keys, 0)
    block_slot = jnp.arange(query_blocks, dtype=jnp.int32)[:, None]
    far_keys = received[0][owners, block_slot]
    far_values = received[1][owners, block_slot]
    listed_keys = QUERY_BLOCK_SPAN + NFAR * KEY_BLOCK_SPAN
    row_offset = my_index * tok_rows
    query_pos = row_offset + jnp.arange(tok_rows, dtype=jnp.int32).reshape(
        query_blocks, QUERY_BLOCK_SPAN
    )
    far_pos = (
        jnp.maximum(chosen, 0)[:, :, None] * KEY_BLOCK_SPAN
        + jnp.arange(KEY_BLOCK_SPAN, dtype=jnp.int32)
    ).reshape(query_blocks, NFAR * KEY_BLOCK_SPAN)
    far_ok = jnp.broadcast_to(
        (chosen >= 0)[:, :, None], (query_blocks, NFAR, KEY_BLOCK_SPAN)
    ).reshape(query_blocks, NFAR * KEY_BLOCK_SPAN)
    key_pos = jnp.concatenate([query_pos, far_pos], axis=1)
    key_ok = jnp.concatenate(
        [jnp.ones((query_blocks, QUERY_BLOCK_SPAN), dtype=bool), far_ok], axis=1
    )
    allowed = key_ok[:, None, :] & (key_pos[:, None, :] <= query_pos[:, :, None])
    all_keys = jnp.concatenate(
        [
            key_vectors.reshape(query_blocks, QUERY_BLOCK_SPAN, kv_width),
            far_keys.reshape(query_blocks, NFAR * KEY_BLOCK_SPAN, kv_width),
        ],
        axis=1,
    )
    all_values = jnp.concatenate(
        [
            value_vectors.reshape(query_blocks, QUERY_BLOCK_SPAN, kv_width),
            far_values.reshape(query_blocks, NFAR * KEY_BLOCK_SPAN, kv_width),
        ],
        axis=1,
    )
    grouped = queries.reshape(
        query_blocks, QUERY_BLOCK_SPAN, kv_heads, grouped_head_index, HEAD_SIZE
    )
    scores = jnp.einsum(
        "bqgrd,bkgd->bgrqk",
        grouped,
        all_keys.reshape(query_blocks, listed_keys, kv_heads, HEAD_SIZE),
        preferred_element_type=jnp.float32,
    ) * HEAD_SIZE ** (-0.5)
    scores = jnp.where(allowed[:, None, None], scores, -jnp.inf)
    row_max = jnp.max(scores, axis=-1, keepdims=True)
    exp_scores = jnp.exp(scores - row_max)
    row_sum = jnp.sum(exp_scores, axis=-1, keepdims=True)
    weights = (exp_scores / row_sum).astype(jnp.bfloat16)
    mixed = jnp.einsum(
        "bgrqk,bkgd->bqgrd",
        weights,
        all_values.reshape(query_blocks, listed_keys, kv_heads, HEAD_SIZE),
        preferred_element_type=jnp.float32,
    )
    mixed = mixed.astype(jnp.bfloat16).reshape(tok_rows, q_heads * HEAD_SIZE)
    return lax.psum_scatter(
        jnp.dot(mixed, out_weight, preferred_element_type=jnp.float32).astype(jnp.bfloat16),
        "tp",
        scatter_dimension=0,
        tiled=True,
    )


def solution(mesh):
    return jax.shard_map(
        shards,
        mesh=mesh,
        in_specs=(
            P("kv", None),
            P(None, "tp"),
            P(None, "tp"),
            P(None, "tp"),
            P("tp", None),
            P("kv", None),
        ),
        out_specs=P(("kv", "tp"), None),
        check_vma=False,
    )
```

profile of v0, /device:TPU:2, one launch (start us, length us, event | category | flops | bytes accessed | tf_op | source)
XLA Modules:
  0.0 195.8 jit_solution(3449374113824474936)
XLA Ops:
  6.5 0.0 copy-start
  6.5 1.4 broadcast_in_dim.20
  8.0 11.6 %all-to-all-start = ((s32[32,8,12]{2,1,0:T(8,128)}), s32[32,8,12]{2,1,0:T(8,128)S(1)}, u32[]{:S(2)}, u32[]{:S(2)}) async-start(s32[32,8,12]{2,1,0:T(8,128)} %broadcast_in_dim.20), calls=%async_computation | async-start | bytes 262144 | tf_op jit(solution)/shard_map/all_to_all | solution.py:20
  19.6 3.5 %convolution_convert_fusion.3 = bf16[1024,128]{1,0:T(8,128)(2,1)S(1)} fusion(bf16[1024,2048]{1,0:T(8,128)(2,1)} %param.6, bf16[2048,128]{1,0:T(8,128)(2,1)} %param.9), kind=kOutput, calls=%fused_computation.18 | convolution fusion | flops 537001984 | bytes 4980736 | tf_op jit(solution)/shard_map/dot_general | solution.py:41
  23.2 5.3 %all-to-all-done = s32[32,8,12]{2,1,0:T(8,128)S(1)} async-done(((s32[32,8,12]{2,1,0:T(8,128)}), s32[32,8,12]{2,1,0:T(8,128)S(1)}, u32[]{:S(2)}, u32[]{:S(2)}) %all-to-all-start) | async-done | bytes 12320 | tf_op jit(solution)/shard_map/all_to_all | solution.py:20
  28.5 0.6 select_reduce_fusion
  29.1 0.1 copy.40
  29.2 0.1 copy.31
  29.2 0.1 reshape.112
  29.4 0.0 copy-start.4
  29.4 2.2 %gather_fusion = bf16[256,32,128]{2,1,0:T(8,128)(2,1)} fusion(bf16[32,32,128]{2,1,0:T(8,128)(2,1)S(1)} %bitcast.72, s32[1024]{0:T(1024)S(1)} %pad_clamp_fusion), kind=kCustom, calls=%fused_computation | custom fusion | bytes 4195328 | tf_op jit(solution)/shard_map/gather | solution.py:54
  31.5 6.2 %all-to-all-start.1 = ((bf16[32,8,32,128]{3,2,1,0:T(8,128)(2,1)}), bf16[32,8,32,128]{3,2,1,0:T(8,128)(2,1)}, u32[]{:S(2)}, u32[]{:S(2)}) async-start(bf16[32,8,32,128]{3,2,1,0:T(8,128)(2,1)} %bitcast.3), calls=%async_computation.1 | async-start | bytes 4194304 | tf_op jit(solution)/shard_map/all_to_all | solution.py:54
  37.7 0.0 copy-done.4
  37.7 3.4 %convolution_convert_fusion.2 = bf16[1024,128]{1,0:T(8,128)(2,1)S(1)} fusion(bf16[1024,2048]{1,0:T(8,128)(2,1)} %param.6, bf16[2048,128]{1,0:T(8,128)(2,1)S(1)} %copy-done.4), kind=kOutput, calls=%fused_computation.17 | convolution fusion | flops 537001984 | bytes 4980736 | tf_op jit(solution)/shard_map/dot_general | solution.py:38
  41.2 0.0 copy-start.3
  41.2 2.2 %gather_fusion.2 = bf16[256,32,128]{2,1,0:T(8,128)(2,1)} fusion(bf16[32,32,128]{2,1,0:T(8,128)(2,1)S(1)} %bitcast.74, s32[1024]{0:T(1024)S(1)} %pad_clamp_fusion), kind=kCustom, calls=%fused_computation.2 | custom fusion | bytes 4195328 | tf_op jit(solution)/shard_map/gather | solution.py:53
  43.4 43.0 %all-to-all-done.1 = bf16[32,8,32,128]{3,2,1,0:T(8,128)(2,1)} async-done(((bf16[32,8,32,128]{3,2,1,0:T(8,128)(2,1)}), bf16[32,8,32,128]{3,2,1,0:T(8,128)(2,1)}, u32[]{:S(2)}, u32[]{:S(2)}) %all-to-all-start.1) | async-done | bytes 2097184 | tf_op jit(solution)/shard_map/all_to_all | solution.py:54
  86.3 6.6 %all-to-all-start.2 = ((bf16[32,8,32,128]{3,2,1,0:T(8,128)(2,1)}), bf16[32,8,32,128]{3,2,1,0:T(8,128)(2,1)}, u32[]{:S(2)}, u32[]{:S(2)}) async-start(bf16[32,8,32,128]{3,2,1,0:T(8,128)(2,1)} %bitcast.76), calls=%async_computation.2 | async-start | bytes 4194304 | tf_op jit(solution)/shard_map/all_to_all | solution.py:53
  92.9 0.2 reduce-scatter.2.cloned.1.call-start
  93.1 0.0 copy-done.3
  93.2 0.1 reshape.118
  93.2 0.1 add.63
  93.3 0.1 broadcast_in_dim.23
  93.4 0.1 reshape.100
  93.5 0.1 add.60
  93.6 0.1 add.61
  93.7 0.9 copy.32
  94.6 3.7 %convolution_convert_fusion.1 = bf16[1024,256]{1,0:T(8,128)(2,1)S(1)} fusion(bf16[1024,2048]{1,0:T(8,128)(2,1)} %param.6, bf16[2048,256]{1,0:T(8,128)(2,1)} %param.7), kind=kOutput, calls=%fused_computation.15 | convolution fusion | flops 1074003968 | bytes 5767168 | tf_op jit(solution)/shard_map/dot_general | solution.py:37
  98.3 0.1 reshape.107
  98.5 1.4 compare_and_fusion
  99.9 2.7 %gather_fusion.1 = bf16[96,32,128]{2,1,0:T(8,128)(2,1)S(1)} fusion(bf16[32,8,32,128]{3,2,1,0:T(8,128)(2,1)} %all-to-all-done.1, s32[96]{0:T(128)S(1)} %reshape.118), kind=kCustom, calls=%fused_computation.1 | custom fusion | bytes 1573632 | tf_op jit(solution)/shard_map/gather | solution.py:59
  102.7 1.2 copy.33
  103.9 37.1 %all-to-all-done.2 = bf16[32,8,32,128]{3,2,1,0:T(8,128)(2,1)} async-done(((bf16[32,8,32,128]{3,2,1,0:T(8,128)(2,1)}), bf16[32,8,32,128]{3,2,1,0:T(8,128)(2,1)}, u32[]{:S(2)}, u32[]{:S(2)}) %all-to-all-start.2) | async-done | bytes 2097184 | tf_op jit(solution)/shard_map/all_to_all | solution.py:53
  141.0 2.7 %gather_fusion.3 = bf16[96,32,128]{2,1,0:T(8,128)(2,1)S(1)} fusion(bf16[32,8,32,128]{3,2,1,0:T(8,128)(2,1)} %all-to-all-done.2, s32[96]{0:T(128)S(1)} %reshape.118), kind=kCustom, calls=%fused_computation.3 | custom fusion | bytes 1573632 | tf_op jit(solution)/shard_map/gather | solution.py:58
  143.8 0.8 fusion.1
  144.5 0.0 copy-start.1
  144.5 0.0 copy-start.2
  144.6 1.0 fusion
  145.5 0.1 copy-done.1
  145.7 0.1 copy-done.2
  145.7 1.3 fusion.8
  147.1 0.3 copy.36
  147.4 0.0 copy-done
  147.4 3.2 %convolution_convert_fusion = bf16[1024,2048]{1,0:T(8,128)(2,1)} fusion(bf16[256,2048]{1,0:T(8,128)(2,1)S(1)} %copy-done, bf16[32,8,8,128]{3,2,1,0:T(8,128)(2,1)S(1)} %bitcast.77), kind=kOutput, calls=%fused_computation.7 | convolution fusion | flops 1075838976 | bytes 5767168 | tf_op jit(solution)/shard_map/dot_general | solution.py:113
  150.7 0.0 reduce-scatter.2.cloned.1.call-update
  150.7 38.2 %reduce-scatter.2.cloned.1.call-done = bf16[128,2048]{1,0:T(8,128)(2,1)} async-done(((bf16[1024,2048]{1,0:T(8,128)(2,1)}), bf16[128,2048]{1,0:T(8,128)(2,1)}) %reduce-scatter.2.cloned.1.call-update) | async-done | bytes 524304 | tf_op jit(solution)/shard_map/reduce_scatter | solution.py:112
  (10 shorter events, 0.1 us)
Async XLA Ops:
  6.5 140.9 %copy-start = (bf16[256,2048]{1,0:T(8,128)(2,1)S(1)}, bf16[256,2048]{1,0:T(8,128)(2,1)}, u32[]{:S(2)}) copy-start(bf16[256,2048]{1,0:T(8,128)(2,1)} %param.10) | copy-start | bytes 3145732
  8.0 20.5 %all-to-all-start = ((s32[32,8,12]{2,1,0:T(8,128)}), s32[32,8,12]{2,1,0:T(8,128)S(1)}, u32[]{:S(2)}, u32[]{:S(2)}) async-start(s32[32,8,12]{2,1,0:T(8,128)} %broadcast_in_dim.20), calls=%async_computation | async-start | bytes 262144 | tf_op jit(solution)/shard_map/all_to_all | solution.py:20
  29.4 8.4 %copy-start.4 = (bf16[2048,128]{1,0:T(8,128)(2,1)S(1)}, bf16[2048,128]{1,0:T(8,128)(2,1)}, u32[]{:S(2)}) copy-start(bf16[2048,128]{1,0:T(8,128)(2,1)} %param.8) | copy-start | bytes 1572868
  31.5 54.8 %all-to-all-start.1 = ((bf16[32,8,32,128]{3,2,1,0:T(8,128)(2,1)}), bf16[32,8,32,128]{3,2,1,0:T(8,128)(2,1)}, u32[]{:S(2)}, u32[]{:S(2)}) async-start(bf16[32,8,32,128]{3,2,1,0:T(8,128)(2,1)} %bitcast.3), calls=%async_computation.1 | async-start | bytes 4194304 | tf_op jit(solution)/shard_map/all_to_all | solution.py:54
  41.2 52.0 %copy-start.3 = (s32[8,12]{1,0:T(8,128)S(1)}, s32[8,12]{1,0:T(8,128)}, u32[]{:S(2)}) copy-start(s32[8,12]{1,0:T(8,128)} %param.11) | copy-start | bytes 1156
  86.3 54.7 %all-to-all-start.2 = ((bf16[32,8,32,128]{3,2,1,0:T(8,128)(2,1)}), bf16[32,8,32,128]{3,2,1,0:T(8,128)(2,1)}, u32[]{:S(2)}, u32[]{:S(2)}) async-start(bf16[32,8,32,128]{3,2,1,0:T(8,128)(2,1)} %bitcast.76), calls=%async_computation.2 | async-start | bytes 4194304 | tf_op jit(solution)/shard_map/all_to_all | solution.py:53
  92.9 96.0 %reduce-scatter.2.cloned.1.call-start = ((), (), s32[]{:S(2)}) async-start(), calls=%async_computation.4 | async-start | bytes 4718592 | tf_op jit(solution)/shard_map/reduce_scatter | solution.py:112
  144.5 1.1 copy-start.1
  144.5 1.2 copy-start.2
Sparse Core Ops, SparseCore 0:
  150.8 38.0 reduce-scatter.1
where the time goes:
time: 196 us
  waiting for transfers between devices  124 us (63%)
  starting transfers between devices  24.6 us (13%)
  matrix products  16.1 us (8%)
  local copies, waits for them, and re-layouts  14.8 us (8%)
  between operations  13.6 us (7%)
  other arithmetic  3.09 us (2%)
    all_to_all x1, waiting for transfers between devices, shards(): lax.all_to_all(value_rows[wanted], 'kv', split_axis=0, concat_axis=0, til...  43 us
    reduce_scatter x1, waiting for transfers between devices, shards(): lax.psum_scatter(jnp.dot(mixed, out_weight, preferred_element_type=jnp.fl...  38.2 us
    all_to_all x1, waiting for transfers between devices, shards(): lax.all_to_all(key_rows[wanted], 'kv', split_axis=0, concat_axis=0, tiled...  37.1 us
    all_to_all x1, starting transfers between devices, from_everyone(): lax.all_to_all(jnp.broadcast_to(x[None], (size, *x.shape)), axis, 0, 0, t...  11.6 us
    all_to_all x1, starting transfers between devices, shards(): lax.all_to_all(key_rows[wanted], 'kv', split_axis=0, concat_axis=0, tiled...  6.55 us
    all_to_all x1, starting transfers between devices, shards(): lax.all_to_all(value_rows[wanted], 'kv', split_axis=0, concat_axis=0, til...  6.16 us
    all_to_all x1, waiting for transfers between devices, from_everyone(): lax.all_to_all(jnp.broadcast_to(x[None], (size, *x.shape)), axis, 0, 0, t...  5.3 us
  transfers between devices with their start and end apart: 4, of which 4 were waited for; matrix products, arithmetic and copies ran while one was open for 10% of the time, Pallas kernels for 0%

commit v1 on v0

v1 whole, which is shorter than its diff:
```python
import jax
import jax.numpy as jnp
from jax import lax
from jax.experimental import pallas as pl
from jax.experimental.pallas import tpu as pltpu
from jax.sharding import PartitionSpec as P

HEAD = 128
QB = 128
KB = 32
NFAR = 12
NX = 4
NZ = 8
NY = 4
BF = jnp.bfloat16
F32 = jnp.float32
NT = (((1,), (1,)), ((), ()))


CORES = [(t, t ^ 1) for t in range(2 * NY)]


def along_z(k):
    return [(z * NX + x, (z + k) % NZ * NX + x) for z in range(NZ) for x in range(NX)]


def along_x(k):
    return [(z * NX + x, z * NX + (x + k) % NX) for z in range(NZ) for x in range(NX)]


def along_y(k):
    return [(y * 2 + c, (y + k) % NY * 2 + c) for y in range(NY) for c in range(2)]


def dot(a, b):
    return jnp.dot(a, b, preferred_element_type=F32)


VMEM = pl.BlockSpec(memory_space=pltpu.VMEM)
SMEM = pl.BlockSpec(memory_space=pltpu.SMEM)


def params(mib):
    return pltpu.CompilerParams(vmem_limit_bytes=mib * 1024 * 1024)


def pick_body(count):
    def body(want, *refs):
        ins, outs = refs[: 2 * count], refs[2 * count :]

        def step(j, carry):
            for d in range(count):
                for r in range(NX):
                    b = pl.multiple_of(want[r, d * 8 + j] * KB, KB)
                    for s in range(2):
                        outs[r][d, s, j] = ins[2 * d + s][pl.ds(b, KB), :]
            return carry

        lax.fori_loop(0, 8, step, 0)

    return body


def pick(want, pairs):
    count = len(pairs)
    return pl.pallas_call(
        pick_body(count),
        out_shape=[jax.ShapeDtypeStruct((count, 2, 8, KB, HEAD), BF)] * NX,
        in_specs=[SMEM] + [VMEM] * (2 * count),
        out_specs=[VMEM] * NX,
        compiler_params=params(8),
        cost_estimate=pl.CostEstimate(
            flops=4_000_000 * count, bytes_accessed=1_000_000 * count, transcendentals=0
        ),
    )(want, *[a for p in pairs for a in p])


def attend_body(counts):
    def body(place, named, q, k, v, *refs):
        recv, (out, kbuf, vbuf) = refs[:-3], refs[-3:]
        far = NFAR * KB
        row = lax.broadcasted_iota(jnp.int32, (2 * QB, QB), 0) % QB
        col = lax.broadcasted_iota(jnp.int32, (2 * QB, QB), 1)
        causal = jnp.where(col <= row, 0.0, -jnp.inf).astype(F32)
        scale = HEAD ** (-0.5)

        def step(j, carry):
            at = pl.multiple_of(j * QB, QB)
            vbuf[...] = jnp.zeros_like(vbuf)
            slot = 0
            for b, count in enumerate(counts):
                for d in range(count):
                    for r in range(NX):
                        p = pl.multiple_of(place[j, slot] * KB, KB)
                        kbuf[pl.ds(p, KB), :] = recv[NX * b + r][d, 0, j]
                        vbuf[pl.ds(p, KB), :] = recv[NX * b + r][d, 1, j]
                        slot += 1
            fcol = lax.broadcasted_iota(jnp.int32, (1, far), 1)
            bias = jnp.where(fcol < named[j] * KB, 0.0, -jnp.inf).astype(F32)
            qq = jnp.concatenate([q[pl.ds(at, QB), :HEAD], q[pl.ds(at, QB), HEAD:]], axis=0)
            own = lax.dot_general(qq, k[pl.ds(at, QB), :], NT, preferred_element_type=F32)
            oth = lax.dot_general(qq, kbuf[:far, :], NT, preferred_element_type=F32)
            own = own * scale + causal
            oth = oth * scale + bias
            top = jnp.maximum(jnp.max(own, axis=1, keepdims=True), jnp.max(oth, axis=1, keepdims=True))
            own = jnp.exp(own - top)
            oth = jnp.exp(oth - top)
            total = jnp.sum(own, axis=1, keepdims=True) + jnp.sum(oth, axis=1, keepdims=True)
            inv = 1.0 / total
            mixed = dot((own * inv).astype(BF), v[pl.ds(at, QB), :])
            mixed = (mixed + dot((oth * inv).astype(BF), vbuf[:far, :])).astype(BF)
            out[pl.ds(at, QB), :HEAD] = mixed[:QB]
            out[pl.ds(at, QB), HEAD:] = mixed[QB:]
            return carry

        lax.fori_loop(0, q.shape[0] // QB, step, 0)

    return body


def attend(place, named, q, k, v, recv):
    counts = [r[0].shape[0] for r in recv]
    return pl.pallas_call(
        attend_body(counts),
        out_shape=jax.ShapeDtypeStruct(q.shape, BF),
        in_specs=[SMEM, SMEM] + [VMEM] * (3 + NX * len(recv)),
        out_specs=VMEM,
        scratch_shapes=[pltpu.VMEM(((NFAR + 1) * KB, HEAD), BF)] * 2,
        compiler_params=params(16),
        cost_estimate=pl.CostEstimate(
            flops=600_000_000, bytes_accessed=6_000_000, transcendentals=1_000_000
        ),
        name="attend",
    )(place, named, q, k, v, *[a for r in recv for a in r])


def project_body(spot, att, *refs):
    weights, out = refs[:-1], refs[-1]
    tile = 256

    def step(n, carry):
        cols = pl.ds(pl.multiple_of(n * tile, tile), tile)
        acc = jnp.zeros((QB, tile), F32)
        for core in range(2):
            w0, wm, wp, top, low = weights[5 * core : 5 * core + 5]
            for i, w in enumerate((w0, wm, wp)):
                acc += dot(att[spot[core, i]], w[:, cols]).astype(BF).astype(F32)
            a = att[spot[core, 3]]
            part = dot(a[:, :HEAD], top[:, cols]) + dot(a[:, HEAD:], low[:, cols])
            acc += part.astype(BF).astype(F32)
        out[:, cols] = acc.astype(BF)
        return carry

    lax.fori_loop(0, out.shape[1] // tile, step, 0)


def project(spot, att, weights):
    width = weights[0].shape[1]
    return pl.pallas_call(
        project_body,
        out_shape=jax.ShapeDtypeStruct((QB, width), BF),
        in_specs=[SMEM] + [VMEM] * (1 + len(weights)),
        out_specs=VMEM,
        compiler_params=params(14),
        cost_estimate=pl.CostEstimate(
            flops=1_000_000_000, bytes_accessed=9_000_000, transcendentals=0
        ),
        name="project",
    )(spot, att, *weights)


def layer(tokens, wq, wk, wv, wo, chosen):
    me = lax.axis_index("kv")
    z, x = me // NX, me % NX
    tp = lax.axis_index("tp")
    per = tokens.shape[0] // KB

    lists = [chosen] + [lax.ppermute(chosen, "kv", along_x(-r)) for r in range(1, NX)]
    k = dot(tokens, wk).astype(BF)
    v = dot(tokens, wv).astype(BF)

    dist = jnp.arange(NZ, dtype=jnp.int32)
    step_x = jnp.arange(NX, dtype=jnp.int32)
    home = (z - dist) % NZ * NX
    lists = jnp.stack(lists)[:, None]
    mine = lists // per == (home + x)[None, :, None, None]
    want = jnp.sum(jnp.where(mine, lists % per, 0), axis=3)
    source = home[:, None] + (x - step_x) % NX
    here = chosen[:, None, None, :] // per == source[None, :, :, None]
    order = jnp.arange(NFAR, dtype=jnp.int32) - NFAR
    place = NFAR + jnp.sum(jnp.where(here, order, 0), axis=3)
    named = jnp.sum((chosen >= 0).astype(jnp.int32), axis=1)

    up, down = along_z(1), along_z(-1)
    got_k, got_v = {0: k}, {0: v}
    uk, uv, dk, dv = k, v, k, v
    for step in range(1, NZ // 2 + 1):
        uk = got_k[step] = lax.ppermute(uk, "kv", up)
        if step < NZ // 2:
            dk = got_k[NZ - step] = lax.ppermute(dk, "kv", down)
            uv = got_v[step] = lax.ppermute(uv, "kv", up)
        dv = got_v[NZ - step] = lax.ppermute(dv, "kv", down)

    batches = [[0]] + [[s, NZ - s] for s in range(1, NZ // 2)] + [[NZ // 2]]
    recv = []
    for batch in batches:
        rows = jnp.concatenate([want[:, d] for d in batch], axis=1)
        sent = pick(rows, [(got_k[d], got_v[d]) for d in batch])
        recv.append([sent[0]] + [lax.ppermute(sent[r], "kv", along_x(r)) for r in range(1, NX)])
    spots = jnp.concatenate([place[:, d] for batch in batches for d in batch], axis=1)

    wm = lax.ppermute(wo, "tp", along_y(1))
    wp = lax.ppermute(wo, "tp", along_y(-1))
    top = lax.ppermute(wm[:HEAD], "tp", along_y(1))
    low = lax.ppermute(wp[HEAD:], "tp", along_y(-1))
    weights = [wo, wm, wp, top, low]
    weights += [lax.ppermute(w, "tp", CORES) for w in weights]

    q = dot(tokens, wq).astype(BF)
    mixed = attend(spots, named, q, k, v, recv)
    att = lax.all_to_all(mixed.reshape(2 * NY, QB, -1), "tp", 0, 0, tiled=True)
    y, c = tp // 2, tp % 2
    rows = jnp.stack([y, (y - 1) % NY, (y + 1) % NY, (y + 2) % NY]) * 2
    return project(jnp.stack([rows + c, rows + 1 - c]), att, weights)


def solution(mesh):
    return jax.shard_map(
        layer,
        mesh=mesh,
        in_specs=(
            P("kv", None),
            P(None, "tp"),
            P(None, "tp"),
            P(None, "tp"),
            P("tp", None),
            P("kv", None),
        ),
        out_specs=P(("kv", "tp"), None),
        check_vma=False,
    )
```

time: 196 us -> 171 us (0.87); the launches traced: 196 us -> 168 us
  waiting for transfers between devices: 124 us -> 29.8 us
  starting transfers between devices: 24.6 us -> 63.8 us
  local copies, waits for them, and re-layouts: 14.8 us -> 44.5 us
  Pallas kernels: 0 us -> 16.6 us
  between operations: 13.6 us -> 0.41 us
  matrix products: 16.1 us -> 11.2 us
    all_to_all x3 -> x1, waiting for transfers between devices: 85.4 us -> 10.1 us  [layer(): att = lax.all_to_all(mixed.reshape(2 * NY, QB, -1), 'tp', 0, 0, tiled=True)]
    ppermute x0 -> x41, starting transfers between devices: none -> 59.7 us  [the longest x15 24.8 us: layer(): lax.ppermute(sent[r], 'kv', along_x(r))]
    reduce_scatter x1 -> x0, waiting for transfers between devices: 38.2 us -> none  [shards(): lax.psum_scatter(jnp.dot(mixed, out_weight, preferred_element_type=jnp.fl...]
    unnamed x11 -> x90, local copies, waits for them, and re-layouts: 0.27 us -> 32.2 us
    all_to_all x3 -> x1, starting transfers between devices: 24.3 us -> 4.16 us  [layer(): att = lax.all_to_all(mixed.reshape(2 * NY, QB, -1), 'tp', 0, 0, tiled=True)]
    ppermute x0 -> x41, waiting for transfers between devices: none -> 19.6 us  [the longest x15 7.52 us: layer(): lax.ppermute(sent[r], 'kv', along_x(r))]
    pallas_call x0 -> x7, Pallas kernels: none -> 16.6 us  [the longest x1 6.61 us: project(): pl.pallas_call(project_body, out_shape=jax.ShapeDtypeStruct((QB, width),...]
    gather x4 -> x0, local copies, waits for them, and re-layouts: 9.86 us -> none  [the longest x1 2.75 us: shards(): far_values = received[1][owners, block_slot]]
  transfers between devices with their start and end apart: 4 -> 42, of which waited for: 4 -> 8; matrix products, arithmetic and copies ran while one was open for 10% -> 15% of each run, Pallas kernels for 0% -> 6%
where the time goes in v1:
time: 171 us; the launch traced here: 168 us
  starting transfers between devices  63.8 us (37%)
  local copies, waits for them, and re-layouts  44.5 us (26%)
  waiting for transfers between devices  29.8 us (17%)
  Pallas kernels  16.6 us (10%)
  matrix products  11.2 us (7%)
  other arithmetic  1.94 us (1%)
    unnamed x90, local copies, waits for them, and re-layouts  32.2 us
    ppermute x15, starting transfers between devices, layer(): lax.ppermute(sent[r], 'kv', along_x(r))  24.8 us
    ppermute x4, starting transfers between devices, layer(): dv = got_v[NZ - step] = lax.ppermute(dv, 'kv', down)  14.2 us
    dot_general x3, matrix products, dot(): return jnp.dot(a, b, preferred_element_type=F32)  11.2 us
    all_to_all x1, waiting for transfers between devices, layer(): att = lax.all_to_all(mixed.reshape(2 * NY, QB, -1), 'tp', 0, 0, tiled=True)  10.1 us
    ppermute x3, starting transfers between devices, layer(): dk = got_k[NZ - step] = lax.ppermute(dk, 'kv', down)  8.13 us
    ppermute x15, waiting for transfers between devices, layer(): lax.ppermute(sent[r], 'kv', along_x(r))  7.52 us
    slice x9, local copies, waits for them, and re-layouts, layer(): place[:, d]  7.27 us
  transfers between devices with their start and end apart: 42, of which 8 were waited for; matrix products, arithmetic and copies ran while one was open for 15% of the time, Pallas kernels for 6%

profile of v1, /device:TPU:2, one launch (start us, length us, event | category | flops | bytes accessed | tf_op | source)
XLA Modules:
  0.0 168.3 jit_solution(8134462845647883351)
XLA Ops:
  0.0 2.2 %collective-permute-start = (s32[8,12]{1,0:T(8,128)}, s32[8,12]{1,0:T(8,128)S(1)}, u32[]{:S(2)}, u32[]{:S(2)}) collective-permute-start(s32[8,12]{1,0:T(8,128)} %param.11), channel_id=1, source_target_pairs={{0,24},{8,0},{16,8},{24,16},{32,56},{40,32},{48,40},{56,48},{64,88... | collective-permute-start | bytes 1160 | tf_op jit(solution)/shard_map/ppermute | solution.py:178
  2.3 3.1 %collective-permute-start.1 = (s32[8,12]{1,0:T(8,128)}, s32[8,12]{1,0:T(8,128)S(1)}, u32[]{:S(2)}, u32[]{:S(2)}) collective-permute-start(s32[8,12]{1,0:T(8,128)} %param.11), channel_id=1, source_target_pairs={{0,16},{8,24},{16,0},{24,8},{32,48},{40,56},{48,32},{56,40},{64,80... | collective-permute-start | bytes 1160 | tf_op jit(solution)/shard_map/ppermute | solution.py:178
  5.4 3.5 %convolution_convert_fusion.1.refs_1_.v = bf16[1024,128]{1,0:T(8,128)(2,1)S(1)} fusion(bf16[1024,2048]{1,0:T(8,128)(2,1)} %param.6, bf16[2048,128]{1,0:T(8,128)(2,1)} %param.9), kind=kOutput, calls=%fused_computation.1 | convolution fusion | flops 537001984 | bytes 4980736 | tf_op jit(solution)/shard_map/dot_general | solution.py:36
  8.9 5.9 %collective-permute-start.9 = (bf16[1024,128]{1,0:T(8,128)(2,1)S(1)}, bf16[1024,128]{1,0:T(8,128)(2,1)}, u32[]{:S(2)}, u32[]{:S(2)}) collective-permute-start(bf16[1024,128]{1,0:T(8,128)(2,1)S(1)} %convolution_convert_fusion.1.refs_1_.v), channel_id=1, source_target_pairs={{0,224},{8,232},{16,240},{24,248},{32,0},{40,8},{48,16},{56,24},{6... | collective-permute-start | bytes 786440 | tf_op jit(solution)/shard_map/ppermute | solution.py:202
  14.9 3.4 %convolution_convert_fusion.2.refs_0_.k = bf16[1024,128]{1,0:T(8,128)(2,1)S(1)} fusion(bf16[1024,2048]{1,0:T(8,128)(2,1)} %param.6, bf16[2048,128]{1,0:T(8,128)(2,1)S(1)} %copy-done.44), kind=kOutput, calls=%fused_computation.2 | convolution fusion | flops 537001984 | bytes 4980736 | tf_op jit(solution)/shard_map/dot_general | solution.py:36
  18.4 3.3 %collective-permute-start.8 = (bf16[1024,128]{1,0:T(8,128)(2,1)S(1)}, bf16[1024,128]{1,0:T(8,128)(2,1)S(1)}, u32[]{:S(2)}, u32[]{:S(2)}) collective-permute-start(bf16[1024,128]{1,0:T(8,128)(2,1)S(1)} %convolution_convert_fusion.2.refs_0_.k), channel_id=1, source_target_pairs={{0,224},{8,232},{16,240},{24,248},{32,0},{40,8},{48,16},{56,24},{6... | collective-permute-start | bytes 786440 | tf_op jit(solution)/shard_map/ppermute | solution.py:200
  23.2 5.0 %collective-permute-done.3.refs_1_ = bf16[1,2,8,32,128]{4,3,2,1,0:T(8,128)(2,1)S(1)} collective-permute-done((bf16[1,2,8,32,128]{4,3,2,1,0:T(8,128)(2,1)S(1)}, bf16[1,2,8,32,128]{4,3,2,1,0:T(8,128)(2,1)S(1)}, u32[]{:S(2)}, u32[]{:S(2)}) %collective-permute-start.3) | collective-permute-done | bytes 131104 | tf_op jit(solution)/shard_map/ppermute | solution.py:209
  29.0 1.9 %collective-permute-start.5 = (bf16[1,2,8,32,128]{4,3,2,1,0:T(8,128)(2,1)S(1)}, bf16[1,2,8,32,128]{4,3,2,1,0:T(8,128)(2,1)S(1)}, u32[]{:S(2)}, u32[]{:S(2)}) collective-permute-start(bf16[1,2,8,32,128]{4,3,2,1,0:T(8,128)(2,1)S(1)} %get-tuple-element.28), channel_id=1, source_target_pairs={{0,24},{8,0},{16,8},{24,16},{32,56},{40,32},{48,40},{56,48},{64,88... | collective-permute-start | bytes 393224 | tf_op jit(solution)/shard_map/ppermute | solution.py:209
  30.9 3.2 %collective-permute-start.16 = (bf16[1024,128]{1,0:T(8,128)(2,1)}, bf16[1024,128]{1,0:T(8,128)(2,1)S(1)}, u32[]{:S(2)}, u32[]{:S(2)}) collective-permute-start(bf16[1024,128]{1,0:T(8,128)(2,1)} %collective-permute-done.9.refs_3_), channel_id=1, source_target_pairs={{0,224},{8,232},{16,240},{24,248},{32,0},{40,8},{48,16},{56,24},{6... | collective-permute-start | bytes 786440 | tf_op jit(solution)/shard_map/ppermute | solution.py:202
  34.1 3.2 %collective-permute-start.15 = (bf16[1024,128]{1,0:T(8,128)(2,1)S(1)}, bf16[1024,128]{1,0:T(8,128)(2,1)S(1)}, u32[]{:S(2)}, u32[]{:S(2)}) collective-permute-start(bf16[1024,128]{1,0:T(8,128)(2,1)S(1)} %collective-permute-done.8.refs_2_), channel_id=1, source_target_pairs={{0,224},{8,232},{16,240},{24,248},{32,0},{40,8},{48,16},{56,24},{6... | collective-permute-start | bytes 786440 | tf_op jit(solution)/shard_map/ppermute | solution.py:200
  37.5 1.2 shard_map.65
  40.0 0.9 collective-permute-start.10
  41.6 3.8 %collective-permute-start.11 = (bf16[2,2,8,32,128]{4,3,2,1,0:T(8,128)(2,1)S(1)}, bf16[2,2,8,32,128]{4,3,2,1,0:T(8,128)(2,1)S(1)}, u32[]{:S(2)}, u32[]{:S(2)}) collective-permute-start(bf16[2,2,8,32,128]{4,3,2,1,0:T(8,128)(2,1)S(1)} %get-tuple-element.31), channel_id=1, source_target_pairs={{0,16},{8,24},{16,0},{24,8},{32,48},{40,56},{48,32},{56,40},{64,80... | collective-permute-start | bytes 786440 | tf_op jit(solution)/shard_map/ppermute | solution.py:209
  45.6 3.2 %collective-permute-start.23 = (bf16[1024,128]{1,0:T(8,128)(2,1)S(1)}, bf16[1024,128]{1,0:T(8,128)(2,1)S(1)}, u32[]{:S(2)}, u32[]{:S(2)}) collective-permute-start(bf16[1024,128]{1,0:T(8,128)(2,1)S(1)} %collective-permute-done.16.refs_3_), channel_id=1, source_target_pairs={{0,224},{8,232},{16,240},{24,248},{32,0},{40,8},{48,16},{56,24},{6... | collective-permute-start | bytes 786440 | tf_op jit(solution)/shard_map/ppermute | solution.py:202
  49.5 3.0 %collective-permute-start.33 = (bf16[256,2048]{1,0:T(8,128)(2,1)}, bf16[256,2048]{1,0:T(8,128)(2,1)S(1)}, u32[]{:S(2)}, u32[]{:S(2)}) collective-permute-start(bf16[256,2048]{1,0:T(8,128)(2,1)} %refs_0_.1), channel_id=1, source_target_pairs={{0,6},{1,7},{2,0},{3,1},{4,2},{5,3},{6,4},{7,5},{8,14},{9,15},{10,... | collective-permute-start | bytes 3145736 | tf_op jit(solution)/shard_map/ppermute | solution.py:213
  53.4 1.6 collective-permute-done.13.refs_0_
  55.0 1.6 collective-permute-start.22
  58.6 3.0 %collective-permute-done.21.refs_1_ = bf16[1024,128]{1,0:T(8,128)(2,1)S(1)} collective-permute-done((bf16[1024,128]{1,0:T(8,128)(2,1)S(1)}, bf16[1024,128]{1,0:T(8,128)(2,1)S(1)}, u32[]{:S(2)}, u32[]{:S(2)}) %collective-permute-start.21) | collective-permute-done | bytes 262176 | tf_op jit(solution)/shard_map/ppermute | solution.py:201
  61.6 1.8 %collective-permute-start.17 = (bf16[2,2,8,32,128]{4,3,2,1,0:T(8,128)(2,1)S(1)}, bf16[2,2,8,32,128]{4,3,2,1,0:T(8,128)(2,1)S(1)}, u32[]{:S(2)}, u32[]{:S(2)}) collective-permute-start(bf16[2,2,8,32,128]{4,3,2,1,0:T(8,128)(2,1)S(1)} %get-tuple-element.34), channel_id=1, source_target_pairs={{0,8},{8,16},{16,24},{24,0},{32,40},{40,48},{48,56},{56,32},{64,72... | collective-permute-start | bytes 786440 | tf_op jit(solution)/shard_map/ppermute | solution.py:209
  63.4 1.8 %collective-permute-start.28 = (bf16[1024,128]{1,0:T(8,128)(2,1)S(1)}, bf16[1024,128]{1,0:T(8,128)(2,1)S(1)}, u32[]{:S(2)}, u32[]{:S(2)}) collective-permute-start(bf16[1024,128]{1,0:T(8,128)(2,1)S(1)} %collective-permute-done.23.refs_3_), channel_id=1, source_target_pairs={{0,224},{8,232},{16,240},{24,248},{32,0},{40,8},{48,16},{56,24},{6... | collective-permute-start | bytes 786440 | tf_op jit(solution)/shard_map/ppermute | solution.py:202
  65.5 4.2 %convolution_convert_fusion.q = bf16[1024,256]{1,0:T(8,128)(2,1)} fusion(bf16[1024,2048]{1,0:T(8,128)(2,1)} %param.6, bf16[2048,256]{1,0:T(8,128)(2,1)S(1)} %copy-done), kind=kOutput, calls=%fused_computation | convolution fusion | flops 1074003968 | bytes 5767168 | tf_op jit(solution)/shard_map/dot_general | solution.py:36
  71.2 4.5 %collective-permute-start.18 = (bf16[2,2,8,32,128]{4,3,2,1,0:T(8,128)(2,1)S(1)}, bf16[2,2,8,32,128]{4,3,2,1,0:T(8,128)(2,1)S(1)}, u32[]{:S(2)}, u32[]{:S(2)}) collective-permute-start(bf16[2,2,8,32,128]{4,3,2,1,0:T(8,128)(2,1)S(1)} %get-tuple-element.35), channel_id=1, source_target_pairs={{0,16},{8,24},{16,0},{24,8},{32,48},{40,56},{48,32},{56,40},{64,80... | collective-permute-start | bytes 786440 | tf_op jit(solution)/shard_map/ppermute | solution.py:209
  75.7 1.6 collective-permute-start.19
  77.3 1.7 %collective-permute-start.24 = (bf16[2,2,8,32,128]{4,3,2,1,0:T(8,128)(2,1)S(1)}, bf16[2,2,8,32,128]{4,3,2,1,0:T(8,128)(2,1)S(1)}, u32[]{:S(2)}, u32[]{:S(2)}) collective-permute-start(bf16[2,2,8,32,128]{4,3,2,1,0:T(8,128)(2,1)S(1)} %get-tuple-element.38), channel_id=1, source_target_pairs={{0,8},{8,16},{16,24},{24,0},{32,40},{40,48},{48,56},{56,32},{64,72... | collective-permute-start | bytes 786440 | tf_op jit(solution)/shard_map/ppermute | solution.py:209
  79.0 1.8 %collective-permute-start.25 = (bf16[2,2,8,32,128]{4,3,2,1,0:T(8,128)(2,1)S(1)}, bf16[2,2,8,32,128]{4,3,2,1,0:T(8,128)(2,1)S(1)}, u32[]{:S(2)}, u32[]{:S(2)}) collective-permute-start(bf16[2,2,8,32,128]{4,3,2,1,0:T(8,128)(2,1)S(1)} %get-tuple-element.39), channel_id=1, source_target_pairs={{0,16},{8,24},{16,0},{24,8},{32,48},{40,56},{48,32},{56,40},{64,80... | collective-permute-start | bytes 786440 | tf_op jit(solution)/shard_map/ppermute | solution.py:209
  80.8 2.0 %collective-permute-start.26 = (bf16[2,2,8,32,128]{4,3,2,1,0:T(8,128)(2,1)S(1)}, bf16[2,2,8,32,128]{4,3,2,1,0:T(8,128)(2,1)S(1)}, u32[]{:S(2)}, u32[]{:S(2)}) collective-permute-start(bf16[2,2,8,32,128]{4,3,2,1,0:T(8,128)(2,1)S(1)} %get-tuple-element.40), channel_id=1, source_target_pairs={{0,24},{8,0},{16,8},{24,16},{32,56},{40,32},{48,40},{56,48},{64,88... | collective-permute-start | bytes 786440 | tf_op jit(solution)/shard_map/ppermute | solution.py:209
  85.1 1.0 collective-permute-start.29
  86.1 2.5 %collective-permute-done.19.refs_11_ = bf16[2,2,8,32,128]{4,3,2,1,0:T(8,128)(2,1)S(1)} collective-permute-done((bf16[2,2,8,32,128]{4,3,2,1,0:T(8,128)(2,1)S(1)}, bf16[2,2,8,32,128]{4,3,2,1,0:T(8,128)(2,1)S(1)}, u32[]{:S(2)}, u32[]{:S(2)}) %collective-permute-start.19) | collective-permute-done | bytes 262176 | tf_op jit(solution)/shard_map/ppermute | solution.py:209
  89.4 2.8 %collective-permute-start.30 = (bf16[1,2,8,32,128]{4,3,2,1,0:T(8,128)(2,1)S(1)}, bf16[1,2,8,32,128]{4,3,2,1,0:T(8,128)(2,1)S(1)}, u32[]{:S(2)}, u32[]{:S(2)}) collective-permute-start(bf16[1,2,8,32,128]{4,3,2,1,0:T(8,128)(2,1)S(1)} %get-tuple-element.43), channel_id=1, source_target_pairs={{0,16},{8,24},{16,0},{24,8},{32,48},{40,56},{48,32},{56,40},{64,80... | collective-permute-start | bytes 393224 | tf_op jit(solution)/shard_map/ppermute | solution.py:209
  94.1 3.1 %collective-permute-start.35 = (bf16[128,2048]{1,0:T(8,128)(2,1)S(1)}, bf16[128,2048]{1,0:T(8,128)(2,1)}, u32[]{:S(2)}, u32[]{:S(2)}) collective-permute-start(bf16[128,2048]{1,0:T(8,128)(2,1)S(1)} %slice.89), channel_id=1, source_target_pairs={{0,6},{1,7},{2,0},{3,1},{4,2},{5,3},{6,4},{7,5},{8,14},{9,15},{10,... | collective-permute-start | bytes 1572872 | tf_op jit(solution)/shard_map/ppermute | solution.py:215
  101.3 2.7 %collective-permute-done.35.refs_4_ = bf16[128,2048]{1,0:T(8,128)(2,1)} collective-permute-done((bf16[128,2048]{1,0:T(8,128)(2,1)S(1)}, bf16[128,2048]{1,0:T(8,128)(2,1)}, u32[]{:S(2)}, u32[]{:S(2)}) %collective-permute-start.35) | collective-permute-done | bytes 524320 | tf_op jit(solution)/shard_map/ppermute | solution.py:215
  104.0 4.5 %collective-permute-done.34.refs_3_ = bf16[128,2048]{1,0:T(8,128)(2,1)} collective-permute-done((bf16[128,2048]{1,0:T(8,128)(2,1)S(1)}, bf16[128,2048]{1,0:T(8,128)(2,1)}, u32[]{:S(2)}, u32[]{:S(2)}) %collective-permute-start.34) | collective-permute-done | bytes 524320 | tf_op jit(solution)/shard_map/ppermute | solution.py:214
  109.2 0.8 copy.22
  110.1 0.8 copy.21
  111.0 0.8 copy.20
  112.5 0.8 copy.19
  115.5 0.8 copy.17
  117.0 0.8 copy.16
  118.5 0.8 copy.15
  120.7 0.9 copy-done.3
  121.7 1.0 copy-done.4
  122.7 0.9 copy-done.6
  123.7 0.9 copy-done.8
  124.6 0.9 copy-done.10
  125.6 0.9 copy-done.12
  126.5 0.9 copy-done.14
  127.5 0.9 copy-done.16
  128.4 0.9 copy-done.18
  129.4 0.9 copy-done.20
  130.3 0.9 copy-done.22
  131.3 0.9 copy-done.24
  132.2 0.9 copy-done.26
  133.2 0.9 copy-done.28
  134.2 0.9 copy-done.30
  135.1 0.9 copy-done.32
  136.0 0.9 copy-done.34
  136.9 0.9 copy-done.36
  137.8 0.9 copy-done.38
  138.7 0.9 copy-done.40
  139.6 0.9 copy-done.42
  140.5 5.9 %attend.1 = bf16[1024,256]{1,0:T(8,128)(2,1)S(1)} custom-call(s32[8,32]{1,0:T(8,128)S(1)} %concatenate.46.place, s32[8]{0:T(128)S(1)} %get-tuple-element.65.named, bf16[1024,256]{1,0:T(8,128)(2,1)S(1)} %copy-done.4, bf16[1024,128]{1,0:T(8,128)(2,1)S(1)} %copy-done.3, bf16[1024,128]{1,0:T(8,128)(2,1)S(1)} %convolution_convert_fusion.1.refs_1_.v, ...), custom_call_target="tpu_custom_call" | custom-call | flops 600000000 | bytes 6000000 | tf_op jit(solution)/shard_map/attend/pallas_call | solution.py:123
  147.2 4.2 %all-to-all-start = ((bf16[8,128,256]{2,1,0:T(8,128)(2,1)}), bf16[8,128,256]{2,1,0:T(8,128)(2,1)}, u32[]{:S(2)}, u32[]{:S(2)}) async-start(bf16[8,128,256]{2,1,0:T(8,128)(2,1)} %bitcast.31), calls=%async_computation | async-start | bytes 1048576 | tf_op jit(solution)/shard_map/all_to_all | solution.py:221
  151.5 10.1 %all-to-all-done.att = bf16[8,128,256]{2,1,0:T(8,128)(2,1)} async-done(((bf16[8,128,256]{2,1,0:T(8,128)(2,1)}), bf16[8,128,256]{2,1,0:T(8,128)(2,1)}, u32[]{:S(2)}, u32[]{:S(2)}) %all-to-all-start) | async-done | bytes 524320 | tf_op jit(solution)/shard_map/all_to_all | solution.py:221
  161.7 6.6 %project.1 = bf16[128,2048]{1,0:T(8,128)(2,1)} custom-call(s32[2,4]{1,0:T(2,128)S(1)} %pad_add_fusion.4.spot, bf16[8,128,256]{2,1,0:T(8,128)(2,1)} %all-to-all-done.att, bf16[256,2048]{1,0:T(8,128)(2,1)} %refs_0_.1, bf16[256,2048]{1,0:T(8,128)(2,1)S(1)} %collective-permute-done.32.refs_1_, bf16[256,2048]{1,0:T(8,128)(2,1)S(1)} %collective-permute-done.33.refs_2_, ...), custom_call_target="tpu_custom_call" | custom-call | flops 1000000000 | bytes 9000000 | tf_op jit(solution)/shard_map/project/pallas_call | solution.py:159
  (156 shorter events, 26.4 us)
Async XLA Ops:
  0.0 65.5 %copy-start = (bf16[2048,256]{1,0:T(8,128)(2,1)S(1)}, bf16[2048,256]{1,0:T(8,128)(2,1)}, u32[]{:S(2)}) copy-start(bf16[2048,256]{1,0:T(8,128)(2,1)} %param.7) | copy-start | bytes 3145732
  0.0 14.9 %copy-start.44 = (bf16[2048,128]{1,0:T(8,128)(2,1)S(1)}, bf16[2048,128]{1,0:T(8,128)(2,1)}, u32[]{:S(2)}) copy-start(bf16[2048,128]{1,0:T(8,128)(2,1)} %param.8) | copy-start | bytes 1572868
  0.0 18.4 %collective-permute-start = (s32[8,12]{1,0:T(8,128)}, s32[8,12]{1,0:T(8,128)S(1)}, u32[]{:S(2)}, u32[]{:S(2)}) collective-permute-start(s32[8,12]{1,0:T(8,128)} %param.11), channel_id=1, source_target_pairs={{0,24},{8,0},{16,8},{24,16},{32,56},{40,32},{48,40},{56,48},{64,88... | collective-permute-start | bytes 1160 | tf_op jit(solution)/shard_map/ppermute | solution.py:178
  2.2 19.4 %collective-permute-start.2 = (s32[8,12]{1,0:T(8,128)}, s32[8,12]{1,0:T(8,128)S(1)}, u32[]{:S(2)}, u32[]{:S(2)}) collective-permute-start(s32[8,12]{1,0:T(8,128)} %param.11), channel_id=1, source_target_pairs={{0,8},{8,16},{16,24},{24,0},{32,40},{40,48},{48,56},{56,32},{64,72... | collective-permute-start | bytes 1160 | tf_op jit(solution)/shard_map/ppermute | solution.py:178
  2.3 19.4 %collective-permute-start.1 = (s32[8,12]{1,0:T(8,128)}, s32[8,12]{1,0:T(8,128)S(1)}, u32[]{:S(2)}, u32[]{:S(2)}) collective-permute-start(s32[8,12]{1,0:T(8,128)} %param.11), channel_id=1, source_target_pairs={{0,16},{8,24},{16,0},{24,8},{32,48},{40,56},{48,32},{56,40},{64,80... | collective-permute-start | bytes 1160 | tf_op jit(solution)/shard_map/ppermute | solution.py:178
  8.9 12.8 %copy-start.43 = (s32[8,12]{1,0:T(8,128)S(1)}, s32[8,12]{1,0:T(8,128)}, u32[]{:S(2)}) copy-start(s32[8,12]{1,0:T(8,128)} %param.11) | copy-start | bytes 1156
  8.9 20.1 %collective-permute-start.9 = (bf16[1024,128]{1,0:T(8,128)(2,1)S(1)}, bf16[1024,128]{1,0:T(8,128)(2,1)}, u32[]{:S(2)}, u32[]{:S(2)}) collective-permute-start(bf16[1024,128]{1,0:T(8,128)(2,1)S(1)} %convolution_convert_fusion.1.refs_1_.v), channel_id=1, source_target_pairs={{0,224},{8,232},{16,240},{24,248},{32,0},{40,8},{48,16},{56,24},{6... | collective-permute-start | bytes 786440 | tf_op jit(solution)/shard_map/ppermute | solution.py:202
  14.9 16.0 %collective-permute-start.7 = (bf16[1024,128]{1,0:T(8,128)(2,1)S(1)}, bf16[1024,128]{1,0:T(8,128)(2,1)}, u32[]{:S(2)}, u32[]{:S(2)}) collective-permute-start(bf16[1024,128]{1,0:T(8,128)(2,1)S(1)} %convolution_convert_fusion.1.refs_1_.v), channel_id=1, source_target_pairs={{0,32},{8,40},{16,48},{24,56},{32,64},{40,72},{48,80},{56,88},{64,... | collective-permute-start | bytes 786440 | tf_op jit(solution)/shard_map/ppermute | solution.py:201
  18.3 12.6 %copy-start.2 = (bf16[1024,128]{1,0:T(8,128)(2,1)}, bf16[1024,128]{1,0:T(8,128)(2,1)S(1)}, u32[]{:S(2)}) copy-start(bf16[1024,128]{1,0:T(8,128)(2,1)S(1)} %convolution_convert_fusion.2.refs_0_.k) | copy-start | bytes 786436
  18.4 15.8 %collective-permute-start.8 = (bf16[1024,128]{1,0:T(8,128)(2,1)S(1)}, bf16[1024,128]{1,0:T(8,128)(2,1)S(1)}, u32[]{:S(2)}, u32[]{:S(2)}) collective-permute-start(bf16[1024,128]{1,0:T(8,128)(2,1)S(1)} %convolution_convert_fusion.2.refs_0_.k), channel_id=1, source_target_pairs={{0,224},{8,232},{16,240},{24,248},{32,0},{40,8},{48,16},{56,24},{6... | collective-permute-start | bytes 786440 | tf_op jit(solution)/shard_map/ppermute | solution.py:200
  21.7 12.5 %collective-permute-start.6 = (bf16[1024,128]{1,0:T(8,128)(2,1)S(1)}, bf16[1024,128]{1,0:T(8,128)(2,1)S(1)}, u32[]{:S(2)}, u32[]{:S(2)}) collective-permute-start(bf16[1024,128]{1,0:T(8,128)(2,1)S(1)} %convolution_convert_fusion.2.refs_0_.k), channel_id=1, source_target_pairs={{0,32},{8,40},{16,48},{24,56},{32,64},{40,72},{48,80},{56,88},{64,... | collective-permute-start | bytes 786440 | tf_op jit(solution)/shard_map/ppermute | solution.py:198
  23.1 5.0 %collective-permute-start.3 = (bf16[1,2,8,32,128]{4,3,2,1,0:T(8,128)(2,1)S(1)}, bf16[1,2,8,32,128]{4,3,2,1,0:T(8,128)(2,1)S(1)}, u32[]{:S(2)}, u32[]{:S(2)}) collective-permute-start(bf16[1,2,8,32,128]{4,3,2,1,0:T(8,128)(2,1)S(1)} %get-tuple-element.26), channel_id=1, source_target_pairs={{0,8},{8,16},{16,24},{24,0},{32,40},{40,48},{48,56},{56,32},{64,72... | collective-permute-start | bytes 393224 | tf_op jit(solution)/shard_map/ppermute | solution.py:209
  28.8 10.6 %collective-permute-start.4 = (bf16[1,2,8,32,128]{4,3,2,1,0:T(8,128)(2,1)S(1)}, bf16[1,2,8,32,128]{4,3,2,1,0:T(8,128)(2,1)S(1)}, u32[]{:S(2)}, u32[]{:S(2)}) collective-permute-start(bf16[1,2,8,32,128]{4,3,2,1,0:T(8,128)(2,1)S(1)} %get-tuple-element.27), channel_id=1, source_target_pairs={{0,16},{8,24},{16,0},{24,8},{32,48},{40,56},{48,32},{56,40},{64,80... | collective-permute-start | bytes 393224 | tf_op jit(solution)/shard_map/ppermute | solution.py:209
  29.0 11.9 %collective-permute-start.5 = (bf16[1,2,8,32,128]{4,3,2,1,0:T(8,128)(2,1)S(1)}, bf16[1,2,8,32,128]{4,3,2,1,0:T(8,128)(2,1)S(1)}, u32[]{:S(2)}, u32[]{:S(2)}) collective-permute-start(bf16[1,2,8,32,128]{4,3,2,1,0:T(8,128)(2,1)S(1)} %get-tuple-element.28), channel_id=1, source_target_pairs={{0,24},{8,0},{16,8},{24,16},{32,56},{40,32},{48,40},{56,48},{64,88... | collective-permute-start | bytes 393224 | tf_op jit(solution)/shard_map/ppermute | solution.py:209
  30.9 14.5 %collective-permute-start.16 = (bf16[1024,128]{1,0:T(8,128)(2,1)}, bf16[1024,128]{1,0:T(8,128)(2,1)S(1)}, u32[]{:S(2)}, u32[]{:S(2)}) collective-permute-start(bf16[1024,128]{1,0:T(8,128)(2,1)} %collective-permute-done.9.refs_3_), channel_id=1, source_target_pairs={{0,224},{8,232},{16,240},{24,248},{32,0},{40,8},{48,16},{56,24},{6... | collective-permute-start | bytes 786440 | tf_op jit(solution)/shard_map/ppermute | solution.py:202
  34.1 11.5 %collective-permute-start.14 = (bf16[1024,128]{1,0:T(8,128)(2,1)}, bf16[1024,128]{1,0:T(8,128)(2,1)S(1)}, u32[]{:S(2)}, u32[]{:S(2)}) collective-permute-start(bf16[1024,128]{1,0:T(8,128)(2,1)} %collective-permute-done.7.refs_1_), channel_id=1, source_target_pairs={{0,32},{8,40},{16,48},{24,56},{32,64},{40,72},{48,80},{56,88},{64,... | collective-permute-start | bytes 786440 | tf_op jit(solution)/shard_map/ppermute | solution.py:201
  34.1 11.5 %collective-permute-start.15 = (bf16[1024,128]{1,0:T(8,128)(2,1)S(1)}, bf16[1024,128]{1,0:T(8,128)(2,1)S(1)}, u32[]{:S(2)}, u32[]{:S(2)}) collective-permute-start(bf16[1024,128]{1,0:T(8,128)(2,1)S(1)} %collective-permute-done.8.refs_2_), channel_id=1, source_target_pairs={{0,224},{8,232},{16,240},{24,248},{32,0},{40,8},{48,16},{56,24},{6... | collective-permute-start | bytes 786440 | tf_op jit(solution)/shard_map/ppermute | solution.py:200
  40.0 8.8 %collective-permute-start.10 = (bf16[2,2,8,32,128]{4,3,2,1,0:T(8,128)(2,1)S(1)}, bf16[2,2,8,32,128]{4,3,2,1,0:T(8,128)(2,1)S(1)}, u32[]{:S(2)}, u32[]{:S(2)}) collective-permute-start(bf16[2,2,8,32,128]{4,3,2,1,0:T(8,128)(2,1)S(1)} %get-tuple-element.30), channel_id=1, source_target_pairs={{0,8},{8,16},{16,24},{24,0},{32,40},{40,48},{48,56},{56,32},{64,72... | collective-permute-start | bytes 786440 | tf_op jit(solution)/shard_map/ppermute | solution.py:209
  41.6 11.0 %collective-permute-start.11 = (bf16[2,2,8,32,128]{4,3,2,1,0:T(8,128)(2,1)S(1)}, bf16[2,2,8,32,128]{4,3,2,1,0:T(8,128)(2,1)S(1)}, u32[]{:S(2)}, u32[]{:S(2)}) collective-permute-start(bf16[2,2,8,32,128]{4,3,2,1,0:T(8,128)(2,1)S(1)} %get-tuple-element.31), channel_id=1, source_target_pairs={{0,16},{8,24},{16,0},{24,8},{32,48},{40,56},{48,32},{56,40},{64,80... | collective-permute-start | bytes 786440 | tf_op jit(solution)/shard_map/ppermute | solution.py:209
  45.4 7.9 %collective-permute-start.12 = (bf16[2,2,8,32,128]{4,3,2,1,0:T(8,128)(2,1)S(1)}, bf16[2,2,8,32,128]{4,3,2,1,0:T(8,128)(2,1)S(1)}, u32[]{:S(2)}, u32[]{:S(2)}) collective-permute-start(bf16[2,2,8,32,128]{4,3,2,1,0:T(8,128)(2,1)S(1)} %get-tuple-element.32), channel_id=1, source_target_pairs={{0,24},{8,0},{16,8},{24,16},{32,56},{40,32},{48,40},{56,48},{64,88... | collective-permute-start | bytes 786440 | tf_op jit(solution)/shard_map/ppermute | solution.py:209
  45.6 9.4 %collective-permute-start.13 = (bf16[1024,128]{1,0:T(8,128)(2,1)S(1)}, bf16[1024,128]{1,0:T(8,128)(2,1)S(1)}, u32[]{:S(2)}, u32[]{:S(2)}) collective-permute-start(bf16[1024,128]{1,0:T(8,128)(2,1)S(1)} %collective-permute-done.6.refs_0_), channel_id=1, source_target_pairs={{0,32},{8,40},{16,48},{24,56},{32,64},{40,72},{48,80},{56,88},{64,... | collective-permute-start | bytes 786440 | tf_op jit(solution)/shard_map/ppermute | solution.py:198
  45.6 11.0 %collective-permute-start.23 = (bf16[1024,128]{1,0:T(8,128)(2,1)S(1)}, bf16[1024,128]{1,0:T(8,128)(2,1)S(1)}, u32[]{:S(2)}, u32[]{:S(2)}) collective-permute-start(bf16[1024,128]{1,0:T(8,128)(2,1)S(1)} %collective-permute-done.16.refs_3_), channel_id=1, source_target_pairs={{0,224},{8,232},{16,240},{24,248},{32,0},{40,8},{48,16},{56,24},{6... | collective-permute-start | bytes 786440 | tf_op jit(solution)/shard_map/ppermute | solution.py:202
  49.5 29.4 %collective-permute-start.33 = (bf16[256,2048]{1,0:T(8,128)(2,1)}, bf16[256,2048]{1,0:T(8,128)(2,1)S(1)}, u32[]{:S(2)}, u32[]{:S(2)}) collective-permute-start(bf16[256,2048]{1,0:T(8,128)(2,1)} %refs_0_.1), channel_id=1, source_target_pairs={{0,6},{1,7},{2,0},{3,1},{4,2},{5,3},{6,4},{7,5},{8,14},{9,15},{10,... | collective-permute-start | bytes 3145736 | tf_op jit(solution)/shard_map/ppermute | solution.py:213
  53.3 27.5 %collective-permute-start.32 = (bf16[256,2048]{1,0:T(8,128)(2,1)}, bf16[256,2048]{1,0:T(8,128)(2,1)S(1)}, u32[]{:S(2)}, u32[]{:S(2)}) collective-permute-start(bf16[256,2048]{1,0:T(8,128)(2,1)} %refs_0_.1), channel_id=1, source_target_pairs={{0,2},{1,3},{2,4},{3,5},{4,6},{5,7},{6,0},{7,1},{8,10},{9,11},{10,... | collective-permute-start | bytes 3145736 | tf_op jit(solution)/shard_map/ppermute | solution.py:212
  53.3 12.2 %copy-start.11 = (bf16[2,2,8,32,128]{4,3,2,1,0:T(8,128)(2,1)}, bf16[2,2,8,32,128]{4,3,2,1,0:T(8,128)(2,1)S(1)}, u32[]{:S(2)}) copy-start(bf16[2,2,8,32,128]{4,3,2,1,0:T(8,128)(2,1)S(1)} %collective-permute-done.12.refs_7_) | copy-start | bytes 786436
  53.3 8.3 %collective-permute-start.21 = (bf16[1024,128]{1,0:T(8,128)(2,1)S(1)}, bf16[1024,128]{1,0:T(8,128)(2,1)S(1)}, u32[]{:S(2)}, u32[]{:S(2)}) collective-permute-start(bf16[1024,128]{1,0:T(8,128)(2,1)S(1)} %collective-permute-done.14.refs_1_), channel_id=1, source_target_pairs={{0,32},{8,40},{16,48},{24,56},{32,64},{40,72},{48,80},{56,88},{64,... | collective-permute-start | bytes 786440 | tf_op jit(solution)/shard_map/ppermute | solution.py:201
  55.0 8.4 %collective-permute-start.22 = (bf16[1024,128]{1,0:T(8,128)(2,1)S(1)}, bf16[1024,128]{1,0:T(8,128)(2,1)S(1)}, u32[]{:S(2)}, u32[]{:S(2)}) collective-permute-start(bf16[1024,128]{1,0:T(8,128)(2,1)S(1)} %collective-permute-done.15.refs_2_), channel_id=1, source_target_pairs={{0,224},{8,232},{16,240},{24,248},{32,0},{40,8},{48,16},{56,24},{6... | collective-permute-start | bytes 786440 | tf_op jit(solution)/shard_map/ppermute | solution.py:200
  56.6 8.8 %collective-permute-start.20 = (bf16[1024,128]{1,0:T(8,128)(2,1)S(1)}, bf16[1024,128]{1,0:T(8,128)(2,1)S(1)}, u32[]{:S(2)}, u32[]{:S(2)}) collective-permute-start(bf16[1024,128]{1,0:T(8,128)(2,1)S(1)} %collective-permute-done.13.refs_0_), channel_id=1, source_target_pairs={{0,32},{8,40},{16,48},{24,56},{32,64},{40,72},{48,80},{56,88},{64,... | collective-permute-start | bytes 786440 | tf_op jit(solution)/shard_map/ppermute | solution.py:198
  61.6 9.6 %collective-permute-start.17 = (bf16[2,2,8,32,128]{4,3,2,1,0:T(8,128)(2,1)S(1)}, bf16[2,2,8,32,128]{4,3,2,1,0:T(8,128)(2,1)S(1)}, u32[]{:S(2)}, u32[]{:S(2)}) collective-permute-start(bf16[2,2,8,32,128]{4,3,2,1,0:T(8,128)(2,1)S(1)} %get-tuple-element.34), channel_id=1, source_target_pairs={{0,8},{8,16},{16,24},{24,0},{32,40},{40,48},{48,56},{56,32},{64,72... | collective-permute-start | bytes 786440 | tf_op jit(solution)/shard_map/ppermute | solution.py:209
  63.4 12.3 %collective-permute-start.28 = (bf16[1024,128]{1,0:T(8,128)(2,1)S(1)}, bf16[1024,128]{1,0:T(8,128)(2,1)S(1)}, u32[]{:S(2)}, u32[]{:S(2)}) collective-permute-start(bf16[1024,128]{1,0:T(8,128)(2,1)S(1)} %collective-permute-done.23.refs_3_), channel_id=1, source_target_pairs={{0,224},{8,232},{16,240},{24,248},{32,0},{40,8},{48,16},{56,24},{6... | collective-permute-start | bytes 786440 | tf_op jit(solution)/shard_map/ppermute | solution.py:202
  65.5 11.8 %collective-permute-start.27 = (bf16[1024,128]{1,0:T(8,128)(2,1)S(1)}, bf16[1024,128]{1,0:T(8,128)(2,1)S(1)}, u32[]{:S(2)}, u32[]{:S(2)}) collective-permute-start(bf16[1024,128]{1,0:T(8,128)(2,1)S(1)} %collective-permute-done.20.refs_0_), channel_id=1, source_target_pairs={{0,32},{8,40},{16,48},{24,56},{32,64},{40,72},{48,80},{56,88},{64,... | collective-permute-start | bytes 786440 | tf_op jit(solution)/shard_map/ppermute | solution.py:198
  71.2 28.7 %copy-start.15 = (bf16[2,2,8,32,128]{4,3,2,1,0:T(8,128)(2,1)}, bf16[2,2,8,32,128]{4,3,2,1,0:T(8,128)(2,1)S(1)}, u32[]{:S(2)}) copy-start(bf16[2,2,8,32,128]{4,3,2,1,0:T(8,128)(2,1)S(1)} %collective-permute-done.17.refs_9_) | copy-start | bytes 786436
  71.2 13.1 %collective-permute-start.18 = (bf16[2,2,8,32,128]{4,3,2,1,0:T(8,128)(2,1)S(1)}, bf16[2,2,8,32,128]{4,3,2,1,0:T(8,128)(2,1)S(1)}, u32[]{:S(2)}, u32[]{:S(2)}) collective-permute-start(bf16[2,2,8,32,128]{4,3,2,1,0:T(8,128)(2,1)S(1)} %get-tuple-element.35), channel_id=1, source_target_pairs={{0,16},{8,24},{16,0},{24,8},{32,48},{40,56},{48,32},{56,40},{64,80... | collective-permute-start | bytes 786440 | tf_op jit(solution)/shard_map/ppermute | solution.py:209
  75.7 12.9 %collective-permute-start.19 = (bf16[2,2,8,32,128]{4,3,2,1,0:T(8,128)(2,1)S(1)}, bf16[2,2,8,32,128]{4,3,2,1,0:T(8,128)(2,1)S(1)}, u32[]{:S(2)}, u32[]{:S(2)}) collective-permute-start(bf16[2,2,8,32,128]{4,3,2,1,0:T(8,128)(2,1)S(1)} %get-tuple-element.36), channel_id=1, source_target_pairs={{0,24},{8,0},{16,8},{24,16},{32,56},{40,32},{48,40},{56,48},{64,88... | collective-permute-start | bytes 786440 | tf_op jit(solution)/shard_map/ppermute | solution.py:209
  77.3 14.9 %collective-permute-start.24 = (bf16[2,2,8,32,128]{4,3,2,1,0:T(8,128)(2,1)S(1)}, bf16[2,2,8,32,128]{4,3,2,1,0:T(8,128)(2,1)S(1)}, u32[]{:S(2)}, u32[]{:S(2)}) collective-permute-start(bf16[2,2,8,32,128]{4,3,2,1,0:T(8,128)(2,1)S(1)} %get-tuple-element.38), channel_id=1, source_target_pairs={{0,8},{8,16},{16,24},{24,0},{32,40},{40,48},{48,56},{56,32},{64,72... | collective-permute-start | bytes 786440 | tf_op jit(solution)/shard_map/ppermute | solution.py:209
  79.0 14.4 %collective-permute-start.25 = (bf16[2,2,8,32,128]{4,3,2,1,0:T(8,128)(2,1)S(1)}, bf16[2,2,8,32,128]{4,3,2,1,0:T(8,128)(2,1)S(1)}, u32[]{:S(2)}, u32[]{:S(2)}) collective-permute-start(bf16[2,2,8,32,128]{4,3,2,1,0:T(8,128)(2,1)S(1)} %get-tuple-element.39), channel_id=1, source_target_pairs={{0,16},{8,24},{16,0},{24,8},{32,48},{40,56},{48,32},{56,40},{64,80... | collective-permute-start | bytes 786440 | tf_op jit(solution)/shard_map/ppermute | solution.py:209
  80.8 16.5 %collective-permute-start.26 = (bf16[2,2,8,32,128]{4,3,2,1,0:T(8,128)(2,1)S(1)}, bf16[2,2,8,32,128]{4,3,2,1,0:T(8,128)(2,1)S(1)}, u32[]{:S(2)}, u32[]{:S(2)}) collective-permute-start(bf16[2,2,8,32,128]{4,3,2,1,0:T(8,128)(2,1)S(1)} %get-tuple-element.40), channel_id=1, source_target_pairs={{0,24},{8,0},{16,8},{24,16},{32,56},{40,32},{48,40},{56,48},{64,88... | collective-permute-start | bytes 786440 | tf_op jit(solution)/shard_map/ppermute | solution.py:209
  85.1 13.0 %collective-permute-start.29 = (bf16[1,2,8,32,128]{4,3,2,1,0:T(8,128)(2,1)S(1)}, bf16[1,2,8,32,128]{4,3,2,1,0:T(8,128)(2,1)S(1)}, u32[]{:S(2)}, u32[]{:S(2)}) collective-permute-start(bf16[1,2,8,32,128]{4,3,2,1,0:T(8,128)(2,1)S(1)} %get-tuple-element.42), channel_id=1, source_target_pairs={{0,8},{8,16},{16,24},{24,0},{32,40},{40,48},{48,56},{56,32},{64,72... | collective-permute-start | bytes 393224 | tf_op jit(solution)/shard_map/ppermute | solution.py:209
  89.4 9.4 %collective-permute-start.30 = (bf16[1,2,8,32,128]{4,3,2,1,0:T(8,128)(2,1)S(1)}, bf16[1,2,8,32,128]{4,3,2,1,0:T(8,128)(2,1)S(1)}, u32[]{:S(2)}, u32[]{:S(2)}) collective-permute-start(bf16[1,2,8,32,128]{4,3,2,1,0:T(8,128)(2,1)S(1)} %get-tuple-element.43), channel_id=1, source_target_pairs={{0,16},{8,24},{16,0},{24,8},{32,48},{40,56},{48,32},{56,40},{64,80... | collective-permute-start | bytes 393224 | tf_op jit(solution)/shard_map/ppermute | solution.py:209
  92.9 7.0 %collective-permute-start.31 = (bf16[1,2,8,32,128]{4,3,2,1,0:T(8,128)(2,1)S(1)}, bf16[1,2,8,32,128]{4,3,2,1,0:T(8,128)(2,1)S(1)}, u32[]{:S(2)}, u32[]{:S(2)}) collective-permute-start(bf16[1,2,8,32,128]{4,3,2,1,0:T(8,128)(2,1)S(1)} %get-tuple-element.44), channel_id=1, source_target_pairs={{0,24},{8,0},{16,8},{24,16},{32,56},{40,32},{48,40},{56,48},{64,88... | collective-permute-start | bytes 393224 | tf_op jit(solution)/shard_map/ppermute | solution.py:209
  94.1 9.8 %collective-permute-start.35 = (bf16[128,2048]{1,0:T(8,128)(2,1)S(1)}, bf16[128,2048]{1,0:T(8,128)(2,1)}, u32[]{:S(2)}, u32[]{:S(2)}) collective-permute-start(bf16[128,2048]{1,0:T(8,128)(2,1)S(1)} %slice.89), channel_id=1, source_target_pairs={{0,6},{1,7},{2,0},{3,1},{4,2},{5,3},{6,4},{7,5},{8,14},{9,15},{10,... | collective-permute-start | bytes 1572872 | tf_op jit(solution)/shard_map/ppermute | solution.py:215
  98.0 10.5 %collective-permute-start.34 = (bf16[128,2048]{1,0:T(8,128)(2,1)S(1)}, bf16[128,2048]{1,0:T(8,128)(2,1)}, u32[]{:S(2)}, u32[]{:S(2)}) collective-permute-start(bf16[128,2048]{1,0:T(8,128)(2,1)S(1)} %slice.88), channel_id=1, source_target_pairs={{0,2},{1,3},{2,4},{3,5},{4,6},{5,7},{6,0},{7,1},{8,10},{9,11},{10,... | collective-permute-start | bytes 1572872 | tf_op jit(solution)/shard_map/ppermute | solution.py:214
  98.7 52.8 %collective-permute-start.36 = (bf16[256,2048]{1,0:T(8,128)(2,1)}, bf16[256,2048]{1,0:T(8,128)(2,1)}, u32[]{:S(2)}, u32[]{:S(2)}) collective-permute-start(bf16[256,2048]{1,0:T(8,128)(2,1)} %refs_0_.1), channel_id=1, source_target_pairs={{0,1},{1,0},{2,3},{3,2},{4,5},{5,4},{6,7},{7,6},{8,9},{9,8},{10,11... | collective-permute-start | bytes 3145736 | tf_op jit(solution)/shard_map/ppermute | solution.py:217
  99.4 62.3 %collective-permute-start.38 = (bf16[256,2048]{1,0:T(8,128)(2,1)S(1)}, bf16[256,2048]{1,0:T(8,128)(2,1)}, u32[]{:S(2)}, u32[]{:S(2)}) collective-permute-start(bf16[256,2048]{1,0:T(8,128)(2,1)S(1)} %collective-permute-done.33.refs_2_), channel_id=1, source_target_pairs={{0,1},{1,0},{2,3},{3,2},{4,5},{5,4},{6,7},{7,6},{8,9},{9,8},{10,11... | collective-permute-start | bytes 3145736 | tf_op jit(solution)/shard_map/ppermute | solution.py:217
  100.6 61.1 %collective-permute-start.37 = (bf16[256,2048]{1,0:T(8,128)(2,1)S(1)}, bf16[256,2048]{1,0:T(8,128)(2,1)}, u32[]{:S(2)}, u32[]{:S(2)}) collective-permute-start(bf16[256,2048]{1,0:T(8,128)(2,1)S(1)} %collective-permute-done.32.refs_1_), channel_id=1, source_target_pairs={{0,1},{1,0},{2,3},{3,2},{4,5},{5,4},{6,7},{7,6},{8,9},{9,8},{10,11... | collective-permute-start | bytes 3145736 | tf_op jit(solution)/shard_map/ppermute | solution.py:217
  104.0 57.7 %collective-permute-start.40 = (bf16[128,2048]{1,0:T(8,128)(2,1)}, bf16[128,2048]{1,0:T(8,128)(2,1)}, u32[]{:S(2)}, u32[]{:S(2)}) collective-permute-start(bf16[128,2048]{1,0:T(8,128)(2,1)} %collective-permute-done.35.refs_4_), channel_id=1, source_target_pairs={{0,1},{1,0},{2,3},{3,2},{4,5},{5,4},{6,7},{7,6},{8,9},{9,8},{10,11... | collective-permute-start | bytes 1572872 | tf_op jit(solution)/shard_map/ppermute | solution.py:217
  108.5 53.2 %collective-permute-start.39 = (bf16[128,2048]{1,0:T(8,128)(2,1)}, bf16[128,2048]{1,0:T(8,128)(2,1)}, u32[]{:S(2)}, u32[]{:S(2)}) collective-permute-start(bf16[128,2048]{1,0:T(8,128)(2,1)} %collective-permute-done.34.refs_3_), channel_id=1, source_target_pairs={{0,1},{1,0},{2,3},{3,2},{4,5},{5,4},{6,7},{7,6},{8,9},{9,8},{10,11... | collective-permute-start | bytes 1572872 | tf_op jit(solution)/shard_map/ppermute | solution.py:217
  120.7 1.0 copy-start.3
  121.7 1.0 copy-start.4
  122.7 0.9 copy-start.6
  123.7 0.9 copy-start.8
  124.6 0.9 copy-start.10
  125.6 0.9 copy-start.12
  126.5 0.9 copy-start.14
  127.5 0.9 copy-start.16
  128.4 0.9 copy-start.18
  129.4 0.9 copy-start.20
  130.3 0.9 copy-start.22
  131.3 0.9 copy-start.24
  132.2 0.9 copy-start.26
  133.2 0.9 copy-start.28
  136.9 0.9 copy-start.36
  137.8 0.9 copy-start.38
  147.2 14.5 %all-to-all-start = ((bf16[8,128,256]{2,1,0:T(8,128)(2,1)}), bf16[8,128,256]{2,1,0:T(8,128)(2,1)}, u32[]{:S(2)}, u32[]{:S(2)}) async-start(bf16[8,128,256]{2,1,0:T(8,128)(2,1)} %bitcast.31), calls=%async_computation | async-start | bytes 1048576 | tf_op jit(solution)/shard_map/all_to_all | solution.py:221
  (23 other events, 17.0 us)

commit v2 on v1

v2 whole, which is shorter than its diff:
```python
import jax
import jax.numpy as jnp
import numpy as np
from jax import lax
from jax.experimental import pallas as pl
from jax.experimental.pallas import tpu as pltpu
from jax.sharding import PartitionSpec as P

HEAD = 128
QB = 128
KB = 32
NFAR = 12
NX = 4
NZ = 8
NY = 4
GROUP = 4
BF = jnp.bfloat16
F32 = jnp.float32
NT = (((1,), (1,)), ((), ()))


CORES = [(t, t ^ 1) for t in range(2 * NY)]


def along_z(k):
    return [(z * NX + x, (z + k) % NZ * NX + x) for z in range(NZ) for x in range(NX)]


def along_x(k):
    return [(z * NX + x, z * NX + (x + k) % NX) for z in range(NZ) for x in range(NX)]


def across(r):
    return [(z * NX + x, (z + 1) % NZ * NX + (x + r) % NX) for z in range(NZ) for x in range(NX)]


def along_y(k):
    return [(y * 2 + c, (y + k) % NY * 2 + c) for y in range(NY) for c in range(2)]


def dot(a, b):
    return jnp.dot(a, b, preferred_element_type=F32)


VMEM = pl.BlockSpec(memory_space=pltpu.VMEM)
SMEM = pl.BlockSpec(memory_space=pltpu.SMEM)
ANY = pl.BlockSpec(memory_space=pl.ANY)


def params(mib):
    return pltpu.CompilerParams(vmem_limit_bytes=mib * 1024 * 1024)


def rows_body(count, parts):
    def body(tok, *refs):
        weights, (out, t, w, sems) = refs[:count], refs[count:]
        tile = out.shape[0] // parts
        wide = out.shape[1] // count
        copies = [
            pltpu.make_async_copy(ref, w.at[:, pl.ds(n * wide, wide)], sems.at[n])
            for n, ref in enumerate(weights)
        ]
        blocks = [pl.ds(n * tile, tile) for n in range(parts)]
        copies += [
            pltpu.make_async_copy(tok.at[b], t.at[b], sems.at[count + n]) for n, b in enumerate(blocks)
        ]
        for c in copies:
            c.start()
        for c in copies[:count]:
            c.wait()
        for c, b in zip(copies[count:], blocks):
            c.wait()
            out[b, :] = dot(t[b, :], w[...]).astype(BF)

    return body


def rows_project(tokens, weights, limit):
    rows, width = tokens.shape
    parts = 4
    total = sum(w.shape[1] for w in weights)
    return pl.pallas_call(
        rows_body(len(weights), parts),
        out_shape=jax.ShapeDtypeStruct((rows, total), BF),
        in_specs=[ANY] * (1 + len(weights)),
        out_specs=VMEM,
        scratch_shapes=[
            pltpu.VMEM((rows, width), BF),
            pltpu.VMEM((width, total), BF),
            pltpu.SemaphoreType.DMA((len(weights) + parts,)),
        ],
        compiler_params=params(limit),
        cost_estimate=pl.CostEstimate(
            flops=1_000_000_000, bytes_accessed=6_000_000, transcendentals=0
        ),
    )(tokens, *weights)


def pick_body(first, count, offsets):
    def body(want, *refs):
        ins, outs = refs[:count], refs[count:]

        def step(j, carry):
            for d in range(count):
                for out, r in zip(outs, offsets):
                    b = pl.multiple_of(want[r, (first + d) * 8 + j] * KB, KB)
                    out[d, j] = ins[d][pl.ds(b, KB), :]
            return carry

        lax.fori_loop(0, 8, step, 0)

    return body


def pick(want, first, held, offsets):
    count = len(held)
    return pl.pallas_call(
        pick_body(first, count, offsets),
        out_shape=[jax.ShapeDtypeStruct((count, 8, KB, 2 * HEAD), BF)] * len(offsets),
        in_specs=[SMEM] + [VMEM] * count,
        out_specs=[VMEM] * len(offsets),
        compiler_params=params(6),
        cost_estimate=pl.CostEstimate(
            flops=4_000_000 * count, bytes_accessed=1_000_000 * count, transcendentals=0
        ),
    )(want, *held)


def gather_blocks(kv, want, held, recv, counts, first, last, j):
    slot = 0
    source = 0

    def put(block):
        nonlocal slot
        kv[slot * KB : (slot + 1) * KB, :] = block
        slot += 1

    for b, count in enumerate(counts):
        for d in range(count):
            mine = pl.multiple_of(want[0, (first + source) * 8 + j] * KB, KB)
            put(held[source][pl.ds(mine, KB), :])
            for r in range(1, NX):
                put(recv[(NX - 1) * b + r - 1][d, j])
            source += 1
    for r in range(last):
        put(recv[(NX - 1) * len(counts) + r][0, j])


def both_heads(q, at):
    return jnp.concatenate([q[pl.ds(at, QB), :HEAD], q[pl.ds(at, QB), HEAD:]], axis=0)


def row_max(a):
    return jnp.max(a, axis=1, keepdims=True)


def row_sum(a):
    return jnp.sum(a, axis=1, keepdims=True)


def places(g, n):
    j = g * GROUP + n
    return j, pl.multiple_of(j * QB, QB), pl.ds(pl.multiple_of(j * 2 * QB, 2 * QB), 2 * QB)


def early_body(counts):
    total = sum(counts)
    far = total * NX * KB

    def body(want, bias, q, *refs):
        held, recv = refs[:total], refs[total:-4]
        acc, top, low, kv = refs[-4:]
        row = lax.broadcasted_iota(jnp.int32, (2 * QB, QB), 0) % QB
        col = lax.broadcasted_iota(jnp.int32, (2 * QB, QB), 1)
        causal = jnp.where(col <= row, 0.0, -jnp.inf).astype(F32)
        scale = HEAD ** (-0.5)

        def step(g, carry):
            spots = [places(g, n) for n in range(GROUP)]
            own, oth, m = [], [], []
            for n, (j, at, to) in enumerate(spots):
                gather_blocks(kv.at[n], want, held, recv, counts, 0, 0, j)
            for n, (j, at, to) in enumerate(spots):
                qq = both_heads(q, at)
                mine = held[0][pl.ds(at, QB), :HEAD]
                own.append(lax.dot_general(qq, mine, NT, preferred_element_type=F32) * scale + causal)
                theirs = kv[n, :, :HEAD]
                oth.append(
                    lax.dot_general(qq, theirs, NT, preferred_element_type=F32) * scale
                    + bias[pl.ds(j, 1), :far]
                )
            for n in range(GROUP):
                m.append(jnp.maximum(row_max(own[n]), row_max(oth[n])))
            for n in range(GROUP):
                own[n] = jnp.exp(own[n] - m[n])
                oth[n] = jnp.exp(oth[n] - m[n])
            for n, (j, at, to) in enumerate(spots):
                top[to, :] = jnp.broadcast_to(m[n], (2 * QB, HEAD))
                low[to, :] = jnp.broadcast_to(row_sum(own[n]) + row_sum(oth[n]), (2 * QB, HEAD))
                mixed = dot(own[n].astype(BF), held[0][pl.ds(at, QB), HEAD:])
                acc[to, :] = mixed + dot(oth[n].astype(BF), kv[n, :, HEAD:])
            return carry

        lax.fori_loop(0, q.shape[0] // QB // GROUP, step, 0)

    return body


def late_body(counts, first, last):
    total = sum(counts)

    def body(want, bias, q, acc, top, low, *refs):
        held, recv = refs[:total], refs[total:-2]
        out, kv = refs[-2:]
        begin = first * NX * KB
        far = kv.shape[1]
        scale = HEAD ** (-0.5)

        def step(g, carry):
            spots = [places(g, n) for n in range(GROUP)]
            oth, m, keep, inv = [], [], [], []
            for n, (j, at, to) in enumerate(spots):
                gather_blocks(kv.at[n], want, held, recv, counts, first, last, j)
            for n, (j, at, to) in enumerate(spots):
                part = lax.dot_general(both_heads(q, at), kv[n, :, :HEAD], NT, preferred_element_type=F32)
                oth.append(part * scale + bias[pl.ds(j, 1), begin : begin + far])
            for n, (j, at, to) in enumerate(spots):
                m.append(jnp.maximum(top[to, :], row_max(oth[n])))
            for n, (j, at, to) in enumerate(spots):
                oth[n] = jnp.exp(oth[n] - jnp.concatenate([m[n]] * (far // HEAD), axis=1))
                keep.append(jnp.exp(top[to, :] - m[n]))
            for n, (j, at, to) in enumerate(spots):
                inv.append(1.0 / (low[to, :] * keep[n] + row_sum(oth[n])))
            for n, (j, at, to) in enumerate(spots):
                mixed = acc[to, :] * keep[n] + dot(oth[n].astype(BF), kv[n, :, HEAD:])
                mixed = (mixed * inv[n]).astype(BF)
                out[pl.ds(at, QB), :HEAD] = mixed[:QB]
                out[pl.ds(at, QB), HEAD:] = mixed[QB:]
            return carry

        lax.fori_loop(0, q.shape[0] // QB // GROUP, step, 0)

    return body


def attend_early(want, bias, q, held, recv):
    counts = [r[0].shape[0] for r in recv]
    ins = [*held, *[a for r in recv for a in r]]
    rows = 2 * q.shape[0]
    return pl.pallas_call(
        early_body(counts),
        out_shape=[
            jax.ShapeDtypeStruct((rows, HEAD), F32),
            jax.ShapeDtypeStruct((rows, HEAD), F32),
            jax.ShapeDtypeStruct((rows, HEAD), F32),
        ],
        in_specs=[SMEM] + [VMEM] * (2 + len(ins)),
        out_specs=[VMEM] * 3,
        scratch_shapes=[pltpu.VMEM((GROUP, sum(counts) * NX * KB, 2 * HEAD), BF)],
        compiler_params=params(16),
        cost_estimate=pl.CostEstimate(
            flops=900_000_000, bytes_accessed=6_000_000, transcendentals=1_600_000
        ),
        name="early",
    )(want, bias, q, *ins)


def attend_late(want, bias, q, sums, held, recv, last):
    counts = [r[0].shape[0] for r in recv]
    first = bias.shape[1] // (NX * KB) - sum(counts) - 1
    ins = [*held, *[a for r in recv for a in r], *last]
    return pl.pallas_call(
        late_body(counts, first, len(last)),
        out_shape=jax.ShapeDtypeStruct(q.shape, BF),
        in_specs=[SMEM] + [VMEM] * (2 + len(sums) + len(ins)),
        out_specs=VMEM,
        scratch_shapes=[pltpu.VMEM((GROUP, (sum(counts) + 1) * NX * KB, 2 * HEAD), BF)],
        compiler_params=params(16),
        cost_estimate=pl.CostEstimate(
            flops=400_000_000, bytes_accessed=6_000_000, transcendentals=800_000
        ),
        name="late",
    )(want, bias, q, *sums, *ins)


def project_body(spot, att, *refs):
    count = 2 * NY
    weights, (out, near, acc, sems) = refs[:count], refs[count:]
    copies = [pltpu.make_async_copy(w, near.at[i], sems.at[i]) for i, w in enumerate(weights)]
    for c in copies:
        c.start()
    tile = 512
    for i, c in enumerate(copies):
        c.wait()
        mine = att[spot[i // NY, i % NY]]
        for n in range(out.shape[1] // tile):
            cols = slice(n * tile, (n + 1) * tile)
            part = dot(mine, near[i, :, cols]).astype(BF).astype(F32)
            if i == 0:
                acc[:, cols] = part
            elif i < count - 1:
                acc[:, cols] += part
            else:
                out[:, cols] = (acc[:, cols] + part).astype(BF)


def project(spot, att, weights):
    deep, width = weights[0].shape
    return pl.pallas_call(
        project_body,
        out_shape=jax.ShapeDtypeStruct((QB, width), BF),
        in_specs=[SMEM, VMEM] + [ANY] * len(weights),
        out_specs=VMEM,
        scratch_shapes=[
            pltpu.VMEM((len(weights), deep, width), BF),
            pltpu.VMEM((QB, width), F32),
            pltpu.SemaphoreType.DMA((len(weights),)),
        ],
        compiler_params=params(14),
        cost_estimate=pl.CostEstimate(
            flops=1_000_000_000, bytes_accessed=9_000_000, transcendentals=0
        ),
        name="project",
    )(spot, att, *weights)


def layer(tokens, wq, wk, wv, wo, chosen):
    me = lax.axis_index("kv")
    z, x = me // NX, me % NX
    tp = lax.axis_index("tp")
    per = tokens.shape[0] // KB

    kv = rows_project(tokens, (wk, wv), 60)

    row = jnp.stack([chosen] + [lax.ppermute(chosen, "kv", along_x(-r)) for r in range(1, NX)])
    above = lax.ppermute(row, "kv", along_z(-1))

    order = [0, *[d for s in range(1, NZ // 2) for d in (s, NZ - s)], NZ // 2]

    def wants(lists, dist):
        groups = (z - np.repeat(np.array(dist, np.int32), chosen.shape[0])) % NZ * NX + x
        named = jnp.concatenate([lists] * len(dist), axis=1)
        mine = named // per == groups[None, :, None]
        return jnp.sum(jnp.where(mine, named % per, 0), axis=2)

    want = wants(row, order[:-1])
    want_above = wants(above, [NZ // 2 - 1])
    dist = np.repeat(np.array(order, np.int32), NX * KB)
    beyond = np.tile(np.repeat(np.arange(NX, dtype=np.int32), KB), NZ)
    source = (z - dist) % NZ * NX + (x - beyond) % NX
    groups = chosen // per
    here = groups[:, :1] == source[None, :]
    for n in range(1, NFAR):
        here = here | (groups[:, n : n + 1] == source[None, :])
    bias = jnp.where(here, 0.0, -jnp.inf).astype(F32)

    held = {0: kv}
    up = down = kv
    for step in range(1, NZ // 2):
        up = held[step] = lax.ppermute(up, "kv", along_z(1))
        down = held[NZ - step] = lax.ppermute(down, "kv", along_z(-1))

    recv = []
    batches = [[0, 1, NZ - 1]] + [[s, NZ - s] for s in range(2, NZ // 2)]
    beside = range(1, NX)
    for batch in batches:
        sent = pick(want, order.index(batch[0]), [held[d] for d in batch], beside)
        recv.append([lax.ppermute(a, "kv", along_x(r)) for a, r in zip(sent, beside)])
    sent = pick(want_above, 0, [held[NZ // 2 - 1]], range(NX))
    last = [lax.ppermute(a, "kv", across(r)) for r, a in enumerate(sent)]

    wm = lax.ppermute(wo, "tp", along_y(1))
    wp = lax.ppermute(wo, "tp", along_y(-1))
    weights = [wo, wm, wp, lax.ppermute(wm, "tp", along_y(1))]
    weights += [lax.ppermute(w, "tp", CORES) for w in weights]

    q = rows_project(tokens, (wq,), 60)
    line = [held[d] for d in order[:-1]]
    cut = len(line) - len(batches[-1])
    sums = attend_early(want, bias, q, line[:cut], recv[:-1])
    mixed = attend_late(want, bias, q, sums, line[cut:], recv[-1:], last)
    att = lax.all_to_all(mixed.reshape(2 * NY, QB, -1), "tp", 0, 0, tiled=True)
    y, c = tp // 2, tp % 2
    rows = jnp.stack([y, (y - 1) % NY, (y + 1) % NY, (y + 2) % NY]) * 2
    return project(jnp.stack([rows + c, rows + 1 - c]), att, weights)


def solution(mesh):
    return jax.shard_map(
        layer,
        mesh=mesh,
        in_specs=(
            P("kv", None),
            P(None, "tp"),
            P(None, "tp"),
            P(None, "tp"),
            P("tp", None),
            P("kv", None),
        ),
        out_specs=P(("kv", "tp"), None),
        check_vma=False,
    )
```

time: 171 us -> 134 us (0.78); the launches traced: 168 us -> 133 us
  local copies, waits for them, and re-layouts: 44.5 us -> 9.21 us
  Pallas kernels: 16.6 us -> 28.3 us
  matrix products: 11.2 us -> 0 us
  starting transfers between devices: 63.8 us -> 56.6 us
  waiting for transfers between devices: 29.8 us -> 36.8 us
    unnamed x90 -> x46, local copies, waits for them, and re-layouts: 32.2 us -> 8.03 us
    pallas_call x6 -> x8, Pallas kernels: 9.98 us -> 23.1 us  [the longest x2 10.3 us: rows_project(): pl.pallas_call(rows_body(len(weights), parts), out_shape=jax.ShapeDtypeSt...]
    ppermute x31 -> x21, starting transfers between devices: 50.8 us -> 39.3 us  [the longest x9 14.5 us: layer(): lax.ppermute(a, 'kv', along_x(r))]
    dot_general x3 -> x0, matrix products: 11.2 us -> none  [dot(): return jnp.dot(a, b, preferred_element_type=F32)]
    ppermute x31 -> x21, waiting for transfers between devices: 19.6 us -> 26.4 us  [the longest x9 9.89 us: layer(): lax.ppermute(a, 'kv', along_x(r))]
    slice x12 -> x1, local copies, waits for them, and re-layouts: 7.36 us -> 0.9 us  [layer(): here = groups[:, :1] == source[None, :]]
    squeeze x8 -> x0, local copies, waits for them, and re-layouts: 4.19 us -> none  [layer(): place[:, d]]
    all_to_all x1, starting transfers between devices: 4.16 us -> 7.24 us  [layer(): att = lax.all_to_all(mixed.reshape(2 * NY, QB, -1), 'tp', 0, 0, tiled=True)]
  transfers between devices with their start and end apart: 42 -> 31, of which waited for: 8 -> 10; matrix products, arithmetic and copies ran while one was open for 15% -> 2% of each run, Pallas kernels for 6% -> 13%
where the time goes in v2:
time: 134 us; the launch traced here: 133 us
  starting transfers between devices  56.6 us (42%)
  waiting for transfers between devices  36.8 us (27%)
  Pallas kernels  28.3 us (21%)
  local copies, waits for them, and re-layouts  9.21 us (7%)
  other arithmetic  1.93 us (1%)
    ppermute x9, starting transfers between devices, layer(): lax.ppermute(a, 'kv', along_x(r))  14.5 us
    pallas_call x2, Pallas kernels, rows_project(): pl.pallas_call(rows_body(len(weights), parts), out_shape=jax.ShapeDtypeSt...  10.3 us
    all_to_all x1, waiting for transfers between devices, layer(): att = lax.all_to_all(mixed.reshape(2 * NY, QB, -1), 'tp', 0, 0, tiled=True)  10.2 us
    ppermute x3, starting transfers between devices, layer(): down = held[NZ - step] = lax.ppermute(down, 'kv', along_z(-1))  10 us
    ppermute x9, waiting for transfers between devices, layer(): lax.ppermute(a, 'kv', along_x(r))  9.89 us
    ppermute x3, waiting for transfers between devices, layer(): up = held[step] = lax.ppermute(up, 'kv', along_z(1))  9.54 us
    ppermute x4, starting transfers between devices, layer(): last = [lax.ppermute(a, 'kv', across(r)) for r, a in enumerate(sent)]  9.51 us
    unnamed x46, local copies, waits for them, and re-layouts  8.03 us
  transfers between devices with their start and end apart: 31, of which 10 were waited for; matrix products, arithmetic and copies ran while one was open for 2% of the time, Pallas kernels for 13%

profile of v2, /device:TPU:2, one launch (start us, length us, event | category | flops | bytes accessed | tf_op | source)
XLA Modules:
  0.0 133.3 jit_solution(5415378444971538404)
XLA Ops:
  0.0 5.2 %shard_map.101.refs_0_ = bf16[1024,256]{1,0:T(8,128)(2,1)} custom-call(bf16[1024,2048]{1,0:T(8,128)(2,1)} %tok.3, bf16[2048,128]{1,0:T(8,128)(2,1)} %refs_0_.4, bf16[2048,128]{1,0:T(8,128)(2,1)} %refs_1_.1), custom_call_target="tpu_custom_call" | custom-call | flops 1000000000 | bytes 6000000 | tf_op jit(solution)/shard_map/pallas_call | solution.py:82
  5.2 2.0 %collective-permute-start.3 = (bf16[1024,256]{1,0:T(8,128)(2,1)}, bf16[1024,256]{1,0:T(8,128)(2,1)S(1)}, u32[]{:S(2)}, u32[]{:S(2)}) collective-permute-start(bf16[1024,256]{1,0:T(8,128)(2,1)} %shard_map.101.refs_0_), channel_id=1, source_target_pairs={{0,32},{8,40},{16,48},{24,56},{32,64},{40,72},{48,80},{56,88},{64,... | collective-permute-start | bytes 1572872 | tf_op jit(solution)/shard_map/ppermute | solution.py:360
  7.2 4.0 %collective-permute-start.4 = (bf16[1024,256]{1,0:T(8,128)(2,1)}, bf16[1024,256]{1,0:T(8,128)(2,1)S(1)}, u32[]{:S(2)}, u32[]{:S(2)}) collective-permute-start(bf16[1024,256]{1,0:T(8,128)(2,1)} %shard_map.101.refs_0_), channel_id=1, source_target_pairs={{0,224},{8,232},{16,240},{24,248},{32,0},{40,8},{48,16},{56,24},{6... | collective-permute-start | bytes 1572872 | tf_op jit(solution)/shard_map/ppermute | solution.py:361
  11.2 0.5 collective-permute-start
  11.8 2.4 %collective-permute-start.1 = (s32[8,12]{1,0:T(8,128)S(1)}, s32[8,12]{1,0:T(8,128)S(1)}, u32[]{:S(2)}, u32[]{:S(2)}) collective-permute-start(s32[8,12]{1,0:T(8,128)S(1)} %copy-done.19), channel_id=1, source_target_pairs={{0,16},{8,24},{16,0},{24,8},{32,48},{40,56},{48,32},{56,40},{64,80... | collective-permute-start | bytes 1160 | tf_op jit(solution)/shard_map/ppermute | solution.py:335
  14.2 1.8 %collective-permute-start.2 = (s32[8,12]{1,0:T(8,128)S(1)}, s32[8,12]{1,0:T(8,128)S(1)}, u32[]{:S(2)}, u32[]{:S(2)}) collective-permute-start(s32[8,12]{1,0:T(8,128)S(1)} %copy-done.19), channel_id=1, source_target_pairs={{0,8},{8,16},{16,24},{24,0},{32,40},{40,48},{48,56},{56,32},{64,72... | collective-permute-start | bytes 1160 | tf_op jit(solution)/shard_map/ppermute | solution.py:335
  16.0 0.0 collective-permute-done
  16.0 1.6 %collective-permute-start.23 = (bf16[256,2048]{1,0:T(8,128)(2,1)}, bf16[256,2048]{1,0:T(8,128)(2,1)}, u32[]{:S(2)}, u32[]{:S(2)}) collective-permute-start(bf16[256,2048]{1,0:T(8,128)(2,1)} %refs_0_.5), channel_id=1, source_target_pairs={{0,2},{1,3},{2,4},{3,5},{4,6},{5,7},{6,0},{7,1},{8,10},{9,11},{10,... | collective-permute-start | bytes 3145736 | tf_op jit(solution)/shard_map/ppermute | solution.py:372
  17.6 0.2 collective-permute-done.2
  17.8 0.1 copy.11
  17.9 0.2 concatenate.14
  18.1 0.1 fusion.2.want
  18.2 5.1 %collective-permute-done.3.refs_1_ = bf16[1024,256]{1,0:T(8,128)(2,1)S(1)} collective-permute-done((bf16[1024,256]{1,0:T(8,128)(2,1)}, bf16[1024,256]{1,0:T(8,128)(2,1)S(1)}, u32[]{:S(2)}, u32[]{:S(2)}) %collective-permute-start.3) | collective-permute-done | bytes 524320 | tf_op jit(solution)/shard_map/ppermute | solution.py:360
  23.3 1.0 copy-done.1
  24.3 0.7 shard_map.102
  25.1 1.6 %collective-permute-start.7 = (bf16[3,8,32,256]{3,2,1,0:T(8,128)(2,1)S(1)}, bf16[3,8,32,256]{3,2,1,0:T(8,128)(2,1)S(1)}, u32[]{:S(2)}, u32[]{:S(2)}) collective-permute-start(bf16[3,8,32,256]{3,2,1,0:T(8,128)(2,1)S(1)} %get-tuple-element.21), channel_id=1, source_target_pairs={{0,8},{8,16},{16,24},{24,0},{32,40},{40,48},{48,56},{56,32},{64,72... | collective-permute-start | bytes 1179656 | tf_op jit(solution)/shard_map/ppermute | solution.py:368
  26.6 3.0 %collective-permute-start.24 = (bf16[256,2048]{1,0:T(8,128)(2,1)}, bf16[256,2048]{1,0:T(8,128)(2,1)S(1)}, u32[]{:S(2)}, u32[]{:S(2)}) collective-permute-start(bf16[256,2048]{1,0:T(8,128)(2,1)} %refs_0_.5), channel_id=1, source_target_pairs={{0,6},{1,7},{2,0},{3,1},{4,2},{5,3},{6,4},{7,5},{8,14},{9,15},{10,... | collective-permute-start | bytes 3145736 | tf_op jit(solution)/shard_map/ppermute | solution.py:373
  29.7 3.2 %collective-permute-start.18 = (s32[4,8,12]{2,1,0:T(8,128)S(1)}, s32[4,8,12]{2,1,0:T(8,128)S(1)}, u32[]{:S(2)}, u32[]{:S(2)}) collective-permute-start(s32[4,8,12]{2,1,0:T(8,128)S(1)} %pad_add_fusion), channel_id=1, source_target_pairs={{0,224},{8,232},{16,240},{24,248},{32,0},{40,8},{48,16},{56,24},{6... | collective-permute-start | bytes 4616 | tf_op jit(solution)/shard_map/ppermute | solution.py:336
  32.9 1.4 %collective-permute-done.18 = s32[4,8,12]{2,1,0:T(8,128)S(1)} collective-permute-done((s32[4,8,12]{2,1,0:T(8,128)S(1)}, s32[4,8,12]{2,1,0:T(8,128)S(1)}, u32[]{:S(2)}, u32[]{:S(2)}) %collective-permute-start.18) | collective-permute-done | bytes 1568 | tf_op jit(solution)/shard_map/ppermute | solution.py:336
  34.3 3.5 %collective-permute-start.6 = (bf16[1024,256]{1,0:T(8,128)(2,1)S(1)}, bf16[1024,256]{1,0:T(8,128)(2,1)S(1)}, u32[]{:S(2)}, u32[]{:S(2)}) collective-permute-start(bf16[1024,256]{1,0:T(8,128)(2,1)S(1)} %collective-permute-done.4.refs_2_), channel_id=1, source_target_pairs={{0,224},{8,232},{16,240},{24,248},{32,0},{40,8},{48,16},{56,24},{6... | collective-permute-start | bytes 1572872 | tf_op jit(solution)/shard_map/ppermute | solution.py:361
  37.8 1.1 collective-permute-start.8
  39.0 4.4 %collective-permute-done.5.refs_0_.refs_3_ = bf16[1024,256]{1,0:T(8,128)(2,1)S(1)} collective-permute-done((bf16[1024,256]{1,0:T(8,128)(2,1)S(1)}, bf16[1024,256]{1,0:T(8,128)(2,1)S(1)}, u32[]{:S(2)}, u32[]{:S(2)}) %collective-permute-start.5) | collective-permute-done | bytes 524320 | tf_op jit(solution)/shard_map/ppermute | solution.py:360
  43.4 4.4 %collective-permute-done.8.refs_6_ = bf16[3,8,32,256]{3,2,1,0:T(8,128)(2,1)S(1)} collective-permute-done((bf16[3,8,32,256]{3,2,1,0:T(8,128)(2,1)S(1)}, bf16[3,8,32,256]{3,2,1,0:T(8,128)(2,1)S(1)}, u32[]{:S(2)}, u32[]{:S(2)}) %collective-permute-start.8) | collective-permute-done | bytes 393248 | tf_op jit(solution)/shard_map/ppermute | solution.py:368
  47.8 0.8 copy-done.5
  48.6 0.7 collective-permute-start.9
  49.2 2.5 %collective-permute-start.14 = (bf16[1024,256]{1,0:T(8,128)(2,1)S(1)}, bf16[1024,256]{1,0:T(8,128)(2,1)}, u32[]{:S(2)}, u32[]{:S(2)}) collective-permute-start(bf16[1024,256]{1,0:T(8,128)(2,1)S(1)} %collective-permute-done.6.refs_1_.refs_4_), channel_id=1, source_target_pairs={{0,224},{8,232},{16,240},{24,248},{32,0},{40,8},{48,16},{56,24},{6... | collective-permute-start | bytes 1572872 | tf_op jit(solution)/shard_map/ppermute | solution.py:361
  51.7 1.6 %shard_map.103 = (bf16[2,8,32,256]{3,2,1,0:T(8,128)(2,1)}, bf16[2,8,32,256]{3,2,1,0:T(8,128)(2,1)}, bf16[2,8,32,256]{3,2,1,0:T(8,128)(2,1)}) custom-call(s32[4,56]{1,0:T(4,128)S(1)} %fusion.2.want, bf16[1024,256]{1,0:T(8,128)(2,1)S(1)} %collective-permute-done.5.refs_0_.refs_3_, bf16[1024,256]{1,0:T(8,128)(2,1)S(1)} %collective-permute-done.6.refs_1_.refs_4_), custom_call_target="tpu_custom_call" | custom-call | flops 8000000 | bytes 2000000 | tf_op jit(solution)/shard_map/pallas_call | solution.py:117
  53.3 3.1 %collective-permute-done.9.refs_7_ = bf16[3,8,32,256]{3,2,1,0:T(8,128)(2,1)S(1)} collective-permute-done((bf16[3,8,32,256]{3,2,1,0:T(8,128)(2,1)S(1)}, bf16[3,8,32,256]{3,2,1,0:T(8,128)(2,1)S(1)}, u32[]{:S(2)}, u32[]{:S(2)}) %collective-permute-start.9) | collective-permute-done | bytes 393248 | tf_op jit(solution)/shard_map/ppermute | solution.py:368
  56.3 0.8 copy-done.7
  57.1 1.2 collective-permute-start.10
  58.3 1.5 %collective-permute-start.11 = (bf16[2,8,32,256]{3,2,1,0:T(8,128)(2,1)}, bf16[2,8,32,256]{3,2,1,0:T(8,128)(2,1)}, u32[]{:S(2)}, u32[]{:S(2)}) collective-permute-start(bf16[2,8,32,256]{3,2,1,0:T(8,128)(2,1)} %get-tuple-element.25), channel_id=1, source_target_pairs={{0,16},{8,24},{16,0},{24,8},{32,48},{40,56},{48,32},{56,40},{64,80... | collective-permute-start | bytes 786440 | tf_op jit(solution)/shard_map/ppermute | solution.py:368
  59.8 2.2 %collective-permute-start.12 = (bf16[2,8,32,256]{3,2,1,0:T(8,128)(2,1)}, bf16[2,8,32,256]{3,2,1,0:T(8,128)(2,1)}, u32[]{:S(2)}, u32[]{:S(2)}) collective-permute-start(bf16[2,8,32,256]{3,2,1,0:T(8,128)(2,1)} %get-tuple-element.26), channel_id=1, source_target_pairs={{0,24},{8,0},{16,8},{24,16},{32,56},{40,32},{48,40},{56,48},{64,88... | collective-permute-start | bytes 786440 | tf_op jit(solution)/shard_map/ppermute | solution.py:368
  62.1 0.9 fusion.6.want
  63.0 0.7 shard_map.105
  63.7 0.1 collective-permute-start.19
  63.8 1.9 %shard_map.104 = (bf16[2,8,32,256]{3,2,1,0:T(8,128)(2,1)S(1)}, bf16[2,8,32,256]{3,2,1,0:T(8,128)(2,1)}, bf16[2,8,32,256]{3,2,1,0:T(8,128)(2,1)S(1)}) custom-call(s32[4,56]{1,0:T(4,128)S(1)} %fusion.2.want, bf16[1024,256]{1,0:T(8,128)(2,1)S(1)} %collective-permute-done.13.refs_0_, bf16[1024,256]{1,0:T(8,128)(2,1)} %collective-permute-done.14.refs_1_), custom_call_target="tpu_custom_call" | custom-call | flops 8000000 | bytes 2000000 | tf_op jit(solution)/shard_map/pallas_call | solution.py:117
  65.6 0.7 copy-done.17
  66.3 2.1 %collective-permute-start.15 = (bf16[2,8,32,256]{3,2,1,0:T(8,128)(2,1)S(1)}, bf16[2,8,32,256]{3,2,1,0:T(8,128)(2,1)S(1)}, u32[]{:S(2)}, u32[]{:S(2)}) collective-permute-start(bf16[2,8,32,256]{3,2,1,0:T(8,128)(2,1)S(1)} %get-tuple-element.30), channel_id=1, source_target_pairs={{0,8},{8,16},{16,24},{24,0},{32,40},{40,48},{48,56},{56,32},{64,72... | collective-permute-start | bytes 786440 | tf_op jit(solution)/shard_map/ppermute | solution.py:368
  68.4 3.5 %collective-permute-start.20 = (bf16[1,8,32,256]{3,2,1,0:T(8,128)(2,1)S(1)}, bf16[1,8,32,256]{3,2,1,0:T(8,128)(2,1)S(1)}, u32[]{:S(2)}, u32[]{:S(2)}) collective-permute-start(bf16[1,8,32,256]{3,2,1,0:T(8,128)(2,1)S(1)} %get-tuple-element.34), channel_id=1, source_target_pairs={{0,40},{8,48},{16,56},{24,32},{32,72},{40,80},{48,88},{56,64},{64,... | collective-permute-start | bytes 393224 | tf_op jit(solution)/shard_map/ppermute | solution.py:370
  71.9 5.9 %collective-permute-start.21 = (bf16[1,8,32,256]{3,2,1,0:T(8,128)(2,1)S(1)}, bf16[1,8,32,256]{3,2,1,0:T(8,128)(2,1)S(1)}, u32[]{:S(2)}, u32[]{:S(2)}) collective-permute-start(bf16[1,8,32,256]{3,2,1,0:T(8,128)(2,1)S(1)} %get-tuple-element.35), channel_id=1, source_target_pairs={{0,48},{8,56},{16,32},{24,40},{32,80},{40,88},{48,64},{56,72},{64,... | collective-permute-start | bytes 393224 | tf_op jit(solution)/shard_map/ppermute | solution.py:370
  77.8 0.9 slice_reduce_fusion.11
  78.7 5.5 %collective-permute-done.20.refs_6_ = bf16[1,8,32,256]{3,2,1,0:T(8,128)(2,1)S(1)} collective-permute-done((bf16[1,8,32,256]{3,2,1,0:T(8,128)(2,1)S(1)}, bf16[1,8,32,256]{3,2,1,0:T(8,128)(2,1)S(1)}, u32[]{:S(2)}, u32[]{:S(2)}) %collective-permute-start.20) | collective-permute-done | bytes 131104 | tf_op jit(solution)/shard_map/ppermute | solution.py:370
  84.3 0.7 copy-done.11
  84.9 0.6 copy-done.13
  85.6 0.5 collective-permute-start.27
  86.1 0.7 copy-done.15
  86.7 0.0 collective-permute-start.28
  86.8 0.7 copy-done.9
  87.5 3.1 %collective-permute-start.16 = (bf16[2,8,32,256]{3,2,1,0:T(8,128)(2,1)}, bf16[2,8,32,256]{3,2,1,0:T(8,128)(2,1)}, u32[]{:S(2)}, u32[]{:S(2)}) collective-permute-start(bf16[2,8,32,256]{3,2,1,0:T(8,128)(2,1)} %get-tuple-element.31), channel_id=1, source_target_pairs={{0,16},{8,24},{16,0},{24,8},{32,48},{40,56},{48,32},{56,40},{64,80... | collective-permute-start | bytes 786440 | tf_op jit(solution)/shard_map/ppermute | solution.py:368
  90.5 0.2 collective-permute-start.29
  90.7 5.1 %shard_map.100.q = bf16[1024,256]{1,0:T(8,128)(2,1)} custom-call(bf16[1024,2048]{1,0:T(8,128)(2,1)} %tok.3, bf16[2048,256]{1,0:T(8,128)(2,1)} %refs_0_.3), custom_call_target="tpu_custom_call" | custom-call | flops 1000000000 | bytes 6000000 | tf_op jit(solution)/shard_map/pallas_call | solution.py:82
  95.9 2.1 %collective-permute-done.16.refs_3_ = bf16[2,8,32,256]{3,2,1,0:T(8,128)(2,1)} collective-permute-done((bf16[2,8,32,256]{3,2,1,0:T(8,128)(2,1)}, bf16[2,8,32,256]{3,2,1,0:T(8,128)(2,1)}, u32[]{:S(2)}, u32[]{:S(2)}) %collective-permute-start.16) | collective-permute-done | bytes 262176 | tf_op jit(solution)/shard_map/ppermute | solution.py:368
  98.0 1.1 collective-permute-start.17
  99.1 0.8 or_select_fusion.bias
  99.9 0.0 copy-start
  99.9 1.0 copy-done
  101.0 1.0 copy-done.8
  102.0 4.2 %early.1 = (f32[2048,128]{1,0:T(8,128)S(1)}, f32[2048,128]{1,0:T(8,128)S(1)}, f32[2048,128]{1,0:T(8,128)S(1)}) custom-call(s32[4,56]{1,0:T(4,128)S(1)} %fusion.2.want, f32[8,1024]{1,0:T(8,128)S(1)} %or_select_fusion.bias, bf16[1024,256]{1,0:T(8,128)(2,1)S(1)} %copy-done, bf16[1024,256]{1,0:T(8,128)(2,1)S(1)} %copy-done.2, ...), custom_call_target="tpu_custom_call" | custom-call | flops 900000000 | bytes 6000000 | tf_op jit(solution)/shard_map/early/pallas_call | solution.py:250
  106.2 0.4 collective-permute-done.17.refs_4_
  106.6 3.7 %late.1 = bf16[1024,256]{1,0:T(8,128)(2,1)} custom-call(s32[4,56]{1,0:T(4,128)S(1)} %fusion.2.want, f32[8,1024]{1,0:T(8,128)S(1)} %or_select_fusion.bias, bf16[1024,256]{1,0:T(8,128)(2,1)S(1)} %copy-done, f32[2048,128]{1,0:T(8,128)S(1)} %get-tuple-element.27.acc, f32[2048,128]{1,0:T(8,128)S(1)} %get-tuple-element.28.top, ...), custom_call_target="tpu_custom_call" | custom-call | flops 400000000 | bytes 6000000 | tf_op jit(solution)/shard_map/late/pallas_call | solution.py:272
  110.3 7.2 %all-to-all-start = ((bf16[8,128,256]{2,1,0:T(8,128)(2,1)}), bf16[8,128,256]{2,1,0:T(8,128)(2,1)S(1)}, u32[]{:S(2)}, u32[]{:S(2)}) async-start(bf16[8,128,256]{2,1,0:T(8,128)(2,1)} %bitcast.8), calls=%async_computation | async-start | bytes 1048576 | tf_op jit(solution)/shard_map/all_to_all | solution.py:382
  117.6 0.1 broadcast_add_fusion
  117.7 10.2 %all-to-all-done.att = bf16[8,128,256]{2,1,0:T(8,128)(2,1)S(1)} async-done(((bf16[8,128,256]{2,1,0:T(8,128)(2,1)}), bf16[8,128,256]{2,1,0:T(8,128)(2,1)S(1)}, u32[]{:S(2)}, u32[]{:S(2)}) %all-to-all-start) | async-done | bytes 524320 | tf_op jit(solution)/shard_map/all_to_all | solution.py:382
  127.9 5.2 %project.1 = bf16[128,2048]{1,0:T(8,128)(2,1)} custom-call(s32[2,4]{1,0:T(2,128)S(1)} %pad_add_fusion.1.spot, bf16[8,128,256]{2,1,0:T(8,128)(2,1)S(1)} %all-to-all-done.att, bf16[256,2048]{1,0:T(8,128)(2,1)} %refs_0_.5, bf16[256,2048]{1,0:T(8,128)(2,1)} %collective-permute-done.23.refs_1_, bf16[256,2048]{1,0:T(8,128)(2,1)S(1)} %copy-done.4, ...), custom_call_target="tpu_custom_call" | custom-call | flops 1000000000 | bytes 9000000 | tf_op jit(solution)/shard_map/project/pallas_call | solution.py:309
  (66 shorter events, 0.2 us)
Async XLA Ops:
  0.0 17.6 %copy-start.22 = (s32[56]{0:T(128)S(1)}, s32[56]{0:T(128)}, u32[]{:S(2)}) copy-start(s32[56]{0:T(128)} %constant.174) | copy-start | bytes 676
  0.0 11.2 %copy-start.19 = (s32[8,12]{1,0:T(8,128)S(1)}, s32[8,12]{1,0:T(8,128)}, u32[]{:S(2)}) copy-start(s32[8,12]{1,0:T(8,128)} %param.15) | copy-start | bytes 1156
  5.2 18.1 %collective-permute-start.3 = (bf16[1024,256]{1,0:T(8,128)(2,1)}, bf16[1024,256]{1,0:T(8,128)(2,1)S(1)}, u32[]{:S(2)}, u32[]{:S(2)}) collective-permute-start(bf16[1024,256]{1,0:T(8,128)(2,1)} %shard_map.101.refs_0_), channel_id=1, source_target_pairs={{0,32},{8,40},{16,48},{24,56},{32,64},{40,72},{48,80},{56,88},{64,... | collective-permute-start | bytes 1572872 | tf_op jit(solution)/shard_map/ppermute | solution.py:360
  7.2 16.1 %collective-permute-start.4 = (bf16[1024,256]{1,0:T(8,128)(2,1)}, bf16[1024,256]{1,0:T(8,128)(2,1)S(1)}, u32[]{:S(2)}, u32[]{:S(2)}) collective-permute-start(bf16[1024,256]{1,0:T(8,128)(2,1)} %shard_map.101.refs_0_), channel_id=1, source_target_pairs={{0,224},{8,232},{16,240},{24,248},{32,0},{40,8},{48,16},{56,24},{6... | collective-permute-start | bytes 1572872 | tf_op jit(solution)/shard_map/ppermute | solution.py:361
  11.2 4.8 %collective-permute-start = (s32[8,12]{1,0:T(8,128)S(1)}, s32[8,12]{1,0:T(8,128)S(1)}, u32[]{:S(2)}, u32[]{:S(2)}) collective-permute-start(s32[8,12]{1,0:T(8,128)S(1)} %copy-done.19), channel_id=1, source_target_pairs={{0,24},{8,0},{16,8},{24,16},{32,56},{40,32},{48,40},{56,48},{64,88... | collective-permute-start | bytes 1160 | tf_op jit(solution)/shard_map/ppermute | solution.py:335
  11.8 5.8 %collective-permute-start.1 = (s32[8,12]{1,0:T(8,128)S(1)}, s32[8,12]{1,0:T(8,128)S(1)}, u32[]{:S(2)}, u32[]{:S(2)}) collective-permute-start(s32[8,12]{1,0:T(8,128)S(1)} %copy-done.19), channel_id=1, source_target_pairs={{0,16},{8,24},{16,0},{24,8},{32,48},{40,56},{48,32},{56,40},{64,80... | collective-permute-start | bytes 1160 | tf_op jit(solution)/shard_map/ppermute | solution.py:335
  14.2 3.6 %collective-permute-start.2 = (s32[8,12]{1,0:T(8,128)S(1)}, s32[8,12]{1,0:T(8,128)S(1)}, u32[]{:S(2)}, u32[]{:S(2)}) collective-permute-start(s32[8,12]{1,0:T(8,128)S(1)} %copy-done.19), channel_id=1, source_target_pairs={{0,8},{8,16},{16,24},{24,0},{32,40},{40,48},{48,56},{56,32},{64,72... | collective-permute-start | bytes 1160 | tf_op jit(solution)/shard_map/ppermute | solution.py:335
  16.0 27.4 %collective-permute-start.23 = (bf16[256,2048]{1,0:T(8,128)(2,1)}, bf16[256,2048]{1,0:T(8,128)(2,1)}, u32[]{:S(2)}, u32[]{:S(2)}) collective-permute-start(bf16[256,2048]{1,0:T(8,128)(2,1)} %refs_0_.5), channel_id=1, source_target_pairs={{0,2},{1,3},{2,4},{3,5},{4,6},{5,7},{6,0},{7,1},{8,10},{9,11},{10,... | collective-permute-start | bytes 3145736 | tf_op jit(solution)/shard_map/ppermute | solution.py:372
  23.3 1.0 copy-start.1
  25.1 12.8 %collective-permute-start.7 = (bf16[3,8,32,256]{3,2,1,0:T(8,128)(2,1)S(1)}, bf16[3,8,32,256]{3,2,1,0:T(8,128)(2,1)S(1)}, u32[]{:S(2)}, u32[]{:S(2)}) collective-permute-start(bf16[3,8,32,256]{3,2,1,0:T(8,128)(2,1)S(1)} %get-tuple-element.21), channel_id=1, source_target_pairs={{0,8},{8,16},{16,24},{24,0},{32,40},{40,48},{48,56},{56,32},{64,72... | collective-permute-start | bytes 1179656 | tf_op jit(solution)/shard_map/ppermute | solution.py:368
  26.6 31.7 %collective-permute-start.24 = (bf16[256,2048]{1,0:T(8,128)(2,1)}, bf16[256,2048]{1,0:T(8,128)(2,1)S(1)}, u32[]{:S(2)}, u32[]{:S(2)}) collective-permute-start(bf16[256,2048]{1,0:T(8,128)(2,1)} %refs_0_.5), channel_id=1, source_target_pairs={{0,6},{1,7},{2,0},{3,1},{4,2},{5,3},{6,4},{7,5},{8,14},{9,15},{10,... | collective-permute-start | bytes 3145736 | tf_op jit(solution)/shard_map/ppermute | solution.py:373
  29.7 13.7 %collective-permute-start.5 = (bf16[1024,256]{1,0:T(8,128)(2,1)S(1)}, bf16[1024,256]{1,0:T(8,128)(2,1)S(1)}, u32[]{:S(2)}, u32[]{:S(2)}) collective-permute-start(bf16[1024,256]{1,0:T(8,128)(2,1)S(1)} %collective-permute-done.3.refs_1_), channel_id=1, source_target_pairs={{0,32},{8,40},{16,48},{24,56},{32,64},{40,72},{48,80},{56,88},{64,... | collective-permute-start | bytes 1572872 | tf_op jit(solution)/shard_map/ppermute | solution.py:360
  29.7 4.7 %collective-permute-start.18 = (s32[4,8,12]{2,1,0:T(8,128)S(1)}, s32[4,8,12]{2,1,0:T(8,128)S(1)}, u32[]{:S(2)}, u32[]{:S(2)}) collective-permute-start(s32[4,8,12]{2,1,0:T(8,128)S(1)} %pad_add_fusion), channel_id=1, source_target_pairs={{0,224},{8,232},{16,240},{24,248},{32,0},{40,8},{48,16},{56,24},{6... | collective-permute-start | bytes 4616 | tf_op jit(solution)/shard_map/ppermute | solution.py:336
  34.3 3.5 %copy-start.18 = (s32[4,8,12]{2,1,0:T(8,128)}, s32[4,8,12]{2,1,0:T(8,128)S(1)}, u32[]{:S(2)}) copy-start(s32[4,8,12]{2,1,0:T(8,128)S(1)} %collective-permute-done.18) | copy-start | bytes 4612
  34.3 14.9 %collective-permute-start.6 = (bf16[1024,256]{1,0:T(8,128)(2,1)S(1)}, bf16[1024,256]{1,0:T(8,128)(2,1)S(1)}, u32[]{:S(2)}, u32[]{:S(2)}) collective-permute-start(bf16[1024,256]{1,0:T(8,128)(2,1)S(1)} %collective-permute-done.4.refs_2_), channel_id=1, source_target_pairs={{0,224},{8,232},{16,240},{24,248},{32,0},{40,8},{48,16},{56,24},{6... | collective-permute-start | bytes 1572872 | tf_op jit(solution)/shard_map/ppermute | solution.py:361
  37.8 9.9 %collective-permute-start.8 = (bf16[3,8,32,256]{3,2,1,0:T(8,128)(2,1)S(1)}, bf16[3,8,32,256]{3,2,1,0:T(8,128)(2,1)S(1)}, u32[]{:S(2)}, u32[]{:S(2)}) collective-permute-start(bf16[3,8,32,256]{3,2,1,0:T(8,128)(2,1)S(1)} %get-tuple-element.22), channel_id=1, source_target_pairs={{0,16},{8,24},{16,0},{24,8},{32,48},{40,56},{48,32},{56,40},{64,80... | collective-permute-start | bytes 1179656 | tf_op jit(solution)/shard_map/ppermute | solution.py:368
  43.4 16.4 %collective-permute-start.13 = (bf16[1024,256]{1,0:T(8,128)(2,1)S(1)}, bf16[1024,256]{1,0:T(8,128)(2,1)S(1)}, u32[]{:S(2)}, u32[]{:S(2)}) collective-permute-start(bf16[1024,256]{1,0:T(8,128)(2,1)S(1)} %collective-permute-done.5.refs_0_.refs_3_), channel_id=1, source_target_pairs={{0,32},{8,40},{16,48},{24,56},{32,64},{40,72},{48,80},{56,88},{64,... | collective-permute-start | bytes 1572872 | tf_op jit(solution)/shard_map/ppermute | solution.py:360
  43.4 47.1 %collective-permute-start.25 = (bf16[256,2048]{1,0:T(8,128)(2,1)}, bf16[256,2048]{1,0:T(8,128)(2,1)}, u32[]{:S(2)}, u32[]{:S(2)}) collective-permute-start(bf16[256,2048]{1,0:T(8,128)(2,1)} %collective-permute-done.23.refs_1_), channel_id=1, source_target_pairs={{0,2},{1,3},{2,4},{3,5},{4,6},{5,7},{6,0},{7,1},{8,10},{9,11},{10,... | collective-permute-start | bytes 3145736 | tf_op jit(solution)/shard_map/ppermute | solution.py:374
  47.8 0.8 copy-start.5
  48.5 47.3 %copy-start.20 = (s32[1024]{0:T(1024)S(1)}, s32[1024]{0:T(1024)}, u32[]{:S(2)}) copy-start(s32[1024]{0:T(1024)} %constant.175) | copy-start | bytes 12292
  48.5 47.4 %copy-start.21 = (s32[1024]{0:T(1024)S(1)}, s32[1024]{0:T(1024)}, u32[]{:S(2)}) copy-start(s32[1024]{0:T(1024)} %constant.176) | copy-start | bytes 12292
  48.6 51.4 %copy-start.2 = (bf16[1024,256]{1,0:T(8,128)(2,1)S(1)}, bf16[1024,256]{1,0:T(8,128)(2,1)}, u32[]{:S(2)}) copy-start(bf16[1024,256]{1,0:T(8,128)(2,1)} %shard_map.101.refs_0_) | copy-start | bytes 1572868
  48.6 7.8 %collective-permute-start.9 = (bf16[3,8,32,256]{3,2,1,0:T(8,128)(2,1)S(1)}, bf16[3,8,32,256]{3,2,1,0:T(8,128)(2,1)S(1)}, u32[]{:S(2)}, u32[]{:S(2)}) collective-permute-start(bf16[3,8,32,256]{3,2,1,0:T(8,128)(2,1)S(1)} %get-tuple-element.23), channel_id=1, source_target_pairs={{0,24},{8,0},{16,8},{24,16},{32,56},{40,32},{48,40},{56,48},{64,88... | collective-permute-start | bytes 1179656 | tf_op jit(solution)/shard_map/ppermute | solution.py:368
  49.2 14.4 %collective-permute-start.14 = (bf16[1024,256]{1,0:T(8,128)(2,1)S(1)}, bf16[1024,256]{1,0:T(8,128)(2,1)}, u32[]{:S(2)}, u32[]{:S(2)}) collective-permute-start(bf16[1024,256]{1,0:T(8,128)(2,1)S(1)} %collective-permute-done.6.refs_1_.refs_4_), channel_id=1, source_target_pairs={{0,224},{8,232},{16,240},{24,248},{32,0},{40,8},{48,16},{56,24},{6... | collective-permute-start | bytes 1572872 | tf_op jit(solution)/shard_map/ppermute | solution.py:361
  56.3 0.8 copy-start.7
  57.1 9.2 %collective-permute-start.10 = (bf16[2,8,32,256]{3,2,1,0:T(8,128)(2,1)}, bf16[2,8,32,256]{3,2,1,0:T(8,128)(2,1)}, u32[]{:S(2)}, u32[]{:S(2)}) collective-permute-start(bf16[2,8,32,256]{3,2,1,0:T(8,128)(2,1)} %get-tuple-element.24), channel_id=1, source_target_pairs={{0,8},{8,16},{16,24},{24,0},{32,40},{40,48},{48,56},{56,32},{64,72... | collective-permute-start | bytes 786440 | tf_op jit(solution)/shard_map/ppermute | solution.py:368
  58.3 1.5 %copy-start.3 = (bf16[256,2048]{1,0:T(8,128)(2,1)}, bf16[256,2048]{1,0:T(8,128)(2,1)S(1)}, u32[]{:S(2)}) copy-start(bf16[256,2048]{1,0:T(8,128)(2,1)S(1)} %collective-permute-done.24.refs_2_) | copy-start | bytes 3145732
  58.3 10.1 %collective-permute-start.11 = (bf16[2,8,32,256]{3,2,1,0:T(8,128)(2,1)}, bf16[2,8,32,256]{3,2,1,0:T(8,128)(2,1)}, u32[]{:S(2)}, u32[]{:S(2)}) collective-permute-start(bf16[2,8,32,256]{3,2,1,0:T(8,128)(2,1)} %get-tuple-element.25), channel_id=1, source_target_pairs={{0,16},{8,24},{16,0},{24,8},{32,48},{40,56},{48,32},{56,40},{64,80... | collective-permute-start | bytes 786440 | tf_op jit(solution)/shard_map/ppermute | solution.py:368
  59.8 12.1 %collective-permute-start.12 = (bf16[2,8,32,256]{3,2,1,0:T(8,128)(2,1)}, bf16[2,8,32,256]{3,2,1,0:T(8,128)(2,1)}, u32[]{:S(2)}, u32[]{:S(2)}) collective-permute-start(bf16[2,8,32,256]{3,2,1,0:T(8,128)(2,1)} %get-tuple-element.26), channel_id=1, source_target_pairs={{0,24},{8,0},{16,8},{24,16},{32,56},{40,32},{48,40},{56,48},{64,88... | collective-permute-start | bytes 786440 | tf_op jit(solution)/shard_map/ppermute | solution.py:368
  62.1 37.9 %copy-start.6 = (bf16[3,8,32,256]{3,2,1,0:T(8,128)(2,1)S(1)}, bf16[3,8,32,256]{3,2,1,0:T(8,128)(2,1)}, u32[]{:S(2)}) copy-start(bf16[3,8,32,256]{3,2,1,0:T(8,128)(2,1)} %copy-done.5) | copy-start | bytes 1179652
  63.7 14.2 %collective-permute-start.19 = (bf16[1,8,32,256]{3,2,1,0:T(8,128)(2,1)S(1)}, bf16[1,8,32,256]{3,2,1,0:T(8,128)(2,1)S(1)}, u32[]{:S(2)}, u32[]{:S(2)}) collective-permute-start(bf16[1,8,32,256]{3,2,1,0:T(8,128)(2,1)S(1)} %get-tuple-element.33), channel_id=1, source_target_pairs={{0,32},{8,40},{16,48},{24,56},{32,64},{40,72},{48,80},{56,88},{64,... | collective-permute-start | bytes 393224 | tf_op jit(solution)/shard_map/ppermute | solution.py:370
  65.6 0.7 copy-start.17
  66.3 20.4 %collective-permute-start.15 = (bf16[2,8,32,256]{3,2,1,0:T(8,128)(2,1)S(1)}, bf16[2,8,32,256]{3,2,1,0:T(8,128)(2,1)S(1)}, u32[]{:S(2)}, u32[]{:S(2)}) collective-permute-start(bf16[2,8,32,256]{3,2,1,0:T(8,128)(2,1)S(1)} %get-tuple-element.30), channel_id=1, source_target_pairs={{0,8},{8,16},{16,24},{24,0},{32,40},{40,48},{48,56},{56,32},{64,72... | collective-permute-start | bytes 786440 | tf_op jit(solution)/shard_map/ppermute | solution.py:368
  68.4 15.9 %collective-permute-start.20 = (bf16[1,8,32,256]{3,2,1,0:T(8,128)(2,1)S(1)}, bf16[1,8,32,256]{3,2,1,0:T(8,128)(2,1)S(1)}, u32[]{:S(2)}, u32[]{:S(2)}) collective-permute-start(bf16[1,8,32,256]{3,2,1,0:T(8,128)(2,1)S(1)} %get-tuple-element.34), channel_id=1, source_target_pairs={{0,40},{8,48},{16,56},{24,32},{32,72},{40,80},{48,88},{56,64},{64,... | collective-permute-start | bytes 393224 | tf_op jit(solution)/shard_map/ppermute | solution.py:370
  71.9 13.0 %collective-permute-start.21 = (bf16[1,8,32,256]{3,2,1,0:T(8,128)(2,1)S(1)}, bf16[1,8,32,256]{3,2,1,0:T(8,128)(2,1)S(1)}, u32[]{:S(2)}, u32[]{:S(2)}) collective-permute-start(bf16[1,8,32,256]{3,2,1,0:T(8,128)(2,1)S(1)} %get-tuple-element.35), channel_id=1, source_target_pairs={{0,48},{8,56},{16,32},{24,40},{32,80},{40,88},{48,64},{56,72},{64,... | collective-permute-start | bytes 393224 | tf_op jit(solution)/shard_map/ppermute | solution.py:370
  77.8 8.3 %collective-permute-start.22 = (bf16[1,8,32,256]{3,2,1,0:T(8,128)(2,1)S(1)}, bf16[1,8,32,256]{3,2,1,0:T(8,128)(2,1)S(1)}, u32[]{:S(2)}, u32[]{:S(2)}) collective-permute-start(bf16[1,8,32,256]{3,2,1,0:T(8,128)(2,1)S(1)} %get-tuple-element.36), channel_id=1, source_target_pairs={{0,56},{8,32},{16,40},{24,48},{32,88},{40,64},{48,72},{56,80},{64,... | collective-permute-start | bytes 393224 | tf_op jit(solution)/shard_map/ppermute | solution.py:370
  84.3 0.7 copy-start.11
  84.9 32.7 %collective-permute-start.26 = (bf16[256,2048]{1,0:T(8,128)(2,1)}, bf16[256,2048]{1,0:T(8,128)(2,1)}, u32[]{:S(2)}, u32[]{:S(2)}) collective-permute-start(bf16[256,2048]{1,0:T(8,128)(2,1)} %refs_0_.5), channel_id=1, source_target_pairs={{0,1},{1,0},{2,3},{3,2},{4,5},{5,4},{6,7},{7,6},{8,9},{9,8},{10,11... | collective-permute-start | bytes 3145736 | tf_op jit(solution)/shard_map/ppermute | solution.py:375
  84.9 0.7 copy-start.13
  85.6 32.1 %collective-permute-start.27 = (bf16[256,2048]{1,0:T(8,128)(2,1)}, bf16[256,2048]{1,0:T(8,128)(2,1)}, u32[]{:S(2)}, u32[]{:S(2)}) collective-permute-start(bf16[256,2048]{1,0:T(8,128)(2,1)} %collective-permute-done.23.refs_1_), channel_id=1, source_target_pairs={{0,1},{1,0},{2,3},{3,2},{4,5},{5,4},{6,7},{7,6},{8,9},{9,8},{10,11... | collective-permute-start | bytes 3145736 | tf_op jit(solution)/shard_map/ppermute | solution.py:375
  86.1 0.7 copy-start.15
  86.7 30.9 %collective-permute-start.28 = (bf16[256,2048]{1,0:T(8,128)(2,1)}, bf16[256,2048]{1,0:T(8,128)(2,1)}, u32[]{:S(2)}, u32[]{:S(2)}) collective-permute-start(bf16[256,2048]{1,0:T(8,128)(2,1)} %copy-done.3), channel_id=1, source_target_pairs={{0,1},{1,0},{2,3},{3,2},{4,5},{5,4},{6,7},{7,6},{8,9},{9,8},{10,11... | collective-permute-start | bytes 3145736 | tf_op jit(solution)/shard_map/ppermute | solution.py:375
  86.8 0.7 copy-start.9
  87.5 10.5 %collective-permute-start.16 = (bf16[2,8,32,256]{3,2,1,0:T(8,128)(2,1)}, bf16[2,8,32,256]{3,2,1,0:T(8,128)(2,1)}, u32[]{:S(2)}, u32[]{:S(2)}) collective-permute-start(bf16[2,8,32,256]{3,2,1,0:T(8,128)(2,1)} %get-tuple-element.31), channel_id=1, source_target_pairs={{0,16},{8,24},{16,0},{24,8},{32,48},{40,56},{48,32},{56,40},{64,80... | collective-permute-start | bytes 786440 | tf_op jit(solution)/shard_map/ppermute | solution.py:368
  90.5 37.4 %collective-permute-start.29 = (bf16[256,2048]{1,0:T(8,128)(2,1)}, bf16[256,2048]{1,0:T(8,128)(2,1)}, u32[]{:S(2)}, u32[]{:S(2)}) collective-permute-start(bf16[256,2048]{1,0:T(8,128)(2,1)} %collective-permute-done.25.refs_3_), channel_id=1, source_target_pairs={{0,1},{1,0},{2,3},{3,2},{4,5},{5,4},{6,7},{7,6},{8,9},{9,8},{10,11... | collective-permute-start | bytes 3145736 | tf_op jit(solution)/shard_map/ppermute | solution.py:375
  98.0 8.6 %collective-permute-start.17 = (bf16[2,8,32,256]{3,2,1,0:T(8,128)(2,1)}, bf16[2,8,32,256]{3,2,1,0:T(8,128)(2,1)S(1)}, u32[]{:S(2)}, u32[]{:S(2)}) collective-permute-start(bf16[2,8,32,256]{3,2,1,0:T(8,128)(2,1)} %copy-done.17), channel_id=1, source_target_pairs={{0,24},{8,0},{16,8},{24,16},{32,56},{40,32},{48,40},{56,48},{64,88... | collective-permute-start | bytes 786440 | tf_op jit(solution)/shard_map/ppermute | solution.py:368
  99.9 1.0 copy-start
  101.0 1.0 copy-start.8
  102.0 4.6 %copy-start.10 = (bf16[2,8,32,256]{3,2,1,0:T(8,128)(2,1)S(1)}, bf16[2,8,32,256]{3,2,1,0:T(8,128)(2,1)}, u32[]{:S(2)}) copy-start(bf16[2,8,32,256]{3,2,1,0:T(8,128)(2,1)} %copy-done.9) | copy-start | bytes 786436
  102.0 4.6 %copy-start.12 = (bf16[1,8,32,256]{3,2,1,0:T(8,128)(2,1)S(1)}, bf16[1,8,32,256]{3,2,1,0:T(8,128)(2,1)}, u32[]{:S(2)}) copy-start(bf16[1,8,32,256]{3,2,1,0:T(8,128)(2,1)} %copy-done.11) | copy-start | bytes 393220
  102.0 4.6 %copy-start.14 = (bf16[1,8,32,256]{3,2,1,0:T(8,128)(2,1)S(1)}, bf16[1,8,32,256]{3,2,1,0:T(8,128)(2,1)}, u32[]{:S(2)}) copy-start(bf16[1,8,32,256]{3,2,1,0:T(8,128)(2,1)} %copy-done.13) | copy-start | bytes 393220
  102.0 4.6 %copy-start.16 = (bf16[1,8,32,256]{3,2,1,0:T(8,128)(2,1)S(1)}, bf16[1,8,32,256]{3,2,1,0:T(8,128)(2,1)}, u32[]{:S(2)}) copy-start(bf16[1,8,32,256]{3,2,1,0:T(8,128)(2,1)} %copy-done.15) | copy-start | bytes 393220
  106.2 21.7 %copy-start.4 = (bf16[256,2048]{1,0:T(8,128)(2,1)S(1)}, bf16[256,2048]{1,0:T(8,128)(2,1)}, u32[]{:S(2)}) copy-start(bf16[256,2048]{1,0:T(8,128)(2,1)} %copy-done.3) | copy-start | bytes 3145732
  110.3 17.6 %all-to-all-start = ((bf16[8,128,256]{2,1,0:T(8,128)(2,1)}), bf16[8,128,256]{2,1,0:T(8,128)(2,1)S(1)}, u32[]{:S(2)}, u32[]{:S(2)}) async-start(bf16[8,128,256]{2,1,0:T(8,128)(2,1)} %bitcast.8), calls=%async_computation | async-start | bytes 1048576 | tf_op jit(solution)/shard_map/all_to_all | solution.py:382

commit v3 on v2

--- a/solution.py
+++ b/solution.py
@@ -28,10 +28,6 @@
 
 def along_x(k):
     return [(z * NX + x, z * NX + (x + k) % NX) for z in range(NZ) for x in range(NX)]
-
-
-def across(r):
-    return [(z * NX + x, (z + 1) % NZ * NX + (x + r) % NX) for z in range(NZ) for x in range(NX)]
 
 
 def along_y(k):
@@ -126,7 +122,7 @@
     )(want, *held)
 
 
-def gather_blocks(kv, want, held, recv, counts, first, last, j):
+def gather_blocks(kv, want, held, recv, counts, first, j):
     slot = 0
     source = 0
 
@@ -142,8 +138,6 @@
             for r in range(1, NX):
                 put(recv[(NX - 1) * b + r - 1][d, j])
             source += 1
-    for r in range(last):
-        put(recv[(NX - 1) * len(counts) + r][0, j])
 
 
 def both_heads(q, at):
@@ -179,7 +173,7 @@
             spots = [places(g, n) for n in range(GROUP)]
             own, oth, m = [], [], []
             for n, (j, at, to) in enumerate(spots):
-                gather_blocks(kv.at[n], want, held, recv, counts, 0, 0, j)
+                gather_blocks(kv.at[n], want, held, recv, counts, 0, j)
             for n, (j, at, to) in enumerate(spots):
                 qq = both_heads(q, at)
                 mine = held[0][pl.ds(at, QB), :HEAD]
@@ -206,7 +200,7 @@
     return body
 
 
-def late_body(counts, first, last):
+def late_body(counts, first):
     total = sum(counts)
 
     def body(want, bias, q, acc, top, low, *refs):
@@ -220,7 +214,7 @@
             spots = [places(g, n) for n in range(GROUP)]
             oth, m, keep, inv = [], [], [], []
             for n, (j, at, to) in enumerate(spots):
-                gather_blocks(kv.at[n], want, held, recv, counts, first, last, j)
+                gather_blocks(kv.at[n], want, held, recv, counts, first, j)
             for n, (j, at, to) in enumerate(spots):
                 part = lax.dot_general(both_heads(q, at), kv[n, :, :HEAD], NT, preferred_element_type=F32)
                 oth.append(part * scale + bias[pl.ds(j, 1), begin : begin + far])
@@ -265,16 +259,16 @@
     )(want, bias, q, *ins)
 
 
-def attend_late(want, bias, q, sums, held, recv, last):
+def attend_late(want, bias, q, sums, held, recv):
     counts = [r[0].shape[0] for r in recv]
-    first = bias.shape[1] // (NX * KB) - sum(counts) - 1
-    ins = [*held, *[a for r in recv for a in r], *last]
-    return pl.pallas_call(
-        late_body(counts, first, len(last)),
+    first = bias.shape[1] // (NX * KB) - sum(counts)
+    ins = [*held, *[a for r in recv for a in r]]
+    return pl.pallas_call(
+        late_body(counts, first),
         out_shape=jax.ShapeDtypeStruct(q.shape, BF),
         in_specs=[SMEM] + [VMEM] * (2 + len(sums) + len(ins)),
         out_specs=VMEM,
-        scratch_shapes=[pltpu.VMEM((GROUP, (sum(counts) + 1) * NX * KB, 2 * HEAD), BF)],
+        scratch_shapes=[pltpu.VMEM((GROUP, sum(counts) * NX * KB, 2 * HEAD), BF)],
         compiler_params=params(16),
         cost_estimate=pl.CostEstimate(
             flops=400_000_000, bytes_accessed=6_000_000, transcendentals=800_000
@@ -333,7 +327,6 @@
     kv = rows_project(tokens, (wk, wv), 60)
 
     row = jnp.stack([chosen] + [lax.ppermute(chosen, "kv", along_x(-r)) for r in range(1, NX)])
-    above = lax.ppermute(row, "kv", along_z(-1))
 
     order = [0, *[d for s in range(1, NZ // 2) for d in (s, NZ - s)], NZ // 2]
 
@@ -343,8 +336,7 @@
         mine = named // per == groups[None, :, None]
         return jnp.sum(jnp.where(mine, named % per, 0), axis=2)
 
-    want = wants(row, order[:-1])
-    want_above = wants(above, [NZ // 2 - 1])
+    want = wants(row, order)
     dist = np.repeat(np.array(order, np.int32), NX * KB)
     beyond = np.tile(np.repeat(np.arange(NX, dtype=np.int32), KB), NZ)
     source = (z - dist) % NZ * NX + (x - beyond) % NX
@@ -356,29 +348,27 @@
 
     held = {0: kv}
     up = down = kv
-    for step in range(1, NZ // 2):
+    for step in range(1, NZ // 2 + 1):
         up = held[step] = lax.ppermute(up, "kv", along_z(1))
-        down = held[NZ - step] = lax.ppermute(down, "kv", along_z(-1))
+        if step < NZ // 2:
+            down = held[NZ - step] = lax.ppermute(down, "kv", along_z(-1))
 
     recv = []
-    batches = [[0, 1, NZ - 1]] + [[s, NZ - s] for s in range(2, NZ // 2)]
+    batches = [[0, 1, NZ - 1]] + [[s, NZ - s] for s in range(2, NZ // 2)] + [[NZ // 2]]
     beside = range(1, NX)
     for batch in batches:
         sent = pick(want, order.index(batch[0]), [held[d] for d in batch], beside)
         recv.append([lax.ppermute(a, "kv", along_x(r)) for a, r in zip(sent, beside)])
-    sent = pick(want_above, 0, [held[NZ // 2 - 1]], range(NX))
-    last = [lax.ppermute(a, "kv", across(r)) for r, a in enumerate(sent)]
-
     wm = lax.ppermute(wo, "tp", along_y(1))
     wp = lax.ppermute(wo, "tp", along_y(-1))
     weights = [wo, wm, wp, lax.ppermute(wm, "tp", along_y(1))]
     weights += [lax.ppermute(w, "tp", CORES) for w in weights]
 
     q = rows_project(tokens, (wq,), 60)
-    line = [held[d] for d in order[:-1]]
-    cut = len(line) - len(batches[-1])
-    sums = attend_early(want, bias, q, line[:cut], recv[:-1])
-    mixed = attend_late(want, bias, q, sums, line[cut:], recv[-1:], last)
+    line = [held[d] for d in order]
+    cut = len(batches[0]) + len(batches[1])
+    sums = attend_early(want, bias, q, line[:cut], recv[:2])
+    mixed = attend_late(want, bias, q, sums, line[cut:], recv[2:])
     att = lax.all_to_all(mixed.reshape(2 * NY, QB, -1), "tp", 0, 0, tiled=True)
     y, c = tp // 2, tp % 2
     rows = jnp.stack([y, (y - 1) % NY, (y + 1) % NY, (y + 2) % NY]) * 2

time: 134 us -> 138 us (1.030)
  waiting for transfers between devices: 36.8 us -> 45.7 us
  starting transfers between devices: 56.6 us -> 50 us
  local copies, waits for them, and re-layouts: 9.21 us -> 14.9 us
  Pallas kernels: 28.3 us -> 26 us
  other arithmetic: 1.93 us -> 0.32 us
    ppermute x9 -> x12, waiting for transfers between devices: 9.89 us -> 25 us  [layer(): lax.ppermute(a, 'kv', along_x(r))]
    ppermute x5 -> x0, starting transfers between devices: 12.7 us -> none  [the longest x4 9.51 us: layer(): last = [lax.ppermute(a, 'kv', across(r)) for r, a in enumerate(sent)]]
    ppermute x9 -> x12, starting transfers between devices: 14.5 us -> 21.6 us  [layer(): lax.ppermute(a, 'kv', along_x(r))]
    ppermute x5 -> x0, waiting for transfers between devices: 6.97 us -> none  [the longest x4 5.53 us: layer(): last = [lax.ppermute(a, 'kv', across(r)) for r, a in enumerate(sent)]]
    unnamed x46 -> x58, local copies, waits for them, and re-layouts: 8.03 us -> 14.2 us
    all_to_all x1, starting transfers between devices: 7.24 us -> 4.19 us  [layer(): att = lax.all_to_all(mixed.reshape(2 * NY, QB, -1), 'tp', 0, 0, tiled=True)]
    ppermute x1, starting transfers between devices: 0.01 us -> 1.47 us  [layer(): weights = [wo, wm, wp, lax.ppermute(wm, 'tp', along_y(1))]]
    pallas_call x4, Pallas kernels: 4.82 us -> 3.41 us  [pick(): pl.pallas_call(pick_body(first, count, offsets), out_shape=[jax.ShapeDtyp...]
  transfers between devices with their start and end apart: 31 -> 30, of which waited for: 10 -> 10; matrix products, arithmetic and copies ran while one was open for 2% -> 1% of each run, Pallas kernels for 13% -> 11%
where the time goes in v3:
time: 138 us; the launch traced here: 137 us
  starting transfers between devices  50 us (36%)
  waiting for transfers between devices  45.7 us (33%)
  Pallas kernels  26 us (19%)
  local copies, waits for them, and re-layouts  14.9 us (11%)
    ppermute x12, waiting for transfers between devices, layer(): lax.ppermute(a, 'kv', along_x(r))  25 us
    ppermute x12, starting transfers between devices, layer(): lax.ppermute(a, 'kv', along_x(r))  21.6 us
    unnamed x58, local copies, waits for them, and re-layouts  14.2 us
    ppermute x3, starting transfers between devices, layer(): down = held[NZ - step] = lax.ppermute(down, 'kv', along_z(-1))  10.8 us
    ppermute x4, waiting for transfers between devices, layer(): up = held[step] = lax.ppermute(up, 'kv', along_z(1))  10.4 us
    pallas_call x2, Pallas kernels, rows_project(): pl.pallas_call(rows_body(len(weights), parts), out_shape=jax.ShapeDtypeSt...  10.3 us
    all_to_all x1, waiting for transfers between devices, layer(): att = lax.all_to_all(mixed.reshape(2 * NY, QB, -1), 'tp', 0, 0, tiled=True)  10.2 us
    pallas_call x1, Pallas kernels, project(): pl.pallas_call(project_body, out_shape=jax.ShapeDtypeStruct((QB, width),...  5.21 us
  transfers between devices with their start and end apart: 30, of which 10 were waited for; matrix products, arithmetic and copies ran while one was open for 1% of the time, Pallas kernels for 11%

profile of v3, /device:TPU:2, one launch (start us, length us, event | category | flops | bytes accessed | tf_op | source)
XLA Modules:
  0.0 137.3 jit_solution(11017587162996163224)
XLA Ops:
  0.0 5.2 %shard_map.92.refs_0_ = bf16[1024,256]{1,0:T(8,128)(2,1)} custom-call(bf16[1024,2048]{1,0:T(8,128)(2,1)} %tok.3, bf16[2048,128]{1,0:T(8,128)(2,1)} %refs_0_.4, bf16[2048,128]{1,0:T(8,128)(2,1)} %refs_1_.1), custom_call_target="tpu_custom_call" | custom-call | flops 1000000000 | bytes 6000000 | tf_op jit(solution)/shard_map/pallas_call | solution.py:78
  5.2 2.0 %collective-permute-start.3 = (bf16[1024,256]{1,0:T(8,128)(2,1)}, bf16[1024,256]{1,0:T(8,128)(2,1)S(1)}, u32[]{:S(2)}, u32[]{:S(2)}) collective-permute-start(bf16[1024,256]{1,0:T(8,128)(2,1)} %shard_map.92.refs_0_), channel_id=1, source_target_pairs={{0,32},{8,40},{16,48},{24,56},{32,64},{40,72},{48,80},{56,88},{64,... | collective-permute-start | bytes 1572872 | tf_op jit(solution)/shard_map/ppermute | solution.py:352
  7.2 4.0 %collective-permute-start.4 = (bf16[1024,256]{1,0:T(8,128)(2,1)}, bf16[1024,256]{1,0:T(8,128)(2,1)S(1)}, u32[]{:S(2)}, u32[]{:S(2)}) collective-permute-start(bf16[1024,256]{1,0:T(8,128)(2,1)} %shard_map.92.refs_0_), channel_id=1, source_target_pairs={{0,224},{8,232},{16,240},{24,248},{32,0},{40,8},{48,16},{56,24},{6... | collective-permute-start | bytes 1572872 | tf_op jit(solution)/shard_map/ppermute | solution.py:354
  11.2 0.5 collective-permute-start
  11.8 2.4 %collective-permute-start.1 = (s32[8,12]{1,0:T(8,128)S(1)}, s32[8,12]{1,0:T(8,128)S(1)}, u32[]{:S(2)}, u32[]{:S(2)}) collective-permute-start(s32[8,12]{1,0:T(8,128)S(1)} %copy-done.25), channel_id=1, source_target_pairs={{0,16},{8,24},{16,0},{24,8},{32,48},{40,56},{48,32},{56,40},{64,80... | collective-permute-start | bytes 1160 | tf_op jit(solution)/shard_map/ppermute | solution.py:329
  14.2 1.8 %collective-permute-start.2 = (s32[8,12]{1,0:T(8,128)S(1)}, s32[8,12]{1,0:T(8,128)S(1)}, u32[]{:S(2)}, u32[]{:S(2)}) collective-permute-start(s32[8,12]{1,0:T(8,128)S(1)} %copy-done.25), channel_id=1, source_target_pairs={{0,8},{8,16},{16,24},{24,0},{32,40},{40,48},{48,56},{56,32},{64,72... | collective-permute-start | bytes 1160 | tf_op jit(solution)/shard_map/ppermute | solution.py:329
  16.0 1.6 %collective-permute-start.22 = (bf16[256,2048]{1,0:T(8,128)(2,1)}, bf16[256,2048]{1,0:T(8,128)(2,1)}, u32[]{:S(2)}, u32[]{:S(2)}) collective-permute-start(bf16[256,2048]{1,0:T(8,128)(2,1)} %refs_0_.5), channel_id=1, source_target_pairs={{0,2},{1,3},{2,4},{3,5},{4,6},{5,7},{6,0},{7,1},{8,10},{9,11},{10,... | collective-permute-start | bytes 3145736 | tf_op jit(solution)/shard_map/ppermute | solution.py:362
  17.6 5.7 %collective-permute-done.3.refs_1_ = bf16[1024,256]{1,0:T(8,128)(2,1)S(1)} collective-permute-done((bf16[1024,256]{1,0:T(8,128)(2,1)}, bf16[1024,256]{1,0:T(8,128)(2,1)S(1)}, u32[]{:S(2)}, u32[]{:S(2)}) %collective-permute-start.3) | collective-permute-done | bytes 524320 | tf_op jit(solution)/shard_map/ppermute | solution.py:352
  23.3 0.1 copy.10
  23.4 0.2 concatenate.14
  23.7 1.0 copy-done.1
  24.7 0.7 shard_map.93
  25.5 1.6 %collective-permute-start.7 = (bf16[3,8,32,256]{3,2,1,0:T(8,128)(2,1)S(1)}, bf16[3,8,32,256]{3,2,1,0:T(8,128)(2,1)S(1)}, u32[]{:S(2)}, u32[]{:S(2)}) collective-permute-start(bf16[3,8,32,256]{3,2,1,0:T(8,128)(2,1)S(1)} %get-tuple-element.20), channel_id=1, source_target_pairs={{0,8},{8,16},{16,24},{24,0},{32,40},{40,48},{48,56},{56,32},{64,72... | collective-permute-start | bytes 1179656 | tf_op jit(solution)/shard_map/ppermute | solution.py:361
  27.0 3.2 %collective-permute-start.6 = (bf16[1024,256]{1,0:T(8,128)(2,1)S(1)}, bf16[1024,256]{1,0:T(8,128)(2,1)S(1)}, u32[]{:S(2)}, u32[]{:S(2)}) collective-permute-start(bf16[1024,256]{1,0:T(8,128)(2,1)S(1)} %collective-permute-done.4.refs_2_), channel_id=1, source_target_pairs={{0,224},{8,232},{16,240},{24,248},{32,0},{40,8},{48,16},{56,24},{6... | collective-permute-start | bytes 1572872 | tf_op jit(solution)/shard_map/ppermute | solution.py:354
  30.3 1.1 collective-permute-start.8
  31.4 6.2 %collective-permute-done.7.refs_5_ = bf16[3,8,32,256]{3,2,1,0:T(8,128)(2,1)S(1)} collective-permute-done((bf16[3,8,32,256]{3,2,1,0:T(8,128)(2,1)S(1)}, bf16[3,8,32,256]{3,2,1,0:T(8,128)(2,1)S(1)}, u32[]{:S(2)}, u32[]{:S(2)}) %collective-permute-start.7) | collective-permute-done | bytes 393248 | tf_op jit(solution)/shard_map/ppermute | solution.py:361
  37.5 3.0 %collective-permute-start.23 = (bf16[256,2048]{1,0:T(8,128)(2,1)}, bf16[256,2048]{1,0:T(8,128)(2,1)}, u32[]{:S(2)}, u32[]{:S(2)}) collective-permute-start(bf16[256,2048]{1,0:T(8,128)(2,1)} %refs_0_.5), channel_id=1, source_target_pairs={{0,6},{1,7},{2,0},{3,1},{4,2},{5,3},{6,4},{7,5},{8,14},{9,15},{10,... | collective-permute-start | bytes 3145736 | tf_op jit(solution)/shard_map/ppermute | solution.py:363
  40.6 3.6 %collective-permute-start.14 = (bf16[1024,256]{1,0:T(8,128)(2,1)S(1)}, bf16[1024,256]{1,0:T(8,128)(2,1)S(1)}, u32[]{:S(2)}, u32[]{:S(2)}) collective-permute-start(bf16[1024,256]{1,0:T(8,128)(2,1)S(1)} %collective-permute-done.6.refs_1_.refs_4_), channel_id=1, source_target_pairs={{0,224},{8,232},{16,240},{24,248},{32,0},{40,8},{48,16},{56,24},{6... | collective-permute-start | bytes 1572872 | tf_op jit(solution)/shard_map/ppermute | solution.py:354
  44.1 1.5 %collective-permute-start.24 = (bf16[256,2048]{1,0:T(8,128)(2,1)}, bf16[256,2048]{1,0:T(8,128)(2,1)}, u32[]{:S(2)}, u32[]{:S(2)}) collective-permute-start(bf16[256,2048]{1,0:T(8,128)(2,1)} %collective-permute-done.22.refs_1_), channel_id=1, source_target_pairs={{0,2},{1,3},{2,4},{3,5},{4,6},{5,7},{6,0},{7,1},{8,10},{9,11},{10,... | collective-permute-start | bytes 3145736 | tf_op jit(solution)/shard_map/ppermute | solution.py:364
  45.6 0.8 copy-done.5
  46.4 1.5 %collective-permute-start.9 = (bf16[3,8,32,256]{3,2,1,0:T(8,128)(2,1)S(1)}, bf16[3,8,32,256]{3,2,1,0:T(8,128)(2,1)S(1)}, u32[]{:S(2)}, u32[]{:S(2)}) collective-permute-start(bf16[3,8,32,256]{3,2,1,0:T(8,128)(2,1)S(1)} %get-tuple-element.22), channel_id=1, source_target_pairs={{0,24},{8,0},{16,8},{24,16},{32,56},{40,32},{48,40},{56,48},{64,88... | collective-permute-start | bytes 1179656 | tf_op jit(solution)/shard_map/ppermute | solution.py:361
  47.9 4.7 %collective-permute-done.13.refs_0_ = bf16[1024,256]{1,0:T(8,128)(2,1)S(1)} collective-permute-done((bf16[1024,256]{1,0:T(8,128)(2,1)S(1)}, bf16[1024,256]{1,0:T(8,128)(2,1)S(1)}, u32[]{:S(2)}, u32[]{:S(2)}) %collective-permute-start.13) | collective-permute-done | bytes 524320 | tf_op jit(solution)/shard_map/ppermute | solution.py:352
  52.6 0.7 shard_map.94
  53.3 1.6 %collective-permute-done.9.refs_7_ = bf16[3,8,32,256]{3,2,1,0:T(8,128)(2,1)S(1)} collective-permute-done((bf16[3,8,32,256]{3,2,1,0:T(8,128)(2,1)S(1)}, bf16[3,8,32,256]{3,2,1,0:T(8,128)(2,1)S(1)}, u32[]{:S(2)}, u32[]{:S(2)}) %collective-permute-start.9) | collective-permute-done | bytes 393248 | tf_op jit(solution)/shard_map/ppermute | solution.py:361
  55.0 1.2 collective-permute-start.10
  56.2 3.3 %collective-permute-start.11 = (bf16[2,8,32,256]{3,2,1,0:T(8,128)(2,1)S(1)}, bf16[2,8,32,256]{3,2,1,0:T(8,128)(2,1)S(1)}, u32[]{:S(2)}, u32[]{:S(2)}) collective-permute-start(bf16[2,8,32,256]{3,2,1,0:T(8,128)(2,1)S(1)} %get-tuple-element.24), channel_id=1, source_target_pairs={{0,16},{8,24},{16,0},{24,8},{32,48},{40,56},{48,32},{56,40},{64,80... | collective-permute-start | bytes 786440 | tf_op jit(solution)/shard_map/ppermute | solution.py:361
  59.5 0.7 shard_map.95
  60.2 1.7 %collective-permute-start.12 = (bf16[2,8,32,256]{3,2,1,0:T(8,128)(2,1)S(1)}, bf16[2,8,32,256]{3,2,1,0:T(8,128)(2,1)S(1)}, u32[]{:S(2)}, u32[]{:S(2)}) collective-permute-start(bf16[2,8,32,256]{3,2,1,0:T(8,128)(2,1)S(1)} %get-tuple-element.25), channel_id=1, source_target_pairs={{0,24},{8,0},{16,8},{24,16},{32,56},{40,32},{48,40},{56,48},{64,88... | collective-permute-start | bytes 786440 | tf_op jit(solution)/shard_map/ppermute | solution.py:361
  61.9 4.2 %collective-permute-done.10.refs_8_ = bf16[2,8,32,256]{3,2,1,0:T(8,128)(2,1)S(1)} collective-permute-done((bf16[2,8,32,256]{3,2,1,0:T(8,128)(2,1)S(1)}, bf16[2,8,32,256]{3,2,1,0:T(8,128)(2,1)S(1)}, u32[]{:S(2)}, u32[]{:S(2)}) %collective-permute-start.10) | collective-permute-done | bytes 262176 | tf_op jit(solution)/shard_map/ppermute | solution.py:361
  66.1 0.7 copy-done.9
  66.8 3.0 %collective-permute-start.16 = (bf16[2,8,32,256]{3,2,1,0:T(8,128)(2,1)S(1)}, bf16[2,8,32,256]{3,2,1,0:T(8,128)(2,1)S(1)}, u32[]{:S(2)}, u32[]{:S(2)}) collective-permute-start(bf16[2,8,32,256]{3,2,1,0:T(8,128)(2,1)S(1)} %get-tuple-element.29), channel_id=1, source_target_pairs={{0,8},{8,16},{16,24},{24,0},{32,40},{40,48},{48,56},{56,32},{64,72... | collective-permute-start | bytes 786440 | tf_op jit(solution)/shard_map/ppermute | solution.py:361
  69.8 0.7 copy-done.11
  70.5 1.2 collective-permute-start.17
  71.7 1.3 collective-permute-start.18
  73.1 1.3 shard_map.96
  74.4 0.9 copy-done.3
  75.2 0.7 copy-done.15
  76.0 2.3 %collective-permute-done.16.refs_3_ = bf16[2,8,32,256]{3,2,1,0:T(8,128)(2,1)S(1)} collective-permute-done((bf16[2,8,32,256]{3,2,1,0:T(8,128)(2,1)S(1)}, bf16[2,8,32,256]{3,2,1,0:T(8,128)(2,1)S(1)}, u32[]{:S(2)}, u32[]{:S(2)}) %collective-permute-start.16) | collective-permute-done | bytes 262176 | tf_op jit(solution)/shard_map/ppermute | solution.py:361
  78.2 0.7 copy-done.13
  78.9 0.7 copy-done.17
  79.7 0.5 collective-permute-start.27
  80.2 1.0 collective-permute-done.18.refs_5_
  81.2 0.7 copy-done.19
  81.9 1.4 %collective-permute-start.19 = (bf16[1,8,32,256]{3,2,1,0:T(8,128)(2,1)S(1)}, bf16[1,8,32,256]{3,2,1,0:T(8,128)(2,1)S(1)}, u32[]{:S(2)}, u32[]{:S(2)}) collective-permute-start(bf16[1,8,32,256]{3,2,1,0:T(8,128)(2,1)S(1)} %get-tuple-element.32), channel_id=1, source_target_pairs={{0,8},{8,16},{16,24},{24,0},{32,40},{40,48},{48,56},{56,32},{64,72... | collective-permute-start | bytes 393224 | tf_op jit(solution)/shard_map/ppermute | solution.py:361
  83.3 0.4 slice_reduce_fusion.11
  83.7 4.7 %collective-permute-done.19.refs_6_ = bf16[1,8,32,256]{3,2,1,0:T(8,128)(2,1)S(1)} collective-permute-done((bf16[1,8,32,256]{3,2,1,0:T(8,128)(2,1)S(1)}, bf16[1,8,32,256]{3,2,1,0:T(8,128)(2,1)S(1)}, u32[]{:S(2)}, u32[]{:S(2)}) %collective-permute-start.19) | collective-permute-done | bytes 131104 | tf_op jit(solution)/shard_map/ppermute | solution.py:361
  88.4 0.7 copy-done.21
  89.1 1.3 collective-permute-start.20
  90.4 0.1 or_select_fusion.bias
  90.5 5.0 %collective-permute-done.20.refs_7_ = bf16[1,8,32,256]{3,2,1,0:T(8,128)(2,1)S(1)} collective-permute-done((bf16[1,8,32,256]{3,2,1,0:T(8,128)(2,1)S(1)}, bf16[1,8,32,256]{3,2,1,0:T(8,128)(2,1)S(1)}, u32[]{:S(2)}, u32[]{:S(2)}) %collective-permute-start.20) | collective-permute-done | bytes 131104 | tf_op jit(solution)/shard_map/ppermute | solution.py:361
  95.5 0.6 copy-done.23
  96.2 3.0 %collective-permute-start.21 = (bf16[1,8,32,256]{3,2,1,0:T(8,128)(2,1)}, bf16[1,8,32,256]{3,2,1,0:T(8,128)(2,1)}, u32[]{:S(2)}, u32[]{:S(2)}) collective-permute-start(bf16[1,8,32,256]{3,2,1,0:T(8,128)(2,1)} %get-tuple-element.34), channel_id=1, source_target_pairs={{0,24},{8,0},{16,8},{24,16},{32,56},{40,32},{48,40},{56,48},{64,88... | collective-permute-start | bytes 393224 | tf_op jit(solution)/shard_map/ppermute | solution.py:361
  99.1 5.1 %shard_map.91.q = bf16[1024,256]{1,0:T(8,128)(2,1)} custom-call(bf16[1024,2048]{1,0:T(8,128)(2,1)} %tok.3, bf16[2048,256]{1,0:T(8,128)(2,1)} %refs_0_.3), custom_call_target="tpu_custom_call" | custom-call | flops 1000000000 | bytes 6000000 | tf_op jit(solution)/shard_map/pallas_call | solution.py:78
  104.3 1.0 copy-done
  105.3 1.0 copy-done.6
  106.3 1.0 copy-done.8
  107.3 0.9 copy-done.10
  108.3 0.9 copy-done.12
  109.2 0.9 copy-done.16
  110.2 3.6 %early.1 = (f32[2048,128]{1,0:T(8,128)S(1)}, f32[2048,128]{1,0:T(8,128)S(1)}, f32[2048,128]{1,0:T(8,128)S(1)}) custom-call(s32[4,64]{1,0:T(4,128)S(1)} %fusion.2.want, f32[8,1024]{1,0:T(8,128)S(1)} %or_select_fusion.bias, bf16[1024,256]{1,0:T(8,128)(2,1)S(1)} %copy-done, bf16[1024,256]{1,0:T(8,128)(2,1)S(1)} %copy-done.2, ...), custom_call_target="tpu_custom_call" | custom-call | flops 900000000 | bytes 6000000 | tf_op jit(solution)/shard_map/early/pallas_call | solution.py:244
  113.9 3.5 %late.1 = bf16[1024,256]{1,0:T(8,128)(2,1)} custom-call(s32[4,64]{1,0:T(4,128)S(1)} %fusion.2.want, f32[8,1024]{1,0:T(8,128)S(1)} %or_select_fusion.bias, bf16[1024,256]{1,0:T(8,128)(2,1)S(1)} %copy-done, f32[2048,128]{1,0:T(8,128)S(1)} %get-tuple-element.26.acc, f32[2048,128]{1,0:T(8,128)S(1)} %get-tuple-element.27.top, ...), custom_call_target="tpu_custom_call" | custom-call | flops 400000000 | bytes 6000000 | tf_op jit(solution)/shard_map/late/pallas_call | solution.py:266
  117.4 4.2 %all-to-all-start = ((bf16[8,128,256]{2,1,0:T(8,128)(2,1)}), bf16[8,128,256]{2,1,0:T(8,128)(2,1)S(1)}, u32[]{:S(2)}, u32[]{:S(2)}) async-start(bf16[8,128,256]{2,1,0:T(8,128)(2,1)} %bitcast.8), calls=%async_computation | async-start | bytes 1048576 | tf_op jit(solution)/shard_map/all_to_all | solution.py:372
  121.7 10.2 %all-to-all-done.att = bf16[8,128,256]{2,1,0:T(8,128)(2,1)S(1)} async-done(((bf16[8,128,256]{2,1,0:T(8,128)(2,1)}), bf16[8,128,256]{2,1,0:T(8,128)(2,1)S(1)}, u32[]{:S(2)}, u32[]{:S(2)}) %all-to-all-start) | async-done | bytes 524320 | tf_op jit(solution)/shard_map/all_to_all | solution.py:372
  131.9 5.2 %project.1 = bf16[128,2048]{1,0:T(8,128)(2,1)} custom-call(s32[2,4]{1,0:T(2,128)S(1)} %pad_add_fusion.1.spot, bf16[8,128,256]{2,1,0:T(8,128)(2,1)S(1)} %all-to-all-done.att, bf16[256,2048]{1,0:T(8,128)(2,1)} %refs_0_.5, bf16[256,2048]{1,0:T(8,128)(2,1)} %collective-permute-done.22.refs_1_, bf16[256,2048]{1,0:T(8,128)(2,1)} %collective-permute-done.23.refs_2_, ...), custom_call_target="tpu_custom_call" | custom-call | flops 1000000000 | bytes 9000000 | tf_op jit(solution)/shard_map/project/pallas_call | solution.py:303
  (75 shorter events, 0.4 us)
Async XLA Ops:
  0.0 17.6 %copy-start.28 = (s32[64]{0:T(128)S(1)}, s32[64]{0:T(128)}, u32[]{:S(2)}) copy-start(s32[64]{0:T(128)} %constant.145) | copy-start | bytes 772
  0.0 73.0 %copy-start.26 = (s32[1024]{0:T(1024)S(1)}, s32[1024]{0:T(1024)}, u32[]{:S(2)}) copy-start(s32[1024]{0:T(1024)} %constant.146) | copy-start | bytes 12292
  0.0 73.0 %copy-start.27 = (s32[1024]{0:T(1024)S(1)}, s32[1024]{0:T(1024)}, u32[]{:S(2)}) copy-start(s32[1024]{0:T(1024)} %constant.147) | copy-start | bytes 12292
  0.0 11.2 %copy-start.25 = (s32[8,12]{1,0:T(8,128)S(1)}, s32[8,12]{1,0:T(8,128)}, u32[]{:S(2)}) copy-start(s32[8,12]{1,0:T(8,128)} %param.14) | copy-start | bytes 1156
  5.2 18.1 %collective-permute-start.3 = (bf16[1024,256]{1,0:T(8,128)(2,1)}, bf16[1024,256]{1,0:T(8,128)(2,1)S(1)}, u32[]{:S(2)}, u32[]{:S(2)}) collective-permute-start(bf16[1024,256]{1,0:T(8,128)(2,1)} %shard_map.92.refs_0_), channel_id=1, source_target_pairs={{0,32},{8,40},{16,48},{24,56},{32,64},{40,72},{48,80},{56,88},{64,... | collective-permute-start | bytes 1572872 | tf_op jit(solution)/shard_map/ppermute | solution.py:352
  7.2 16.5 %collective-permute-start.4 = (bf16[1024,256]{1,0:T(8,128)(2,1)}, bf16[1024,256]{1,0:T(8,128)(2,1)S(1)}, u32[]{:S(2)}, u32[]{:S(2)}) collective-permute-start(bf16[1024,256]{1,0:T(8,128)(2,1)} %shard_map.92.refs_0_), channel_id=1, source_target_pairs={{0,224},{8,232},{16,240},{24,248},{32,0},{40,8},{48,16},{56,24},{6... | collective-permute-start | bytes 1572872 | tf_op jit(solution)/shard_map/ppermute | solution.py:354
  11.2 4.8 %collective-permute-start = (s32[8,12]{1,0:T(8,128)S(1)}, s32[8,12]{1,0:T(8,128)S(1)}, u32[]{:S(2)}, u32[]{:S(2)}) collective-permute-start(s32[8,12]{1,0:T(8,128)S(1)} %copy-done.25), channel_id=1, source_target_pairs={{0,24},{8,0},{16,8},{24,16},{32,56},{40,32},{48,40},{56,48},{64,88... | collective-permute-start | bytes 1160 | tf_op jit(solution)/shard_map/ppermute | solution.py:329
  11.8 11.5 %collective-permute-start.1 = (s32[8,12]{1,0:T(8,128)S(1)}, s32[8,12]{1,0:T(8,128)S(1)}, u32[]{:S(2)}, u32[]{:S(2)}) collective-permute-start(s32[8,12]{1,0:T(8,128)S(1)} %copy-done.25), channel_id=1, source_target_pairs={{0,16},{8,24},{16,0},{24,8},{32,48},{40,56},{48,32},{56,40},{64,80... | collective-permute-start | bytes 1160 | tf_op jit(solution)/shard_map/ppermute | solution.py:329
  14.2 9.1 %collective-permute-start.2 = (s32[8,12]{1,0:T(8,128)S(1)}, s32[8,12]{1,0:T(8,128)S(1)}, u32[]{:S(2)}, u32[]{:S(2)}) collective-permute-start(s32[8,12]{1,0:T(8,128)S(1)} %copy-done.25), channel_id=1, source_target_pairs={{0,8},{8,16},{16,24},{24,0},{32,40},{40,48},{48,56},{56,32},{64,72... | collective-permute-start | bytes 1160 | tf_op jit(solution)/shard_map/ppermute | solution.py:329
  16.0 28.1 %collective-permute-start.22 = (bf16[256,2048]{1,0:T(8,128)(2,1)}, bf16[256,2048]{1,0:T(8,128)(2,1)}, u32[]{:S(2)}, u32[]{:S(2)}) collective-permute-start(bf16[256,2048]{1,0:T(8,128)(2,1)} %refs_0_.5), channel_id=1, source_target_pairs={{0,2},{1,3},{2,4},{3,5},{4,6},{5,7},{6,0},{7,1},{8,10},{9,11},{10,... | collective-permute-start | bytes 3145736 | tf_op jit(solution)/shard_map/ppermute | solution.py:362
  23.3 17.3 %collective-permute-start.5 = (bf16[1024,256]{1,0:T(8,128)(2,1)S(1)}, bf16[1024,256]{1,0:T(8,128)(2,1)S(1)}, u32[]{:S(2)}, u32[]{:S(2)}) collective-permute-start(bf16[1024,256]{1,0:T(8,128)(2,1)S(1)} %collective-permute-done.3.refs_1_), channel_id=1, source_target_pairs={{0,32},{8,40},{16,48},{24,56},{32,64},{40,72},{48,80},{56,88},{64,... | collective-permute-start | bytes 1572872 | tf_op jit(solution)/shard_map/ppermute | solution.py:352
  23.7 1.0 copy-start.1
  25.5 12.1 %collective-permute-start.7 = (bf16[3,8,32,256]{3,2,1,0:T(8,128)(2,1)S(1)}, bf16[3,8,32,256]{3,2,1,0:T(8,128)(2,1)S(1)}, u32[]{:S(2)}, u32[]{:S(2)}) collective-permute-start(bf16[3,8,32,256]{3,2,1,0:T(8,128)(2,1)S(1)} %get-tuple-element.20), channel_id=1, source_target_pairs={{0,8},{8,16},{16,24},{24,0},{32,40},{40,48},{48,56},{56,32},{64,72... | collective-permute-start | bytes 1179656 | tf_op jit(solution)/shard_map/ppermute | solution.py:361
  27.0 13.5 %collective-permute-start.6 = (bf16[1024,256]{1,0:T(8,128)(2,1)S(1)}, bf16[1024,256]{1,0:T(8,128)(2,1)S(1)}, u32[]{:S(2)}, u32[]{:S(2)}) collective-permute-start(bf16[1024,256]{1,0:T(8,128)(2,1)S(1)} %collective-permute-done.4.refs_2_), channel_id=1, source_target_pairs={{0,224},{8,232},{16,240},{24,248},{32,0},{40,8},{48,16},{56,24},{6... | collective-permute-start | bytes 1572872 | tf_op jit(solution)/shard_map/ppermute | solution.py:354
  30.3 15.3 %collective-permute-start.8 = (bf16[3,8,32,256]{3,2,1,0:T(8,128)(2,1)S(1)}, bf16[3,8,32,256]{3,2,1,0:T(8,128)(2,1)S(1)}, u32[]{:S(2)}, u32[]{:S(2)}) collective-permute-start(bf16[3,8,32,256]{3,2,1,0:T(8,128)(2,1)S(1)} %get-tuple-element.21), channel_id=1, source_target_pairs={{0,16},{8,24},{16,0},{24,8},{32,48},{40,56},{48,32},{56,40},{64,80... | collective-permute-start | bytes 1179656 | tf_op jit(solution)/shard_map/ppermute | solution.py:361
  37.5 22.7 %collective-permute-start.23 = (bf16[256,2048]{1,0:T(8,128)(2,1)}, bf16[256,2048]{1,0:T(8,128)(2,1)}, u32[]{:S(2)}, u32[]{:S(2)}) collective-permute-start(bf16[256,2048]{1,0:T(8,128)(2,1)} %refs_0_.5), channel_id=1, source_target_pairs={{0,6},{1,7},{2,0},{3,1},{4,2},{5,3},{6,4},{7,5},{8,14},{9,15},{10,... | collective-permute-start | bytes 3145736 | tf_op jit(solution)/shard_map/ppermute | solution.py:363
  40.5 12.1 %collective-permute-start.13 = (bf16[1024,256]{1,0:T(8,128)(2,1)S(1)}, bf16[1024,256]{1,0:T(8,128)(2,1)S(1)}, u32[]{:S(2)}, u32[]{:S(2)}) collective-permute-start(bf16[1024,256]{1,0:T(8,128)(2,1)S(1)} %collective-permute-done.5.refs_0_.refs_3_), channel_id=1, source_target_pairs={{0,32},{8,40},{16,48},{24,56},{32,64},{40,72},{48,80},{56,88},{64,... | collective-permute-start | bytes 1572872 | tf_op jit(solution)/shard_map/ppermute | solution.py:352
  40.6 15.6 %collective-permute-start.14 = (bf16[1024,256]{1,0:T(8,128)(2,1)S(1)}, bf16[1024,256]{1,0:T(8,128)(2,1)S(1)}, u32[]{:S(2)}, u32[]{:S(2)}) collective-permute-start(bf16[1024,256]{1,0:T(8,128)(2,1)S(1)} %collective-permute-done.6.refs_1_.refs_4_), channel_id=1, source_target_pairs={{0,224},{8,232},{16,240},{24,248},{32,0},{40,8},{48,16},{56,24},{6... | collective-permute-start | bytes 1572872 | tf_op jit(solution)/shard_map/ppermute | solution.py:354
  44.1 39.2 %collective-permute-start.24 = (bf16[256,2048]{1,0:T(8,128)(2,1)}, bf16[256,2048]{1,0:T(8,128)(2,1)}, u32[]{:S(2)}, u32[]{:S(2)}) collective-permute-start(bf16[256,2048]{1,0:T(8,128)(2,1)} %collective-permute-done.22.refs_1_), channel_id=1, source_target_pairs={{0,2},{1,3},{2,4},{3,5},{4,6},{5,7},{6,0},{7,1},{8,10},{9,11},{10,... | collective-permute-start | bytes 3145736 | tf_op jit(solution)/shard_map/ppermute | solution.py:364
  45.6 0.8 copy-start.5
  46.4 57.9 %copy-start.2 = (bf16[1024,256]{1,0:T(8,128)(2,1)S(1)}, bf16[1024,256]{1,0:T(8,128)(2,1)}, u32[]{:S(2)}) copy-start(bf16[1024,256]{1,0:T(8,128)(2,1)} %shard_map.92.refs_0_) | copy-start | bytes 1572868
  46.4 8.5 %collective-permute-start.9 = (bf16[3,8,32,256]{3,2,1,0:T(8,128)(2,1)S(1)}, bf16[3,8,32,256]{3,2,1,0:T(8,128)(2,1)S(1)}, u32[]{:S(2)}, u32[]{:S(2)}) collective-permute-start(bf16[3,8,32,256]{3,2,1,0:T(8,128)(2,1)S(1)} %get-tuple-element.22), channel_id=1, source_target_pairs={{0,24},{8,0},{16,8},{24,16},{32,56},{40,32},{48,40},{56,48},{64,88... | collective-permute-start | bytes 1179656 | tf_op jit(solution)/shard_map/ppermute | solution.py:361
  52.6 19.1 %collective-permute-start.15 = (bf16[1024,256]{1,0:T(8,128)(2,1)S(1)}, bf16[1024,256]{1,0:T(8,128)(2,1)S(1)}, u32[]{:S(2)}, u32[]{:S(2)}) collective-permute-start(bf16[1024,256]{1,0:T(8,128)(2,1)S(1)} %collective-permute-done.13.refs_0_), channel_id=1, source_target_pairs={{0,32},{8,40},{16,48},{24,56},{32,64},{40,72},{48,80},{56,88},{64,... | collective-permute-start | bytes 1572872 | tf_op jit(solution)/shard_map/ppermute | solution.py:352
  55.0 16.8 %copy-start.7 = (bf16[3,8,32,256]{3,2,1,0:T(8,128)(2,1)}, bf16[3,8,32,256]{3,2,1,0:T(8,128)(2,1)S(1)}, u32[]{:S(2)}) copy-start(bf16[3,8,32,256]{3,2,1,0:T(8,128)(2,1)S(1)} %collective-permute-done.9.refs_7_) | copy-start | bytes 1179652
  55.0 11.1 %collective-permute-start.10 = (bf16[2,8,32,256]{3,2,1,0:T(8,128)(2,1)S(1)}, bf16[2,8,32,256]{3,2,1,0:T(8,128)(2,1)S(1)}, u32[]{:S(2)}, u32[]{:S(2)}) collective-permute-start(bf16[2,8,32,256]{3,2,1,0:T(8,128)(2,1)S(1)} %get-tuple-element.23), channel_id=1, source_target_pairs={{0,8},{8,16},{16,24},{24,0},{32,40},{40,48},{48,56},{56,32},{64,72... | collective-permute-start | bytes 786440 | tf_op jit(solution)/shard_map/ppermute | solution.py:361
  56.2 13.6 %collective-permute-start.11 = (bf16[2,8,32,256]{3,2,1,0:T(8,128)(2,1)S(1)}, bf16[2,8,32,256]{3,2,1,0:T(8,128)(2,1)S(1)}, u32[]{:S(2)}, u32[]{:S(2)}) collective-permute-start(bf16[2,8,32,256]{3,2,1,0:T(8,128)(2,1)S(1)} %get-tuple-element.24), channel_id=1, source_target_pairs={{0,16},{8,24},{16,0},{24,8},{32,48},{40,56},{48,32},{56,40},{64,80... | collective-permute-start | bytes 786440 | tf_op jit(solution)/shard_map/ppermute | solution.py:361
  60.2 15.0 %collective-permute-start.12 = (bf16[2,8,32,256]{3,2,1,0:T(8,128)(2,1)S(1)}, bf16[2,8,32,256]{3,2,1,0:T(8,128)(2,1)S(1)}, u32[]{:S(2)}, u32[]{:S(2)}) collective-permute-start(bf16[2,8,32,256]{3,2,1,0:T(8,128)(2,1)S(1)} %get-tuple-element.25), channel_id=1, source_target_pairs={{0,24},{8,0},{16,8},{24,16},{32,56},{40,32},{48,40},{56,48},{64,88... | collective-permute-start | bytes 786440 | tf_op jit(solution)/shard_map/ppermute | solution.py:361
  66.1 0.7 copy-start.9
  66.8 11.4 %collective-permute-start.16 = (bf16[2,8,32,256]{3,2,1,0:T(8,128)(2,1)S(1)}, bf16[2,8,32,256]{3,2,1,0:T(8,128)(2,1)S(1)}, u32[]{:S(2)}, u32[]{:S(2)}) collective-permute-start(bf16[2,8,32,256]{3,2,1,0:T(8,128)(2,1)S(1)} %get-tuple-element.29), channel_id=1, source_target_pairs={{0,8},{8,16},{16,24},{24,0},{32,40},{40,48},{48,56},{56,32},{64,72... | collective-permute-start | bytes 786440 | tf_op jit(solution)/shard_map/ppermute | solution.py:361
  69.8 0.7 copy-start.11
  70.5 8.4 %collective-permute-start.17 = (bf16[2,8,32,256]{3,2,1,0:T(8,128)(2,1)S(1)}, bf16[2,8,32,256]{3,2,1,0:T(8,128)(2,1)S(1)}, u32[]{:S(2)}, u32[]{:S(2)}) collective-permute-start(bf16[2,8,32,256]{3,2,1,0:T(8,128)(2,1)S(1)} %get-tuple-element.30), channel_id=1, source_target_pairs={{0,16},{8,24},{16,0},{24,8},{32,48},{40,56},{48,32},{56,40},{64,80... | collective-permute-start | bytes 786440 | tf_op jit(solution)/shard_map/ppermute | solution.py:361
  71.7 9.4 %collective-permute-start.18 = (bf16[2,8,32,256]{3,2,1,0:T(8,128)(2,1)S(1)}, bf16[2,8,32,256]{3,2,1,0:T(8,128)(2,1)S(1)}, u32[]{:S(2)}, u32[]{:S(2)}) collective-permute-start(bf16[2,8,32,256]{3,2,1,0:T(8,128)(2,1)S(1)} %get-tuple-element.31), channel_id=1, source_target_pairs={{0,24},{8,0},{16,8},{24,16},{32,56},{40,32},{48,40},{56,48},{64,88... | collective-permute-start | bytes 786440 | tf_op jit(solution)/shard_map/ppermute | solution.py:361
  74.4 0.9 copy-start.3
  75.2 0.7 copy-start.15
  76.0 45.7 %collective-permute-start.25 = (bf16[256,2048]{1,0:T(8,128)(2,1)}, bf16[256,2048]{1,0:T(8,128)(2,1)}, u32[]{:S(2)}, u32[]{:S(2)}) collective-permute-start(bf16[256,2048]{1,0:T(8,128)(2,1)} %refs_0_.5), channel_id=1, source_target_pairs={{0,1},{1,0},{2,3},{3,2},{4,5},{5,4},{6,7},{7,6},{8,9},{9,8},{10,11... | collective-permute-start | bytes 3145736 | tf_op jit(solution)/shard_map/ppermute | solution.py:365
  78.2 0.7 copy-start.13
  78.9 42.7 %collective-permute-start.26 = (bf16[256,2048]{1,0:T(8,128)(2,1)}, bf16[256,2048]{1,0:T(8,128)(2,1)}, u32[]{:S(2)}, u32[]{:S(2)}) collective-permute-start(bf16[256,2048]{1,0:T(8,128)(2,1)} %collective-permute-done.22.refs_1_), channel_id=1, source_target_pairs={{0,1},{1,0},{2,3},{3,2},{4,5},{5,4},{6,7},{7,6},{8,9},{9,8},{10,11... | collective-permute-start | bytes 3145736 | tf_op jit(solution)/shard_map/ppermute | solution.py:365
  78.9 0.7 copy-start.17
  79.7 42.0 %collective-permute-start.27 = (bf16[256,2048]{1,0:T(8,128)(2,1)}, bf16[256,2048]{1,0:T(8,128)(2,1)}, u32[]{:S(2)}, u32[]{:S(2)}) collective-permute-start(bf16[256,2048]{1,0:T(8,128)(2,1)} %collective-permute-done.23.refs_2_), channel_id=1, source_target_pairs={{0,1},{1,0},{2,3},{3,2},{4,5},{5,4},{6,7},{7,6},{8,9},{9,8},{10,11... | collective-permute-start | bytes 3145736 | tf_op jit(solution)/shard_map/ppermute | solution.py:365
  81.2 0.7 copy-start.19
  81.9 6.5 %collective-permute-start.19 = (bf16[1,8,32,256]{3,2,1,0:T(8,128)(2,1)S(1)}, bf16[1,8,32,256]{3,2,1,0:T(8,128)(2,1)S(1)}, u32[]{:S(2)}, u32[]{:S(2)}) collective-permute-start(bf16[1,8,32,256]{3,2,1,0:T(8,128)(2,1)S(1)} %get-tuple-element.32), channel_id=1, source_target_pairs={{0,8},{8,16},{16,24},{24,0},{32,40},{40,48},{48,56},{56,32},{64,72... | collective-permute-start | bytes 393224 | tf_op jit(solution)/shard_map/ppermute | solution.py:361
  83.3 48.6 %collective-permute-start.28 = (bf16[256,2048]{1,0:T(8,128)(2,1)}, bf16[256,2048]{1,0:T(8,128)(2,1)}, u32[]{:S(2)}, u32[]{:S(2)}) collective-permute-start(bf16[256,2048]{1,0:T(8,128)(2,1)} %collective-permute-done.24.refs_3_), channel_id=1, source_target_pairs={{0,1},{1,0},{2,3},{3,2},{4,5},{5,4},{6,7},{7,6},{8,9},{9,8},{10,11... | collective-permute-start | bytes 3145736 | tf_op jit(solution)/shard_map/ppermute | solution.py:365
  88.4 0.7 copy-start.21
  89.1 6.5 %collective-permute-start.20 = (bf16[1,8,32,256]{3,2,1,0:T(8,128)(2,1)S(1)}, bf16[1,8,32,256]{3,2,1,0:T(8,128)(2,1)S(1)}, u32[]{:S(2)}, u32[]{:S(2)}) collective-permute-start(bf16[1,8,32,256]{3,2,1,0:T(8,128)(2,1)S(1)} %get-tuple-element.33), channel_id=1, source_target_pairs={{0,16},{8,24},{16,0},{24,8},{32,48},{40,56},{48,32},{56,40},{64,80... | collective-permute-start | bytes 393224 | tf_op jit(solution)/shard_map/ppermute | solution.py:361
  95.5 0.7 copy-start.23
  96.2 17.6 %collective-permute-start.21 = (bf16[1,8,32,256]{3,2,1,0:T(8,128)(2,1)}, bf16[1,8,32,256]{3,2,1,0:T(8,128)(2,1)}, u32[]{:S(2)}, u32[]{:S(2)}) collective-permute-start(bf16[1,8,32,256]{3,2,1,0:T(8,128)(2,1)} %get-tuple-element.34), channel_id=1, source_target_pairs={{0,24},{8,0},{16,8},{24,16},{32,56},{40,32},{48,40},{56,48},{64,88... | collective-permute-start | bytes 393224 | tf_op jit(solution)/shard_map/ppermute | solution.py:361
  104.3 1.0 copy-start
  105.3 1.0 copy-start.6
  106.3 1.0 copy-start.8
  107.3 0.9 copy-start.10
  108.3 0.9 copy-start.12
  109.2 0.9 copy-start.16
  110.2 3.6 %copy-start.4 = (bf16[1024,256]{1,0:T(8,128)(2,1)S(1)}, bf16[1024,256]{1,0:T(8,128)(2,1)}, u32[]{:S(2)}) copy-start(bf16[1024,256]{1,0:T(8,128)(2,1)} %copy-done.3) | copy-start | bytes 1572868
  110.2 3.6 %copy-start.14 = (bf16[2,8,32,256]{3,2,1,0:T(8,128)(2,1)S(1)}, bf16[2,8,32,256]{3,2,1,0:T(8,128)(2,1)}, u32[]{:S(2)}) copy-start(bf16[2,8,32,256]{3,2,1,0:T(8,128)(2,1)} %copy-done.13) | copy-start | bytes 786436
  110.2 3.7 %copy-start.18 = (bf16[2,8,32,256]{3,2,1,0:T(8,128)(2,1)S(1)}, bf16[2,8,32,256]{3,2,1,0:T(8,128)(2,1)}, u32[]{:S(2)}) copy-start(bf16[2,8,32,256]{3,2,1,0:T(8,128)(2,1)} %copy-done.17) | copy-start | bytes 786436
  110.2 3.7 %copy-start.20 = (bf16[2,8,32,256]{3,2,1,0:T(8,128)(2,1)S(1)}, bf16[2,8,32,256]{3,2,1,0:T(8,128)(2,1)}, u32[]{:S(2)}) copy-start(bf16[2,8,32,256]{3,2,1,0:T(8,128)(2,1)} %copy-done.19) | copy-start | bytes 786436
  110.2 3.7 %copy-start.22 = (bf16[1,8,32,256]{3,2,1,0:T(8,128)(2,1)S(1)}, bf16[1,8,32,256]{3,2,1,0:T(8,128)(2,1)}, u32[]{:S(2)}) copy-start(bf16[1,8,32,256]{3,2,1,0:T(8,128)(2,1)} %copy-done.21) | copy-start | bytes 393220
  110.2 3.7 %copy-start.24 = (bf16[1,8,32,256]{3,2,1,0:T(8,128)(2,1)S(1)}, bf16[1,8,32,256]{3,2,1,0:T(8,128)(2,1)}, u32[]{:S(2)}) copy-start(bf16[1,8,32,256]{3,2,1,0:T(8,128)(2,1)} %copy-done.23) | copy-start | bytes 393220
  117.4 14.5 %all-to-all-start = ((bf16[8,128,256]{2,1,0:T(8,128)(2,1)}), bf16[8,128,256]{2,1,0:T(8,128)(2,1)S(1)}, u32[]{:S(2)}, u32[]{:S(2)}) async-start(bf16[8,128,256]{2,1,0:T(8,128)(2,1)} %bitcast.8), calls=%async_computation | async-start | bytes 1048576 | tf_op jit(solution)/shard_map/all_to_all | solution.py:372

commit v4 on v3

--- a/solution.py
+++ b/solution.py
@@ -152,8 +152,7 @@
     return jnp.sum(a, axis=1, keepdims=True)
 
 
-def places(g, n):
-    j = g * GROUP + n
+def places(j):
     return j, pl.multiple_of(j * QB, QB), pl.ds(pl.multiple_of(j * 2 * QB, 2 * QB), 2 * QB)
 
 
@@ -170,7 +169,7 @@
         scale = HEAD ** (-0.5)
 
         def step(g, carry):
-            spots = [places(g, n) for n in range(GROUP)]
+            spots = [places(g * GROUP + n) for n in range(GROUP)]
             own, oth, m = [], [], []
             for n, (j, at, to) in enumerate(spots):
                 gather_blocks(kv.at[n], want, held, recv, counts, 0, j)
@@ -203,15 +202,17 @@
 def late_body(counts, first):
     total = sum(counts)
 
-    def body(want, bias, q, acc, top, low, *refs):
-        held, recv = refs[:total], refs[total:-2]
-        out, kv = refs[-2:]
+    def body(want, turn, bias, q, acc, top, low, *refs):
+        held, recv = refs[:total], refs[total:-3]
+        kv = refs[-1]
         begin = first * NX * KB
         far = kv.shape[1]
         scale = HEAD ** (-0.5)
 
-        def step(g, carry):
-            spots = [places(g, n) for n in range(GROUP)]
+        def step(out, other):
+            y, c = turn[0] // 2, turn[0] % 2
+            c = 1 - c if other else c
+            spots = [places((y + n) % NY * 2 + c) for n in range(NY)]
             oth, m, keep, inv = [], [], [], []
             for n, (j, at, to) in enumerate(spots):
                 gather_blocks(kv.at[n], want, held, recv, counts, first, j)
@@ -228,11 +229,11 @@
             for n, (j, at, to) in enumerate(spots):
                 mixed = acc[to, :] * keep[n] + dot(oth[n].astype(BF), kv[n, :, HEAD:])
                 mixed = (mixed * inv[n]).astype(BF)
-                out[pl.ds(at, QB), :HEAD] = mixed[:QB]
-                out[pl.ds(at, QB), HEAD:] = mixed[QB:]
-            return carry
-
-        lax.fori_loop(0, q.shape[0] // QB // GROUP, step, 0)
+                out[n, :, :HEAD] = mixed[:QB]
+                out[n, :, HEAD:] = mixed[QB:]
+
+        step(refs[-2], True)
+        step(refs[-3], False)
 
     return body
 
@@ -259,63 +260,93 @@
     )(want, bias, q, *ins)
 
 
-def attend_late(want, bias, q, sums, held, recv):
+def attend_late(want, turn, bias, q, sums, held, recv):
     counts = [r[0].shape[0] for r in recv]
     first = bias.shape[1] // (NX * KB) - sum(counts)
     ins = [*held, *[a for r in recv for a in r]]
     return pl.pallas_call(
         late_body(counts, first),
-        out_shape=jax.ShapeDtypeStruct(q.shape, BF),
-        in_specs=[SMEM] + [VMEM] * (2 + len(sums) + len(ins)),
-        out_specs=VMEM,
-        scratch_shapes=[pltpu.VMEM((GROUP, sum(counts) * NX * KB, 2 * HEAD), BF)],
+        out_shape=[jax.ShapeDtypeStruct((NY, QB, 2 * HEAD), BF)] * 2,
+        in_specs=[SMEM] * 2 + [VMEM] * (2 + len(sums) + len(ins)),
+        out_specs=[VMEM] * 2,
+        scratch_shapes=[pltpu.VMEM((NY, sum(counts) * NX * KB, 2 * HEAD), BF)],
         compiler_params=params(16),
         cost_estimate=pl.CostEstimate(
             flops=400_000_000, bytes_accessed=6_000_000, transcendentals=800_000
         ),
         name="late",
-    )(want, bias, q, *sums, *ins)
-
-
-def project_body(spot, att, *refs):
-    count = 2 * NY
-    weights, (out, near, acc, sems) = refs[:count], refs[count:]
-    copies = [pltpu.make_async_copy(w, near.at[i], sems.at[i]) for i, w in enumerate(weights)]
+    )(want, turn, bias, q, *sums, *ins)
+
+
+def pack_body(mine, theirs, *outs):
+    for n, out in enumerate(outs):
+        out[0] = mine[n + 1]
+        out[1] = theirs[n + 1]
+
+
+def pack(mine, theirs):
+    return pl.pallas_call(
+        pack_body,
+        out_shape=[jax.ShapeDtypeStruct((2, *mine.shape[1:]), BF)] * (NY - 1),
+        in_specs=[VMEM] * 2,
+        out_specs=[VMEM] * (NY - 1),
+        compiler_params=params(4),
+        cost_estimate=pl.CostEstimate(flops=1_000_000, bytes_accessed=800_000, transcendentals=0),
+        name="pack",
+    )(mine, theirs)
+
+
+def stage_body(*refs):
+    out, sems = refs[-2:]
+    copies = [pltpu.make_async_copy(ref, out.at[n], sems.at[n]) for n, ref in enumerate(refs[:-2])]
+    run_all(copies)
+
+
+def run_all(copies):
     for c in copies:
         c.start()
+    for c in copies:
+        c.wait()
+
+
+def stage(weights):
+    return pl.pallas_call(
+        stage_body,
+        out_shape=jax.ShapeDtypeStruct((len(weights), *weights[0].shape), BF),
+        in_specs=[ANY] * len(weights),
+        out_specs=VMEM,
+        scratch_shapes=[pltpu.SemaphoreType.DMA((len(weights),))],
+        compiler_params=params(10),
+        cost_estimate=pl.CostEstimate(flops=1_000_000_000, bytes_accessed=16_000_000, transcendentals=0),
+        name="stage",
+    )(*weights)
+
+
+def project_body(mine, theirs, *refs):
+    others, (weights, out) = refs[:-2], refs[-2:]
+    left = [mine[0], *[a[0] for a in others], theirs[0], *[a[1] for a in others]]
     tile = 512
-    for i, c in enumerate(copies):
-        c.wait()
-        mine = att[spot[i // NY, i % NY]]
-        for n in range(out.shape[1] // tile):
-            cols = slice(n * tile, (n + 1) * tile)
-            part = dot(mine, near[i, :, cols]).astype(BF).astype(F32)
-            if i == 0:
-                acc[:, cols] = part
-            elif i < count - 1:
-                acc[:, cols] += part
-            else:
-                out[:, cols] = (acc[:, cols] + part).astype(BF)
-
-
-def project(spot, att, weights):
-    deep, width = weights[0].shape
+    for n in range(out.shape[1] // tile):
+        cols = slice(n * tile, (n + 1) * tile)
+        acc = None
+        for i, a in enumerate(left):
+            part = dot(a, weights[i, :, cols]).astype(BF).astype(F32)
+            acc = part if acc is None else acc + part
+        out[:, cols] = acc.astype(BF)
+
+
+def project(mine, theirs, others, weights):
     return pl.pallas_call(
         project_body,
-        out_shape=jax.ShapeDtypeStruct((QB, width), BF),
-        in_specs=[SMEM, VMEM] + [ANY] * len(weights),
+        out_shape=jax.ShapeDtypeStruct((QB, weights.shape[2]), BF),
+        in_specs=[VMEM] * (3 + len(others)),
         out_specs=VMEM,
-        scratch_shapes=[
-            pltpu.VMEM((len(weights), deep, width), BF),
-            pltpu.VMEM((QB, width), F32),
-            pltpu.SemaphoreType.DMA((len(weights),)),
-        ],
-        compiler_params=params(14),
+        compiler_params=params(10),
         cost_estimate=pl.CostEstimate(
             flops=1_000_000_000, bytes_accessed=9_000_000, transcendentals=0
         ),
         name="project",
-    )(spot, att, *weights)
+    )(mine, theirs, *others, weights)
 
 
 def layer(tokens, wq, wk, wv, wo, chosen):
@@ -325,6 +356,8 @@
     per = tokens.shape[0] // KB
 
     kv = rows_project(tokens, (wk, wv), 60)
+
+    kv, turn = lax.optimization_barrier((kv, tp.reshape(1)))
 
     row = jnp.stack([chosen] + [lax.ppermute(chosen, "kv", along_x(-r)) for r in range(1, NX)])
 
@@ -361,18 +394,17 @@
         recv.append([lax.ppermute(a, "kv", along_x(r)) for a, r in zip(sent, beside)])
     wm = lax.ppermute(wo, "tp", along_y(1))
     wp = lax.ppermute(wo, "tp", along_y(-1))
-    weights = [wo, wm, wp, lax.ppermute(wm, "tp", along_y(1))]
+    weights = [wo, wm, lax.ppermute(wm, "tp", along_y(1)), wp]
     weights += [lax.ppermute(w, "tp", CORES) for w in weights]
 
     q = rows_project(tokens, (wq,), 60)
     line = [held[d] for d in order]
     cut = len(batches[0]) + len(batches[1])
     sums = attend_early(want, bias, q, line[:cut], recv[:2])
-    mixed = attend_late(want, bias, q, sums, line[cut:], recv[2:])
-    att = lax.all_to_all(mixed.reshape(2 * NY, QB, -1), "tp", 0, 0, tiled=True)
-    y, c = tp // 2, tp % 2
-    rows = jnp.stack([y, (y - 1) % NY, (y + 1) % NY, (y + 2) % NY]) * 2
-    return project(jnp.stack([rows + c, rows + 1 - c]), att, weights)
+    mine, cross = attend_late(want, turn, bias, q, sums, line[cut:], recv[2:])
+    theirs = lax.ppermute(cross, "tp", CORES)
+    others = [lax.ppermute(a, "tp", along_y(n + 1)) for n, a in enumerate(pack(mine, theirs))]
+    return project(mine, theirs, others, stage(weights))
 
 
 def solution(mesh):

time: 138 us -> 138 us (level)
  waiting for transfers between devices: 45.7 us -> 36.2 us
  local copies, waits for them, and re-layouts: 14.9 us -> 20.5 us
  starting transfers between devices: 50 us -> 53.5 us
    all_to_all x1 -> x0, waiting for transfers between devices: 10.2 us -> none  [layer(): att = lax.all_to_all(mixed.reshape(2 * NY, QB, -1), 'tp', 0, 0, tiled=True)]
    unnamed x58, local copies, waits for them, and re-layouts: 14.2 us -> 19.9 us
    ppermute x1 -> x5, starting transfers between devices: 1.47 us -> 6.94 us  [the longest x3 5.59 us: layer(): lax.ppermute(a, 'tp', along_y(n + 1))]
    all_to_all x1 -> x0, starting transfers between devices: 4.19 us -> none  [layer(): att = lax.all_to_all(mixed.reshape(2 * NY, QB, -1), 'tp', 0, 0, tiled=True)]
    ppermute x4, waiting for transfers between devices: 10.4 us -> 7 us  [layer(): up = held[step] = lax.ppermute(up, 'kv', along_z(1))]
    ppermute x1 -> x5, waiting for transfers between devices: 0.01 us -> 3.22 us  [the longest x3 1.69 us: layer(): lax.ppermute(a, 'tp', along_y(n + 1))]
    ppermute x12, starting transfers between devices: 21.6 us -> 24.8 us  [layer(): lax.ppermute(a, 'kv', along_x(r))]
    pallas_call x2 -> x4, Pallas kernels: 8.69 us -> 8.06 us  [the longest x1 3.25 us: stage(): pl.pallas_call(stage_body, out_shape=jax.ShapeDtypeStruct((len(weights),...]
  transfers between devices with their start and end apart: 30 -> 33, of which waited for: 10 -> 12; matrix products, arithmetic and copies ran while one was open for 1% -> 2% of each run, Pallas kernels for 11% -> 13%
where the time goes in v4:
time: 138 us; the launch traced here: 137 us
  starting transfers between devices  53.5 us (39%)
  waiting for transfers between devices  36.2 us (26%)
  Pallas kernels  25.4 us (18%)
  local copies, waits for them, and re-layouts  20.5 us (15%)
  other arithmetic  1.56 us (1%)
    ppermute x12, waiting for transfers between devices, layer(): lax.ppermute(a, 'kv', along_x(r))  25.6 us
    ppermute x12, starting transfers between devices, layer(): lax.ppermute(a, 'kv', along_x(r))  24.8 us
    unnamed x58, local copies, waits for them, and re-layouts  19.9 us
    pallas_call x2, Pallas kernels, rows_project(): pl.pallas_call(rows_body(len(weights), parts), out_shape=jax.ShapeDtypeSt...  10.3 us
    ppermute x3, starting transfers between devices, layer(): down = held[NZ - step] = lax.ppermute(down, 'kv', along_z(-1))  9.74 us
    ppermute x4, waiting for transfers between devices, layer(): up = held[step] = lax.ppermute(up, 'kv', along_z(1))  7 us
    ppermute x3, starting transfers between devices, layer(): lax.ppermute(a, 'tp', along_y(n + 1))  5.59 us
    ppermute x3, starting transfers between devices, layer(): lax.ppermute(chosen, 'kv', along_x(-r))  4.76 us
  transfers between devices with their start and end apart: 33, of which 12 were waited for; matrix products, arithmetic and copies ran while one was open for 2% of the time, Pallas kernels for 13%

profile of v4, /device:TPU:2, one launch (start us, length us, event | category | flops | bytes accessed | tf_op | source)
XLA Modules:
  0.0 137.3 jit_solution(367807962689498292)
XLA Ops:
  0.0 5.2 %shard_map.91.refs_0_ = bf16[1024,256]{1,0:T(8,128)(2,1)} custom-call(bf16[1024,2048]{1,0:T(8,128)(2,1)} %tok.3, bf16[2048,128]{1,0:T(8,128)(2,1)} %refs_0_.3, bf16[2048,128]{1,0:T(8,128)(2,1)} %refs_1_.1), custom_call_target="tpu_custom_call" | custom-call | flops 1000000000 | bytes 6000000 | tf_op jit(solution)/shard_map/pallas_call | solution.py:78
  5.2 2.0 %collective-permute-start.3 = (bf16[1024,256]{1,0:T(8,128)(2,1)}, bf16[1024,256]{1,0:T(8,128)(2,1)S(1)}, u32[]{:S(2)}, u32[]{:S(2)}) collective-permute-start(bf16[1024,256]{1,0:T(8,128)(2,1)} %shard_map.91.refs_0_), channel_id=1, source_target_pairs={{0,32},{8,40},{16,48},{24,56},{32,64},{40,72},{48,80},{56,88},{64,... | collective-permute-start | bytes 1572872 | tf_op jit(solution)/shard_map/ppermute | solution.py:385
  7.2 4.0 %collective-permute-start.4 = (bf16[1024,256]{1,0:T(8,128)(2,1)}, bf16[1024,256]{1,0:T(8,128)(2,1)S(1)}, u32[]{:S(2)}, u32[]{:S(2)}) collective-permute-start(bf16[1024,256]{1,0:T(8,128)(2,1)} %shard_map.91.refs_0_), channel_id=1, source_target_pairs={{0,224},{8,232},{16,240},{24,248},{32,0},{40,8},{48,16},{56,24},{6... | collective-permute-start | bytes 1572872 | tf_op jit(solution)/shard_map/ppermute | solution.py:387
  11.8 2.4 %collective-permute-start.1 = (s32[8,12]{1,0:T(8,128)}, s32[8,12]{1,0:T(8,128)S(1)}, u32[]{:S(2)}, u32[]{:S(2)}) collective-permute-start(s32[8,12]{1,0:T(8,128)} %param.14), channel_id=1, source_target_pairs={{0,16},{8,24},{16,0},{24,8},{32,48},{40,56},{48,32},{56,40},{64,80... | collective-permute-start | bytes 1160 | tf_op jit(solution)/shard_map/ppermute | solution.py:362
  14.2 1.8 %collective-permute-start.2 = (s32[8,12]{1,0:T(8,128)}, s32[8,12]{1,0:T(8,128)S(1)}, u32[]{:S(2)}, u32[]{:S(2)}) collective-permute-start(s32[8,12]{1,0:T(8,128)} %param.14), channel_id=1, source_target_pairs={{0,8},{8,16},{16,24},{24,0},{32,40},{40,48},{48,56},{56,32},{64,72... | collective-permute-start | bytes 1160 | tf_op jit(solution)/shard_map/ppermute | solution.py:362
  16.7 1.7 %collective-permute-start.26 = (bf16[256,2048]{1,0:T(8,128)(2,1)}, bf16[256,2048]{1,0:T(8,128)(2,1)}, u32[]{:S(2)}, u32[]{:S(2)}) collective-permute-start(bf16[256,2048]{1,0:T(8,128)(2,1)} %refs_0_.5), channel_id=1, source_target_pairs={{0,2},{1,3},{2,4},{3,5},{4,6},{5,7},{6,0},{7,1},{8,10},{9,11},{10,... | collective-permute-start | bytes 3145736 | tf_op jit(solution)/shard_map/ppermute | solution.py:395
  19.4 3.9 %collective-permute-done.3.refs_1_ = bf16[1024,256]{1,0:T(8,128)(2,1)S(1)} collective-permute-done((bf16[1024,256]{1,0:T(8,128)(2,1)}, bf16[1024,256]{1,0:T(8,128)(2,1)S(1)}, u32[]{:S(2)}, u32[]{:S(2)}) %collective-permute-start.3) | collective-permute-done | bytes 524320 | tf_op jit(solution)/shard_map/ppermute | solution.py:385
  23.3 1.0 copy-done.1
  24.3 0.7 shard_map.93
  25.1 1.6 %collective-permute-start.7 = (bf16[3,8,32,256]{3,2,1,0:T(8,128)(2,1)S(1)}, bf16[3,8,32,256]{3,2,1,0:T(8,128)(2,1)S(1)}, u32[]{:S(2)}, u32[]{:S(2)}) collective-permute-start(bf16[3,8,32,256]{3,2,1,0:T(8,128)(2,1)S(1)} %get-tuple-element.29), channel_id=1, source_target_pairs={{0,8},{8,16},{16,24},{24,0},{32,40},{40,48},{48,56},{56,32},{64,72... | collective-permute-start | bytes 1179656 | tf_op jit(solution)/shard_map/ppermute | solution.py:394
  26.6 3.0 %collective-permute-start.28 = (bf16[256,2048]{1,0:T(8,128)(2,1)}, bf16[256,2048]{1,0:T(8,128)(2,1)}, u32[]{:S(2)}, u32[]{:S(2)}) collective-permute-start(bf16[256,2048]{1,0:T(8,128)(2,1)} %refs_0_.5), channel_id=1, source_target_pairs={{0,6},{1,7},{2,0},{3,1},{4,2},{5,3},{6,4},{7,5},{8,14},{9,15},{10,... | collective-permute-start | bytes 3145736 | tf_op jit(solution)/shard_map/ppermute | solution.py:396
  29.6 3.2 %collective-permute-start.6 = (bf16[1024,256]{1,0:T(8,128)(2,1)S(1)}, bf16[1024,256]{1,0:T(8,128)(2,1)S(1)}, u32[]{:S(2)}, u32[]{:S(2)}) collective-permute-start(bf16[1024,256]{1,0:T(8,128)(2,1)S(1)} %collective-permute-done.4.refs_2_), channel_id=1, source_target_pairs={{0,224},{8,232},{16,240},{24,248},{32,0},{40,8},{48,16},{56,24},{6... | collective-permute-start | bytes 1572872 | tf_op jit(solution)/shard_map/ppermute | solution.py:387
  32.9 2.6 %collective-permute-done.7.refs_5_ = bf16[3,8,32,256]{3,2,1,0:T(8,128)(2,1)S(1)} collective-permute-done((bf16[3,8,32,256]{3,2,1,0:T(8,128)(2,1)S(1)}, bf16[3,8,32,256]{3,2,1,0:T(8,128)(2,1)S(1)}, u32[]{:S(2)}, u32[]{:S(2)}) %collective-permute-start.7) | collective-permute-done | bytes 393248 | tf_op jit(solution)/shard_map/ppermute | solution.py:394
  35.5 2.1 %collective-permute-start.8 = (bf16[3,8,32,256]{3,2,1,0:T(8,128)(2,1)S(1)}, bf16[3,8,32,256]{3,2,1,0:T(8,128)(2,1)S(1)}, u32[]{:S(2)}, u32[]{:S(2)}) collective-permute-start(bf16[3,8,32,256]{3,2,1,0:T(8,128)(2,1)S(1)} %get-tuple-element.30), channel_id=1, source_target_pairs={{0,16},{8,24},{16,0},{24,8},{32,48},{40,56},{48,32},{56,40},{64,80... | collective-permute-start | bytes 1179656 | tf_op jit(solution)/shard_map/ppermute | solution.py:394
  37.7 3.1 %collective-permute-done.5.refs_0_.refs_3_ = bf16[1024,256]{1,0:T(8,128)(2,1)S(1)} collective-permute-done((bf16[1024,256]{1,0:T(8,128)(2,1)S(1)}, bf16[1024,256]{1,0:T(8,128)(2,1)S(1)}, u32[]{:S(2)}, u32[]{:S(2)}) %collective-permute-start.5) | collective-permute-done | bytes 524320 | tf_op jit(solution)/shard_map/ppermute | solution.py:385
  40.8 5.9 %collective-permute-done.8.refs_6_ = bf16[3,8,32,256]{3,2,1,0:T(8,128)(2,1)S(1)} collective-permute-done((bf16[3,8,32,256]{3,2,1,0:T(8,128)(2,1)S(1)}, bf16[3,8,32,256]{3,2,1,0:T(8,128)(2,1)S(1)}, u32[]{:S(2)}, u32[]{:S(2)}) %collective-permute-start.8) | collective-permute-done | bytes 393248 | tf_op jit(solution)/shard_map/ppermute | solution.py:394
  46.7 0.8 copy-done.6
  47.5 1.7 %collective-permute-start.9 = (bf16[3,8,32,256]{3,2,1,0:T(8,128)(2,1)S(1)}, bf16[3,8,32,256]{3,2,1,0:T(8,128)(2,1)S(1)}, u32[]{:S(2)}, u32[]{:S(2)}) collective-permute-start(bf16[3,8,32,256]{3,2,1,0:T(8,128)(2,1)S(1)} %get-tuple-element.31), channel_id=1, source_target_pairs={{0,24},{8,0},{16,8},{24,16},{32,56},{40,32},{48,40},{56,48},{64,88... | collective-permute-start | bytes 1179656 | tf_op jit(solution)/shard_map/ppermute | solution.py:394
  49.2 2.5 %collective-permute-start.14 = (bf16[1024,256]{1,0:T(8,128)(2,1)S(1)}, bf16[1024,256]{1,0:T(8,128)(2,1)S(1)}, u32[]{:S(2)}, u32[]{:S(2)}) collective-permute-start(bf16[1024,256]{1,0:T(8,128)(2,1)S(1)} %collective-permute-done.6.refs_1_.refs_4_), channel_id=1, source_target_pairs={{0,224},{8,232},{16,240},{24,248},{32,0},{40,8},{48,16},{56,24},{6... | collective-permute-start | bytes 1572872 | tf_op jit(solution)/shard_map/ppermute | solution.py:387
  51.7 1.3 collective-permute-start.27
  53.7 2.6 %collective-permute-done.9.refs_7_ = bf16[3,8,32,256]{3,2,1,0:T(8,128)(2,1)S(1)} collective-permute-done((bf16[3,8,32,256]{3,2,1,0:T(8,128)(2,1)S(1)}, bf16[3,8,32,256]{3,2,1,0:T(8,128)(2,1)S(1)}, u32[]{:S(2)}, u32[]{:S(2)}) %collective-permute-start.9) | collective-permute-done | bytes 393248 | tf_op jit(solution)/shard_map/ppermute | solution.py:394
  56.2 1.5 %collective-permute-start.10 = (bf16[2,8,32,256]{3,2,1,0:T(8,128)(2,1)S(1)}, bf16[2,8,32,256]{3,2,1,0:T(8,128)(2,1)S(1)}, u32[]{:S(2)}, u32[]{:S(2)}) collective-permute-start(bf16[2,8,32,256]{3,2,1,0:T(8,128)(2,1)S(1)} %get-tuple-element.32), channel_id=1, source_target_pairs={{0,8},{8,16},{16,24},{24,0},{32,40},{40,48},{48,56},{56,32},{64,72... | collective-permute-start | bytes 786440 | tf_op jit(solution)/shard_map/ppermute | solution.py:394
  57.7 2.4 %collective-permute-start.11 = (bf16[2,8,32,256]{3,2,1,0:T(8,128)(2,1)S(1)}, bf16[2,8,32,256]{3,2,1,0:T(8,128)(2,1)S(1)}, u32[]{:S(2)}, u32[]{:S(2)}) collective-permute-start(bf16[2,8,32,256]{3,2,1,0:T(8,128)(2,1)S(1)} %get-tuple-element.33), channel_id=1, source_target_pairs={{0,16},{8,24},{16,0},{24,8},{32,48},{40,56},{48,32},{56,40},{64,80... | collective-permute-start | bytes 786440 | tf_op jit(solution)/shard_map/ppermute | solution.py:394
  60.5 1.8 %collective-permute-start.12 = (bf16[2,8,32,256]{3,2,1,0:T(8,128)(2,1)S(1)}, bf16[2,8,32,256]{3,2,1,0:T(8,128)(2,1)S(1)}, u32[]{:S(2)}, u32[]{:S(2)}) collective-permute-start(bf16[2,8,32,256]{3,2,1,0:T(8,128)(2,1)S(1)} %get-tuple-element.34), channel_id=1, source_target_pairs={{0,24},{8,0},{16,8},{24,16},{32,56},{40,32},{48,40},{56,48},{64,88... | collective-permute-start | bytes 786440 | tf_op jit(solution)/shard_map/ppermute | solution.py:394
  63.0 3.6 %collective-permute-done.10.refs_8_ = bf16[2,8,32,256]{3,2,1,0:T(8,128)(2,1)S(1)} collective-permute-done((bf16[2,8,32,256]{3,2,1,0:T(8,128)(2,1)S(1)}, bf16[2,8,32,256]{3,2,1,0:T(8,128)(2,1)S(1)}, u32[]{:S(2)}, u32[]{:S(2)}) %collective-permute-start.10) | collective-permute-done | bytes 262176 | tf_op jit(solution)/shard_map/ppermute | solution.py:394
  66.7 0.7 copy-done.10
  67.4 3.0 %collective-permute-start.16 = (bf16[2,8,32,256]{3,2,1,0:T(8,128)(2,1)S(1)}, bf16[2,8,32,256]{3,2,1,0:T(8,128)(2,1)S(1)}, u32[]{:S(2)}, u32[]{:S(2)}) collective-permute-start(bf16[2,8,32,256]{3,2,1,0:T(8,128)(2,1)S(1)} %get-tuple-element.38), channel_id=1, source_target_pairs={{0,8},{8,16},{16,24},{24,0},{32,40},{40,48},{48,56},{56,32},{64,72... | collective-permute-start | bytes 786440 | tf_op jit(solution)/shard_map/ppermute | solution.py:394
  70.4 0.7 copy-done.12
  71.1 2.4 %collective-permute-start.17 = (bf16[2,8,32,256]{3,2,1,0:T(8,128)(2,1)S(1)}, bf16[2,8,32,256]{3,2,1,0:T(8,128)(2,1)S(1)}, u32[]{:S(2)}, u32[]{:S(2)}) collective-permute-start(bf16[2,8,32,256]{3,2,1,0:T(8,128)(2,1)S(1)} %get-tuple-element.39), channel_id=1, source_target_pairs={{0,16},{8,24},{16,0},{24,8},{32,48},{40,56},{48,32},{56,40},{64,80... | collective-permute-start | bytes 786440 | tf_op jit(solution)/shard_map/ppermute | solution.py:394
  73.5 0.7 copy-done.16
  74.2 2.2 %collective-permute-start.18 = (bf16[2,8,32,256]{3,2,1,0:T(8,128)(2,1)S(1)}, bf16[2,8,32,256]{3,2,1,0:T(8,128)(2,1)S(1)}, u32[]{:S(2)}, u32[]{:S(2)}) collective-permute-start(bf16[2,8,32,256]{3,2,1,0:T(8,128)(2,1)S(1)} %get-tuple-element.40), channel_id=1, source_target_pairs={{0,24},{8,0},{16,8},{24,16},{32,56},{40,32},{48,40},{56,48},{64,88... | collective-permute-start | bytes 786440 | tf_op jit(solution)/shard_map/ppermute | solution.py:394
  76.4 0.7 copy-done.14
  77.7 1.3 shard_map.96
  79.0 0.8 copy-done.3
  79.8 0.7 copy-done.18
  80.6 1.6 %collective-permute-done.18.refs_5_ = bf16[2,8,32,256]{3,2,1,0:T(8,128)(2,1)S(1)} collective-permute-done((bf16[2,8,32,256]{3,2,1,0:T(8,128)(2,1)S(1)}, bf16[2,8,32,256]{3,2,1,0:T(8,128)(2,1)S(1)}, u32[]{:S(2)}, u32[]{:S(2)}) %collective-permute-start.18) | collective-permute-done | bytes 262176 | tf_op jit(solution)/shard_map/ppermute | solution.py:394
  82.2 0.7 copy-done.20
  82.9 2.0 %collective-permute-start.19 = (bf16[1,8,32,256]{3,2,1,0:T(8,128)(2,1)S(1)}, bf16[1,8,32,256]{3,2,1,0:T(8,128)(2,1)S(1)}, u32[]{:S(2)}, u32[]{:S(2)}) collective-permute-start(bf16[1,8,32,256]{3,2,1,0:T(8,128)(2,1)S(1)} %get-tuple-element.41), channel_id=1, source_target_pairs={{0,8},{8,16},{16,24},{24,0},{32,40},{40,48},{48,56},{56,32},{64,72... | collective-permute-start | bytes 393224 | tf_op jit(solution)/shard_map/ppermute | solution.py:394
  85.4 3.8 %collective-permute-done.19.refs_6_ = bf16[1,8,32,256]{3,2,1,0:T(8,128)(2,1)S(1)} collective-permute-done((bf16[1,8,32,256]{3,2,1,0:T(8,128)(2,1)S(1)}, bf16[1,8,32,256]{3,2,1,0:T(8,128)(2,1)S(1)}, u32[]{:S(2)}, u32[]{:S(2)}) %collective-permute-start.19) | collective-permute-done | bytes 131104 | tf_op jit(solution)/shard_map/ppermute | solution.py:394
  89.8 1.3 collective-permute-start.20
  91.3 5.4 %collective-permute-done.20.refs_7_ = bf16[1,8,32,256]{3,2,1,0:T(8,128)(2,1)S(1)} collective-permute-done((bf16[1,8,32,256]{3,2,1,0:T(8,128)(2,1)S(1)}, bf16[1,8,32,256]{3,2,1,0:T(8,128)(2,1)S(1)}, u32[]{:S(2)}, u32[]{:S(2)}) %collective-permute-start.20) | collective-permute-done | bytes 131104 | tf_op jit(solution)/shard_map/ppermute | solution.py:394
  97.3 2.7 %collective-permute-start.21 = (bf16[1,8,32,256]{3,2,1,0:T(8,128)(2,1)}, bf16[1,8,32,256]{3,2,1,0:T(8,128)(2,1)}, u32[]{:S(2)}, u32[]{:S(2)}) collective-permute-start(bf16[1,8,32,256]{3,2,1,0:T(8,128)(2,1)} %get-tuple-element.43), channel_id=1, source_target_pairs={{0,24},{8,0},{16,8},{24,16},{32,56},{40,32},{48,40},{56,48},{64,88... | collective-permute-start | bytes 393224 | tf_op jit(solution)/shard_map/ppermute | solution.py:394
  100.0 5.1 %shard_map.92.q = bf16[1024,256]{1,0:T(8,128)(2,1)} custom-call(bf16[1024,2048]{1,0:T(8,128)(2,1)} %tok.3, bf16[2048,256]{1,0:T(8,128)(2,1)} %refs_0_.4), custom_call_target="tpu_custom_call" | custom-call | flops 1000000000 | bytes 6000000 | tf_op jit(solution)/shard_map/pallas_call | solution.py:78
  105.1 1.0 copy-done
  106.2 1.0 copy-done.7
  107.2 1.0 copy-done.9
  108.2 0.9 copy-done.11
  109.1 0.9 copy-done.13
  110.1 0.9 copy-done.17
  111.0 3.6 %early.1 = (f32[2048,128]{1,0:T(8,128)S(1)}, f32[2048,128]{1,0:T(8,128)S(1)}, f32[2048,128]{1,0:T(8,128)S(1)}) custom-call(s32[4,64]{1,0:T(4,128)S(1)} %fusion.2.want, f32[8,1024]{1,0:T(8,128)S(1)} %or_select_fusion.bias, bf16[1024,256]{1,0:T(8,128)(2,1)S(1)} %copy-done, bf16[1024,256]{1,0:T(8,128)(2,1)S(1)} %copy-done.2, ...), custom_call_target="tpu_custom_call" | custom-call | flops 900000000 | bytes 6000000 | tf_op jit(solution)/shard_map/early/pallas_call | solution.py:245
  114.6 1.0 copy-done.4
  115.7 0.9 copy-done.15
  116.6 0.9 copy-done.19
  117.6 0.9 copy-done.21
  118.5 0.9 copy-done.23
  119.4 0.9 copy-done.25
  120.3 2.7 %late.1 = (bf16[4,128,256]{2,1,0:T(8,128)(2,1)S(1)}, bf16[4,128,256]{2,1,0:T(8,128)(2,1)S(1)}) custom-call(s32[4,64]{1,0:T(4,128)S(1)} %fusion.2.want, s32[1]{0:T(128)} %bitcast.4.turn, f32[8,1024]{1,0:T(8,128)S(1)} %or_select_fusion.bias, bf16[1024,256]{1,0:T(8,128)(2,1)S(1)} %copy-done, f32[2048,128]{1,0:T(8,128)S(1)} %get-tuple-element.35.acc, ...), custom_call_target="tpu_custom_call" | custom-call | flops 400000000 | bytes 6000000 | tf_op jit(solution)/shard_map/late/pallas_call | solution.py:267
  123.1 1.5 %collective-permute-done.22.theirs = bf16[4,128,256]{2,1,0:T(8,128)(2,1)S(1)} collective-permute-done((bf16[4,128,256]{2,1,0:T(8,128)(2,1)S(1)}, bf16[4,128,256]{2,1,0:T(8,128)(2,1)S(1)}, u32[]{:S(2)}, u32[]{:S(2)}) %collective-permute-start.22) | collective-permute-done | bytes 262176 | tf_op jit(solution)/shard_map/ppermute | solution.py:405
  124.7 1.3 collective-permute-start.23
  126.0 2.9 %collective-permute-start.24 = (bf16[2,128,256]{2,1,0:T(8,128)(2,1)S(1)}, bf16[2,128,256]{2,1,0:T(8,128)(2,1)S(1)}, u32[]{:S(2)}, u32[]{:S(2)}) collective-permute-start(bf16[2,128,256]{2,1,0:T(8,128)(2,1)S(1)} %get-tuple-element.47), channel_id=1, source_target_pairs={{0,4},{1,5},{2,6},{3,7},{4,0},{5,1},{6,2},{7,3},{8,12},{9,13},{10,... | collective-permute-start | bytes 393224 | tf_op jit(solution)/shard_map/ppermute | solution.py:406
  128.9 1.3 collective-permute-start.25
  130.3 3.2 %stage.1.refs_3_ = bf16[8,256,2048]{2,1,0:T(8,128)(2,1)S(1)} custom-call(bf16[256,2048]{1,0:T(8,128)(2,1)S(1)} %copy-done.5, bf16[256,2048]{1,0:T(8,128)(2,1)} %collective-permute-done.26.refs_1_, bf16[256,2048]{1,0:T(8,128)(2,1)} %collective-permute-done.27.refs_2_, bf16[256,2048]{1,0:T(8,128)(2,1)} %collective-permute-done.28.refs_3_, ...), custom_call_target="tpu_custom_call" | custom-call | flops 1000000000 | bytes 16000000 | tf_op jit(solution)/shard_map/stage/pallas_call | solution.py:313
  133.5 1.7 %collective-permute-done.24.refs_1_ = bf16[2,128,256]{2,1,0:T(8,128)(2,1)S(1)} collective-permute-done((bf16[2,128,256]{2,1,0:T(8,128)(2,1)S(1)}, bf16[2,128,256]{2,1,0:T(8,128)(2,1)S(1)}, u32[]{:S(2)}, u32[]{:S(2)}) %collective-permute-start.24) | collective-permute-done | bytes 131104 | tf_op jit(solution)/shard_map/ppermute | solution.py:406
  135.2 2.1 %project.1 = bf16[128,2048]{1,0:T(8,128)(2,1)} custom-call(bf16[4,128,256]{2,1,0:T(8,128)(2,1)S(1)} %get-tuple-element.44.mine, bf16[4,128,256]{2,1,0:T(8,128)(2,1)S(1)} %collective-permute-done.22.theirs, bf16[2,128,256]{2,1,0:T(8,128)(2,1)S(1)} %collective-permute-done.23.refs_0_, bf16[2,128,256]{2,1,0:T(8,128)(2,1)S(1)} %collective-permute-done.24.refs_1_, ...), custom_call_target="tpu_custom_call" | custom-call | flops 1000000000 | bytes 9000000 | tf_op jit(solution)/shard_map/project/pallas_call | solution.py:339
  (80 shorter events, 6.6 us)
Async XLA Ops:
  0.0 77.7 %copy-start.27 = (s32[1024]{0:T(1024)S(1)}, s32[1024]{0:T(1024)}, u32[]{:S(2)}) copy-start(s32[1024]{0:T(1024)} %constant.114) | copy-start | bytes 12292
  0.0 77.7 %copy-start.28 = (s32[1024]{0:T(1024)S(1)}, s32[1024]{0:T(1024)}, u32[]{:S(2)}) copy-start(s32[1024]{0:T(1024)} %constant.115) | copy-start | bytes 12292
  0.0 85.0 %copy-start.26 = (s32[8,12]{1,0:T(8,128)S(1)}, s32[8,12]{1,0:T(8,128)}, u32[]{:S(2)}) copy-start(s32[8,12]{1,0:T(8,128)} %param.14) | copy-start | bytes 1156
  5.2 18.1 %collective-permute-start.3 = (bf16[1024,256]{1,0:T(8,128)(2,1)}, bf16[1024,256]{1,0:T(8,128)(2,1)S(1)}, u32[]{:S(2)}, u32[]{:S(2)}) collective-permute-start(bf16[1024,256]{1,0:T(8,128)(2,1)} %shard_map.91.refs_0_), channel_id=1, source_target_pairs={{0,32},{8,40},{16,48},{24,56},{32,64},{40,72},{48,80},{56,88},{64,... | collective-permute-start | bytes 1572872 | tf_op jit(solution)/shard_map/ppermute | solution.py:385
  7.2 16.1 %collective-permute-start.4 = (bf16[1024,256]{1,0:T(8,128)(2,1)}, bf16[1024,256]{1,0:T(8,128)(2,1)S(1)}, u32[]{:S(2)}, u32[]{:S(2)}) collective-permute-start(bf16[1024,256]{1,0:T(8,128)(2,1)} %shard_map.91.refs_0_), channel_id=1, source_target_pairs={{0,224},{8,232},{16,240},{24,248},{32,0},{40,8},{48,16},{56,24},{6... | collective-permute-start | bytes 1572872 | tf_op jit(solution)/shard_map/ppermute | solution.py:387
  11.2 5.4 %collective-permute-start = (s32[8,12]{1,0:T(8,128)}, s32[8,12]{1,0:T(8,128)S(1)}, u32[]{:S(2)}, u32[]{:S(2)}) collective-permute-start(s32[8,12]{1,0:T(8,128)} %param.14), channel_id=1, source_target_pairs={{0,24},{8,0},{16,8},{24,16},{32,56},{40,32},{48,40},{56,48},{64,88... | collective-permute-start | bytes 1160 | tf_op jit(solution)/shard_map/ppermute | solution.py:362
  11.8 6.5 %collective-permute-start.1 = (s32[8,12]{1,0:T(8,128)}, s32[8,12]{1,0:T(8,128)S(1)}, u32[]{:S(2)}, u32[]{:S(2)}) collective-permute-start(s32[8,12]{1,0:T(8,128)} %param.14), channel_id=1, source_target_pairs={{0,16},{8,24},{16,0},{24,8},{32,48},{40,56},{48,32},{56,40},{64,80... | collective-permute-start | bytes 1160 | tf_op jit(solution)/shard_map/ppermute | solution.py:362
  14.2 4.1 %collective-permute-start.2 = (s32[8,12]{1,0:T(8,128)}, s32[8,12]{1,0:T(8,128)S(1)}, u32[]{:S(2)}, u32[]{:S(2)}) collective-permute-start(s32[8,12]{1,0:T(8,128)} %param.14), channel_id=1, source_target_pairs={{0,8},{8,16},{16,24},{24,0},{32,40},{40,48},{48,56},{56,32},{64,72... | collective-permute-start | bytes 1160 | tf_op jit(solution)/shard_map/ppermute | solution.py:362
  16.7 35.0 %collective-permute-start.26 = (bf16[256,2048]{1,0:T(8,128)(2,1)}, bf16[256,2048]{1,0:T(8,128)(2,1)}, u32[]{:S(2)}, u32[]{:S(2)}) collective-permute-start(bf16[256,2048]{1,0:T(8,128)(2,1)} %refs_0_.5), channel_id=1, source_target_pairs={{0,2},{1,3},{2,4},{3,5},{4,6},{5,7},{6,0},{7,1},{8,10},{9,11},{10,... | collective-permute-start | bytes 3145736 | tf_op jit(solution)/shard_map/ppermute | solution.py:395
  23.3 1.0 copy-start.1
  24.3 80.8 %copy-start.2 = (bf16[1024,256]{1,0:T(8,128)(2,1)S(1)}, bf16[1024,256]{1,0:T(8,128)(2,1)}, u32[]{:S(2)}) copy-start(bf16[1024,256]{1,0:T(8,128)(2,1)} %shard_map.91.refs_0_) | copy-start | bytes 1572868
  25.1 10.5 %collective-permute-start.7 = (bf16[3,8,32,256]{3,2,1,0:T(8,128)(2,1)S(1)}, bf16[3,8,32,256]{3,2,1,0:T(8,128)(2,1)S(1)}, u32[]{:S(2)}, u32[]{:S(2)}) collective-permute-start(bf16[3,8,32,256]{3,2,1,0:T(8,128)(2,1)S(1)} %get-tuple-element.29), channel_id=1, source_target_pairs={{0,8},{8,16},{16,24},{24,0},{32,40},{40,48},{48,56},{56,32},{64,72... | collective-permute-start | bytes 1179656 | tf_op jit(solution)/shard_map/ppermute | solution.py:394
  26.6 14.1 %collective-permute-start.5 = (bf16[1024,256]{1,0:T(8,128)(2,1)S(1)}, bf16[1024,256]{1,0:T(8,128)(2,1)S(1)}, u32[]{:S(2)}, u32[]{:S(2)}) collective-permute-start(bf16[1024,256]{1,0:T(8,128)(2,1)S(1)} %collective-permute-done.3.refs_1_), channel_id=1, source_target_pairs={{0,32},{8,40},{16,48},{24,56},{32,64},{40,72},{48,80},{56,88},{64,... | collective-permute-start | bytes 1572872 | tf_op jit(solution)/shard_map/ppermute | solution.py:385
  26.6 31.1 %collective-permute-start.28 = (bf16[256,2048]{1,0:T(8,128)(2,1)}, bf16[256,2048]{1,0:T(8,128)(2,1)}, u32[]{:S(2)}, u32[]{:S(2)}) collective-permute-start(bf16[256,2048]{1,0:T(8,128)(2,1)} %refs_0_.5), channel_id=1, source_target_pairs={{0,6},{1,7},{2,0},{3,1},{4,2},{5,3},{6,4},{7,5},{8,14},{9,15},{10,... | collective-permute-start | bytes 3145736 | tf_op jit(solution)/shard_map/ppermute | solution.py:396
  29.6 19.6 %collective-permute-start.6 = (bf16[1024,256]{1,0:T(8,128)(2,1)S(1)}, bf16[1024,256]{1,0:T(8,128)(2,1)S(1)}, u32[]{:S(2)}, u32[]{:S(2)}) collective-permute-start(bf16[1024,256]{1,0:T(8,128)(2,1)S(1)} %collective-permute-done.4.refs_2_), channel_id=1, source_target_pairs={{0,224},{8,232},{16,240},{24,248},{32,0},{40,8},{48,16},{56,24},{6... | collective-permute-start | bytes 1572872 | tf_op jit(solution)/shard_map/ppermute | solution.py:387
  35.5 11.1 %collective-permute-start.8 = (bf16[3,8,32,256]{3,2,1,0:T(8,128)(2,1)S(1)}, bf16[3,8,32,256]{3,2,1,0:T(8,128)(2,1)S(1)}, u32[]{:S(2)}, u32[]{:S(2)}) collective-permute-start(bf16[3,8,32,256]{3,2,1,0:T(8,128)(2,1)S(1)} %get-tuple-element.30), channel_id=1, source_target_pairs={{0,16},{8,24},{16,0},{24,8},{32,48},{40,56},{48,32},{56,40},{64,80... | collective-permute-start | bytes 1179656 | tf_op jit(solution)/shard_map/ppermute | solution.py:394
  40.8 17.0 %collective-permute-start.13 = (bf16[1024,256]{1,0:T(8,128)(2,1)S(1)}, bf16[1024,256]{1,0:T(8,128)(2,1)S(1)}, u32[]{:S(2)}, u32[]{:S(2)}) collective-permute-start(bf16[1024,256]{1,0:T(8,128)(2,1)S(1)} %collective-permute-done.5.refs_0_.refs_3_), channel_id=1, source_target_pairs={{0,32},{8,40},{16,48},{24,56},{32,64},{40,72},{48,80},{56,88},{64,... | collective-permute-start | bytes 1572872 | tf_op jit(solution)/shard_map/ppermute | solution.py:385
  46.7 0.8 copy-start.6
  47.5 8.8 %collective-permute-start.9 = (bf16[3,8,32,256]{3,2,1,0:T(8,128)(2,1)S(1)}, bf16[3,8,32,256]{3,2,1,0:T(8,128)(2,1)S(1)}, u32[]{:S(2)}, u32[]{:S(2)}) collective-permute-start(bf16[3,8,32,256]{3,2,1,0:T(8,128)(2,1)S(1)} %get-tuple-element.31), channel_id=1, source_target_pairs={{0,24},{8,0},{16,8},{24,16},{32,56},{40,32},{48,40},{56,48},{64,88... | collective-permute-start | bytes 1179656 | tf_op jit(solution)/shard_map/ppermute | solution.py:394
  49.2 11.3 %collective-permute-start.14 = (bf16[1024,256]{1,0:T(8,128)(2,1)S(1)}, bf16[1024,256]{1,0:T(8,128)(2,1)S(1)}, u32[]{:S(2)}, u32[]{:S(2)}) collective-permute-start(bf16[1024,256]{1,0:T(8,128)(2,1)S(1)} %collective-permute-done.6.refs_1_.refs_4_), channel_id=1, source_target_pairs={{0,224},{8,232},{16,240},{24,248},{32,0},{40,8},{48,16},{56,24},{6... | collective-permute-start | bytes 1572872 | tf_op jit(solution)/shard_map/ppermute | solution.py:387
  51.7 33.3 %collective-permute-start.27 = (bf16[256,2048]{1,0:T(8,128)(2,1)}, bf16[256,2048]{1,0:T(8,128)(2,1)}, u32[]{:S(2)}, u32[]{:S(2)}) collective-permute-start(bf16[256,2048]{1,0:T(8,128)(2,1)} %collective-permute-done.26.refs_1_), channel_id=1, source_target_pairs={{0,2},{1,3},{2,4},{3,5},{4,6},{5,7},{6,0},{7,1},{8,10},{9,11},{10,... | collective-permute-start | bytes 3145736 | tf_op jit(solution)/shard_map/ppermute | solution.py:397
  56.2 20.9 %copy-start.8 = (bf16[3,8,32,256]{3,2,1,0:T(8,128)(2,1)}, bf16[3,8,32,256]{3,2,1,0:T(8,128)(2,1)S(1)}, u32[]{:S(2)}) copy-start(bf16[3,8,32,256]{3,2,1,0:T(8,128)(2,1)S(1)} %collective-permute-done.9.refs_7_) | copy-start | bytes 1179652
  56.2 10.4 %collective-permute-start.10 = (bf16[2,8,32,256]{3,2,1,0:T(8,128)(2,1)S(1)}, bf16[2,8,32,256]{3,2,1,0:T(8,128)(2,1)S(1)}, u32[]{:S(2)}, u32[]{:S(2)}) collective-permute-start(bf16[2,8,32,256]{3,2,1,0:T(8,128)(2,1)S(1)} %get-tuple-element.32), channel_id=1, source_target_pairs={{0,8},{8,16},{16,24},{24,0},{32,40},{40,48},{48,56},{56,32},{64,72... | collective-permute-start | bytes 786440 | tf_op jit(solution)/shard_map/ppermute | solution.py:394
  57.7 19.4 %collective-permute-start.15 = (bf16[1024,256]{1,0:T(8,128)(2,1)S(1)}, bf16[1024,256]{1,0:T(8,128)(2,1)S(1)}, u32[]{:S(2)}, u32[]{:S(2)}) collective-permute-start(bf16[1024,256]{1,0:T(8,128)(2,1)S(1)} %collective-permute-done.13.refs_0_), channel_id=1, source_target_pairs={{0,32},{8,40},{16,48},{24,56},{32,64},{40,72},{48,80},{56,88},{64,... | collective-permute-start | bytes 1572872 | tf_op jit(solution)/shard_map/ppermute | solution.py:385
  57.7 12.6 %collective-permute-start.11 = (bf16[2,8,32,256]{3,2,1,0:T(8,128)(2,1)S(1)}, bf16[2,8,32,256]{3,2,1,0:T(8,128)(2,1)S(1)}, u32[]{:S(2)}, u32[]{:S(2)}) collective-permute-start(bf16[2,8,32,256]{3,2,1,0:T(8,128)(2,1)S(1)} %get-tuple-element.33), channel_id=1, source_target_pairs={{0,16},{8,24},{16,0},{24,8},{32,48},{40,56},{48,32},{56,40},{64,80... | collective-permute-start | bytes 786440 | tf_op jit(solution)/shard_map/ppermute | solution.py:394
  60.5 12.9 %collective-permute-start.12 = (bf16[2,8,32,256]{3,2,1,0:T(8,128)(2,1)S(1)}, bf16[2,8,32,256]{3,2,1,0:T(8,128)(2,1)S(1)}, u32[]{:S(2)}, u32[]{:S(2)}) collective-permute-start(bf16[2,8,32,256]{3,2,1,0:T(8,128)(2,1)S(1)} %get-tuple-element.34), channel_id=1, source_target_pairs={{0,24},{8,0},{16,8},{24,16},{32,56},{40,32},{48,40},{56,48},{64,88... | collective-permute-start | bytes 786440 | tf_op jit(solution)/shard_map/ppermute | solution.py:394
  66.7 0.7 copy-start.10
  67.4 9.0 %collective-permute-start.16 = (bf16[2,8,32,256]{3,2,1,0:T(8,128)(2,1)S(1)}, bf16[2,8,32,256]{3,2,1,0:T(8,128)(2,1)S(1)}, u32[]{:S(2)}, u32[]{:S(2)}) collective-permute-start(bf16[2,8,32,256]{3,2,1,0:T(8,128)(2,1)S(1)} %get-tuple-element.38), channel_id=1, source_target_pairs={{0,8},{8,16},{16,24},{24,0},{32,40},{40,48},{48,56},{56,32},{64,72... | collective-permute-start | bytes 786440 | tf_op jit(solution)/shard_map/ppermute | solution.py:394
  70.4 0.7 copy-start.12
  71.1 8.8 %collective-permute-start.17 = (bf16[2,8,32,256]{3,2,1,0:T(8,128)(2,1)S(1)}, bf16[2,8,32,256]{3,2,1,0:T(8,128)(2,1)S(1)}, u32[]{:S(2)}, u32[]{:S(2)}) collective-permute-start(bf16[2,8,32,256]{3,2,1,0:T(8,128)(2,1)S(1)} %get-tuple-element.39), channel_id=1, source_target_pairs={{0,16},{8,24},{16,0},{24,8},{32,48},{40,56},{48,32},{56,40},{64,80... | collective-permute-start | bytes 786440 | tf_op jit(solution)/shard_map/ppermute | solution.py:394
  73.5 0.7 copy-start.16
  74.2 8.0 %collective-permute-start.18 = (bf16[2,8,32,256]{3,2,1,0:T(8,128)(2,1)S(1)}, bf16[2,8,32,256]{3,2,1,0:T(8,128)(2,1)S(1)}, u32[]{:S(2)}, u32[]{:S(2)}) collective-permute-start(bf16[2,8,32,256]{3,2,1,0:T(8,128)(2,1)S(1)} %get-tuple-element.40), channel_id=1, source_target_pairs={{0,24},{8,0},{16,8},{24,16},{32,56},{40,32},{48,40},{56,48},{64,88... | collective-permute-start | bytes 786440 | tf_op jit(solution)/shard_map/ppermute | solution.py:394
  76.4 0.7 copy-start.14
  77.1 48.9 %collective-permute-start.29 = (bf16[256,2048]{1,0:T(8,128)(2,1)}, bf16[256,2048]{1,0:T(8,128)(2,1)}, u32[]{:S(2)}, u32[]{:S(2)}) collective-permute-start(bf16[256,2048]{1,0:T(8,128)(2,1)} %refs_0_.5), channel_id=1, source_target_pairs={{0,1},{1,0},{2,3},{3,2},{4,5},{5,4},{6,7},{7,6},{8,9},{9,8},{10,11... | collective-permute-start | bytes 3145736 | tf_op jit(solution)/shard_map/ppermute | solution.py:398
  77.2 51.8 %collective-permute-start.30 = (bf16[256,2048]{1,0:T(8,128)(2,1)}, bf16[256,2048]{1,0:T(8,128)(2,1)}, u32[]{:S(2)}, u32[]{:S(2)}) collective-permute-start(bf16[256,2048]{1,0:T(8,128)(2,1)} %collective-permute-done.26.refs_1_), channel_id=1, source_target_pairs={{0,1},{1,0},{2,3},{3,2},{4,5},{5,4},{6,7},{7,6},{8,9},{9,8},{10,11... | collective-permute-start | bytes 3145736 | tf_op jit(solution)/shard_map/ppermute | solution.py:398
  79.0 0.8 copy-start.3
  79.8 0.7 copy-start.18
  80.5 49.7 %collective-permute-start.32 = (bf16[256,2048]{1,0:T(8,128)(2,1)}, bf16[256,2048]{1,0:T(8,128)(2,1)}, u32[]{:S(2)}, u32[]{:S(2)}) collective-permute-start(bf16[256,2048]{1,0:T(8,128)(2,1)} %collective-permute-done.28.refs_3_), channel_id=1, source_target_pairs={{0,1},{1,0},{2,3},{3,2},{4,5},{5,4},{6,7},{7,6},{8,9},{9,8},{10,11... | collective-permute-start | bytes 3145736 | tf_op jit(solution)/shard_map/ppermute | solution.py:398
  82.2 0.7 copy-start.20
  82.9 6.2 %collective-permute-start.19 = (bf16[1,8,32,256]{3,2,1,0:T(8,128)(2,1)S(1)}, bf16[1,8,32,256]{3,2,1,0:T(8,128)(2,1)S(1)}, u32[]{:S(2)}, u32[]{:S(2)}) collective-permute-start(bf16[1,8,32,256]{3,2,1,0:T(8,128)(2,1)S(1)} %get-tuple-element.41), channel_id=1, source_target_pairs={{0,8},{8,16},{16,24},{24,0},{32,40},{40,48},{48,56},{56,32},{64,72... | collective-permute-start | bytes 393224 | tf_op jit(solution)/shard_map/ppermute | solution.py:394
  85.0 45.3 %collective-permute-start.31 = (bf16[256,2048]{1,0:T(8,128)(2,1)}, bf16[256,2048]{1,0:T(8,128)(2,1)}, u32[]{:S(2)}, u32[]{:S(2)}) collective-permute-start(bf16[256,2048]{1,0:T(8,128)(2,1)} %collective-permute-done.27.refs_2_), channel_id=1, source_target_pairs={{0,1},{1,0},{2,3},{3,2},{4,5},{5,4},{6,7},{7,6},{8,9},{9,8},{10,11... | collective-permute-start | bytes 3145736 | tf_op jit(solution)/shard_map/ppermute | solution.py:398
  89.2 0.6 copy-start.22
  89.8 6.8 %collective-permute-start.20 = (bf16[1,8,32,256]{3,2,1,0:T(8,128)(2,1)S(1)}, bf16[1,8,32,256]{3,2,1,0:T(8,128)(2,1)S(1)}, u32[]{:S(2)}, u32[]{:S(2)}) collective-permute-start(bf16[1,8,32,256]{3,2,1,0:T(8,128)(2,1)S(1)} %get-tuple-element.42), channel_id=1, source_target_pairs={{0,16},{8,24},{16,0},{24,8},{32,48},{40,56},{48,32},{56,40},{64,80... | collective-permute-start | bytes 393224 | tf_op jit(solution)/shard_map/ppermute | solution.py:394
  96.7 0.7 copy-start.24
  97.3 17.3 %collective-permute-start.21 = (bf16[1,8,32,256]{3,2,1,0:T(8,128)(2,1)}, bf16[1,8,32,256]{3,2,1,0:T(8,128)(2,1)}, u32[]{:S(2)}, u32[]{:S(2)}) collective-permute-start(bf16[1,8,32,256]{3,2,1,0:T(8,128)(2,1)} %get-tuple-element.43), channel_id=1, source_target_pairs={{0,24},{8,0},{16,8},{24,16},{32,56},{40,32},{48,40},{56,48},{64,88... | collective-permute-start | bytes 393224 | tf_op jit(solution)/shard_map/ppermute | solution.py:394
  105.1 1.0 copy-start
  106.2 1.0 copy-start.7
  107.2 1.0 copy-start.9
  108.2 0.9 copy-start.11
  109.1 0.9 copy-start.13
  110.1 0.9 copy-start.17
  111.0 19.2 %copy-start.5 = (bf16[256,2048]{1,0:T(8,128)(2,1)S(1)}, bf16[256,2048]{1,0:T(8,128)(2,1)}, u32[]{:S(2)}) copy-start(bf16[256,2048]{1,0:T(8,128)(2,1)} %refs_0_.5) | copy-start | bytes 3145732
  114.6 1.0 copy-start.4
  115.7 0.9 copy-start.15
  116.6 0.9 copy-start.19
  117.6 0.9 copy-start.21
  118.5 0.9 copy-start.23
  119.4 0.9 copy-start.25
  123.0 1.6 %collective-permute-start.22 = (bf16[4,128,256]{2,1,0:T(8,128)(2,1)S(1)}, bf16[4,128,256]{2,1,0:T(8,128)(2,1)S(1)}, u32[]{:S(2)}, u32[]{:S(2)}) collective-permute-start(bf16[4,128,256]{2,1,0:T(8,128)(2,1)S(1)} %get-tuple-element.45), channel_id=1, source_target_pairs={{0,1},{1,0},{2,3},{3,2},{4,5},{5,4},{6,7},{7,6},{8,9},{9,8},{10,11... | collective-permute-start | bytes 786440 | tf_op jit(solution)/shard_map/ppermute | solution.py:405
  124.7 8.9 %collective-permute-start.23 = (bf16[2,128,256]{2,1,0:T(8,128)(2,1)S(1)}, bf16[2,128,256]{2,1,0:T(8,128)(2,1)S(1)}, u32[]{:S(2)}, u32[]{:S(2)}) collective-permute-start(bf16[2,128,256]{2,1,0:T(8,128)(2,1)S(1)} %get-tuple-element.46), channel_id=1, source_target_pairs={{0,2},{1,3},{2,4},{3,5},{4,6},{5,7},{6,0},{7,1},{8,10},{9,11},{10,... | collective-permute-start | bytes 393224 | tf_op jit(solution)/shard_map/ppermute | solution.py:406
  126.0 9.2 %collective-permute-start.24 = (bf16[2,128,256]{2,1,0:T(8,128)(2,1)S(1)}, bf16[2,128,256]{2,1,0:T(8,128)(2,1)S(1)}, u32[]{:S(2)}, u32[]{:S(2)}) collective-permute-start(bf16[2,128,256]{2,1,0:T(8,128)(2,1)S(1)} %get-tuple-element.47), channel_id=1, source_target_pairs={{0,4},{1,5},{2,6},{3,7},{4,0},{5,1},{6,2},{7,3},{8,12},{9,13},{10,... | collective-permute-start | bytes 393224 | tf_op jit(solution)/shard_map/ppermute | solution.py:406
  128.9 6.3 %collective-permute-start.25 = (bf16[2,128,256]{2,1,0:T(8,128)(2,1)S(1)}, bf16[2,128,256]{2,1,0:T(8,128)(2,1)S(1)}, u32[]{:S(2)}, u32[]{:S(2)}) collective-permute-start(bf16[2,128,256]{2,1,0:T(8,128)(2,1)S(1)} %get-tuple-element.48), channel_id=1, source_target_pairs={{0,6},{1,7},{2,0},{3,1},{4,2},{5,3},{6,4},{7,5},{8,14},{9,15},{10,... | collective-permute-start | bytes 393224 | tf_op jit(solution)/shard_map/ppermute | solution.py:406
